TPU v7x, 512 devices: a whole 4x4x16 slice. The times are simulated.
512 devices in a mesh: ep: 128 (over z, x, core), tp: 4 (over y).
Axes of the slice: x: 4, y: 4, z: 16, core: 2. Of those that a mesh axis runs over, the one named last changes fastest.
Arguments:
- tokens: bfloat16 [16384, 1024], P('ep', 'tp'), may hold values from -6 to 6
- cotangent: bfloat16 [16384, 1024], P('ep', 'tp'), may hold values from -12 to 12
- routes: int32 [16384, 2], P('ep'), may hold values from 0 to 63, all different within a row; in each aligned block of 128 rows (0 to 127, 128 to 255, ...) at most 5 rows name the same one
- route_weights: bfloat16 [16384, 2], P('ep'), may hold values from 0.099609375 to 0.8984375
- w_gate: bfloat16 [128, 1024, 1408], P('ep', None, 'tp'), may hold values from -0.1875 to 0.1875
- w_up: bfloat16 [128, 1024, 1408], P('ep', None, 'tp'), may hold values from -0.1875 to 0.1875
- w_down: bfloat16 [128, 1408, 1024], P('ep', 'tp'), may hold values from -0.109375 to 0.109375
- dense_weight: bfloat16 [1024, 1024], P('tp', 'ep'), may hold values from -0.75 to 0.75
- mix_gate: float32 [1024], replicated, may hold values from 0.1 to 1.9
Outputs:
- token_grad: bfloat16 [16384, 1024], P('ep', 'tp')
- route_grad: float32 [16384, 2], P('ep')
- gate_grad: bfloat16 [128, 1024, 1408], P('ep', None, 'tp')
- up_grad: bfloat16 [128, 1024, 1408], P('ep', None, 'tp')
- down_grad: bfloat16 [128, 1408, 1024], P('ep', 'tp')
- dense_grad: float32 [1024, 1024], P('tp', 'ep')
- mix_grad: float32 [1024], replicated
Inputs may be any that keep to these rules, and one draw needn't show every extreme that they name: `routes`: each row names 2 different experts. In the rows of one index of ep (aligned blocks of 128 rows) no expert is named by more than 5 rows, a bound that some block reaches.
All inputs are finite; a program needn't handle non-finite values.
Results may differ from a plain program's by a relative error of at most 0.0065.
Values may be sent and summed in bfloat16 or wider, within the bound.
No kernel may reach another device: no remote copies, remote signals or barrier semaphores. Data moves between devices by JAX's collectives and lax.ppermute only.
A program may use at most 64 MiB of HBM per device.

v0:
```python
import functools

import jax
import jax.numpy as jnp
from jax import lax
from jax.sharding import Mesh
from jax.sharding import PartitionSpec as P

FF = 2816
EP = ("ep_0", "ep_1", "ep_2")
EP_TP = ("ep_0", "ep_1", "ep_2", "tp")


def split_up(value, dim, peers):
    before, after = (value.shape[:dim], value.shape[dim + 1 :])
    return jnp.moveaxis(value.reshape(*before, peers, -1, *after), dim, 0)


def joined_along(pieces, dim):
    lengths = list(pieces.shape[1:])
    lengths[dim] *= pieces.shape[0]
    return jnp.moveaxis(pieces, 0, dim).reshape(lengths)


def exchange_in_order(pieces, axes, order):
    lengths = [lax.axis_size(a) for a in axes]
    pieces = pieces.reshape(*lengths, *pieces.shape[1:])
    for k in order:
        pieces = lax.all_to_all(pieces, axes[k], split_axis=k, concat_axis=k, tiled=True)
    return pieces.reshape(-1, *pieces.shape[len(axes) :])


def two_step_exchange(value, groups, order, split_dim, concat_dim):
    peers = lax.axis_size(groups[0]) * lax.axis_size(groups[1])
    pieces = split_up(value, split_dim, peers)
    return joined_along(exchange_in_order(pieces, groups, order), concat_dim)


def stacked_from(value, axes, order):
    pieces = value
    for k in order:
        pieces = lax.all_gather(pieces, axes[k])
    done = order[::-1]
    back = [done.index(k) for k in range(len(axes))]
    pieces = pieces.transpose(*back, *range(len(axes), pieces.ndim))
    return pieces.reshape(-1, *value.shape)


def whole_of(value, axes, order, dim):
    return joined_along(stacked_from(value, axes, order), dim)


def over_axes(value, axes):
    return functools.reduce(lax.psum, axes, value)


def own_tiles(value, axis, dim):
    peers = lax.axis_size(axis)
    pieces = split_up(value, dim, peers)
    length = value.size // peers
    spare = max(2048 - length, -length % 1024)
    padded = jnp.pad(pieces.reshape(peers, length), ((0, 0), (0, spare)))
    own = lax.psum_scatter(padded.reshape(-1, 128), axis, scatter_dimension=0, tiled=True)
    return own.reshape(-1)[:length].reshape(pieces.shape[1:])


def spread(values, experts, group_size):
    capacity = values.shape[0] // experts
    shaped = values.reshape((experts, 1, capacity) + values.shape[1:])
    copies = jnp.broadcast_to(shaped, (experts, group_size, capacity) + values.shape[1:])
    return copies.reshape((experts * group_size * capacity,) + values.shape[1:])


def local(tokens, cotangent, routes, route_weights, w_gate, w_up, w_down, dense_weight, mix_gate):
    tp_count = lax.axis_size("tp")
    ep_count = lax.axis_size(EP)
    slice_width = w_gate.shape[2]
    group_size = FF // (slice_width * tp_count)
    experts = ep_count // group_size
    token_count, top_count = routes.shape
    capacity = 5 * token_count * top_count // (4 * experts)
    picked = routes.reshape(-1)
    onehot = (picked[:, None] == jnp.arange(experts, dtype=jnp.int32)[None, :]).astype(jnp.int32)
    ranking = jnp.cumsum(onehot, axis=0) - 1
    target = picked * capacity + jnp.sum(onehot * ranking, axis=1)
    matches = (target[:, None] == jnp.arange(experts * capacity, dtype=jnp.int32)[None, :]).astype(
        jnp.int32
    )
    pick_index = jnp.arange(picked.shape[0], dtype=jnp.int32)
    pick_of = jnp.sum(matches * pick_index[:, None], axis=0)
    filled = jnp.sum(matches, axis=0)
    token_of = pick_of // top_count
    slot_weight = jnp.take(route_weights.reshape(-1), pick_of, axis=0) * filled.astype(jnp.bfloat16)
    weight_out = spread(slot_weight, experts, group_size)
    grads_full = lax.all_gather(cotangent, "tp", axis=1, tiled=True)
    rows_part, grads_in, weights_in = (
        lax.all_to_all(
            spread(jnp.take(tokens, token_of, axis=0), experts, group_size),
            EP,
            split_axis=0,
            concat_axis=0,
            tiled=True,
        ),
        lax.all_to_all(
            spread(jnp.take(grads_full, token_of, axis=0), experts, group_size),
            EP,
            split_axis=0,
            concat_axis=0,
            tiled=True,
        ),
        lax.all_to_all(weight_out, EP, split_axis=0, concat_axis=0, tiled=True),
    )
    rows_in = lax.all_gather(rows_part, "tp", axis=1, tiled=True)
    gate_matrix = w_gate[0]
    up_matrix = w_up[0]
    down_matrix = w_down[0]
    pre_gate = jnp.dot(rows_in, gate_matrix, preferred_element_type=jnp.float32)
    pre_up = jnp.dot(rows_in, up_matrix, preferred_element_type=jnp.float32)
    sigmoid_gate = jax.nn.sigmoid(pre_gate)
    activated = pre_gate * sigmoid_gate
    hidden = activated * pre_up
    hidden_bf = hidden.astype(jnp.bfloat16)
    projected = lax.dot_general(
        grads_in, down_matrix, (((1,), (1,)), ((), ())), preferred_element_type=jnp.float32
    )
    route_part = jnp.sum(hidden_bf.astype(jnp.float32) * projected, axis=1)
    weight_col = weights_in.astype(jnp.float32)[:, None]
    hidden_grad = weight_col * projected
    d_gate = (hidden_grad * pre_up * sigmoid_gate * (1.0 + pre_gate * (1.0 - sigmoid_gate))).astype(
        jnp.bfloat16
    )
    d_up = (hidden_grad * activated).astype(jnp.bfloat16)
    weighted = (weight_col * hidden).astype(jnp.bfloat16)
    contract_rows = (((0,), (0,)), ((), ()))
    gate_grad = lax.dot_general(
        rows_in, d_gate, contract_rows, preferred_element_type=jnp.float32
    ).astype(jnp.bfloat16)[None]
    up_grad = lax.dot_general(
        rows_in, d_up, contract_rows, preferred_element_type=jnp.float32
    ).astype(jnp.bfloat16)[None]
    down_grad = lax.dot_general(
        weighted, grads_in, contract_rows, preferred_element_type=jnp.float32
    ).astype(jnp.bfloat16)[None]
    contract_cols = (((1,), (1,)), ((), ()))
    partial_value = (
        lax.dot_general(d_gate, gate_matrix, contract_cols, preferred_element_type=jnp.float32)
        + lax.dot_general(d_up, up_matrix, contract_cols, preferred_element_type=jnp.float32)
    ).astype(jnp.bfloat16)
    mixed = lax.all_to_all(partial_value, "tp", split_axis=1, concat_axis=0, tiled=True)
    rows_here = partial_value.shape[0]
    column_sum = jnp.sum(mixed.reshape(tp_count, rows_here, -1).astype(jnp.float32), axis=0).astype(
        jnp.bfloat16
    )
    route_sum = lax.psum(route_part, "tp")
    returned = lax.all_to_all(column_sum, EP, split_axis=0, concat_axis=0, tiled=True)
    route_back = two_step_exchange(route_sum, (("ep_0", "ep_1"), "ep_2"), (1, 0), 0, 0)
    slot_grad = jnp.sum(
        returned.reshape(experts, group_size, capacity, -1).astype(jnp.float32), axis=1
    ).reshape(experts * capacity, -1)
    slot_route = jnp.sum(route_back.reshape(experts, group_size, capacity), axis=1).reshape(-1)
    expert_grad = jnp.sum(
        jnp.take(slot_grad, target, axis=0).reshape(token_count, top_count, -1), axis=1
    )
    route_grad = jnp.take(slot_route, target, axis=0).reshape(token_count, top_count)
    scaled = (mix_gate[None, :] * grads_full.astype(jnp.float32)).astype(jnp.bfloat16)
    moment = lax.dot_general(tokens, grads_full, contract_rows, preferred_element_type=jnp.float32)
    shard_piece = whole_of(dense_weight, EP, (1, 0, 2), 1)
    scaled_cols = scaled
    dense_acc = lax.dot_general(
        scaled_cols, shard_piece, contract_cols, preferred_element_type=jnp.float32
    )
    gain_cols = jnp.sum(shard_piece.astype(jnp.float32) * moment, axis=0)
    gain_part = gain_cols
    dense_dx, gain_part = (dense_acc, gain_part)
    mix_grad = over_axes(gain_part, EP_TP) / ep_count
    scaled_cols = scaled
    product = lax.dot_general(
        scaled_cols, tokens, contract_rows, preferred_element_type=jnp.float32
    )
    dense_rows_sum = own_tiles(product * (1.0 / ep_count), EP, 0)
    dense_grad = dense_rows_sum.T
    token_grad = (expert_grad + dense_dx).astype(jnp.bfloat16)
    return (token_grad, route_grad, gate_grad, up_grad, down_grad, dense_grad, mix_grad)


def solution(mesh):
    finer = Mesh(mesh.devices.reshape(16, 4, 2, mesh.shape["tp"]), ("ep_0", "ep_1", "ep_2", "tp"))
    in_specs = (
        P(EP, "tp"),
        P(EP, "tp"),
        P(EP, None),
        P(EP, None),
        P(EP, None, "tp"),
        P(EP, None, "tp"),
        P(EP, "tp", None),
        P("tp", EP),
        P(),
    )
    out_specs = (
        P(EP, "tp"),
        P(EP, None),
        P(EP, None, "tp"),
        P(EP, None, "tp"),
        P(EP, "tp", None),
        P("tp", EP),
        P(),
    )
    return jax.shard_map(local, mesh=finer, in_specs=in_specs, out_specs=out_specs, check_vma=False)
```

profile of v0, /device:TPU:33, one launch (start us, length us, event | category | flops | bytes accessed | tf_op | source)
XLA Modules:
  0.0 396.2 jit_solution(6875033105968997943)
XLA Ops:
  11.5 2.4 gather_fusion
  14.9 19.3 %all-to-all-start = ((bf16[128,5,1]{1,2,0:T(2,128)(2,1)}), bf16[128,5,1]{1,2,0:T(2,128)(2,1)S(1)}, u32[]{:S(2)}, u32[]{:S(2)}) async-start(bf16[128,5,1]{1,2,0:T(2,128)(2,1)} %copy.72), calls=%async_computation | async-start | bytes 131072 | tf_op jit(solution)/shard_map/all_to_all | solution.py:111
  34.3 2.0 gather_fusion.2
  36.5 11.9 %all-to-all-done = bf16[128,5,1]{1,2,0:T(2,128)(2,1)S(1)} async-done(((bf16[128,5,1]{1,2,0:T(2,128)(2,1)}), bf16[128,5,1]{1,2,0:T(2,128)(2,1)S(1)}, u32[]{:S(2)}, u32[]{:S(2)}) %all-to-all-start) | async-done | bytes 1312 | tf_op jit(solution)/shard_map/all_to_all | solution.py:111
  49.2 7.5 %all-to-all-start.2 = ((bf16[128,5,256]{2,1,0:T(8,128)(2,1)}), bf16[128,5,256]{2,1,0:T(8,128)(2,1)}, u32[]{:S(2)}, u32[]{:S(2)}) async-start(bf16[128,5,256]{2,1,0:T(8,128)(2,1)} %bitcast.4), calls=%async_computation.2 | async-start | bytes 1048576 | tf_op jit(solution)/shard_map/all_to_all | solution.py:97
  56.7 11.1 %all_gather.24 = bf16[128,1024]{1,0:T(8,128)(2,1)S(1)} all-gather(bf16[128,256]{1,0:T(8,128)(2,1)S(1)} %copy-done.8), channel_id=1, replica_groups=mesh['ep_0'=16,'ep_1'=4,'ep_2'=2,'tp'=4] {'tp'}, dimensions={1}, use_global_device_ids=true | all-gather | bytes 327680 | tf_op jit(solution)/shard_map/all_gather | solution.py:95
  67.8 2.1 gather_fusion.1
  70.3 19.8 %all-to-all-done.2 = bf16[128,5,256]{2,1,0:T(8,128)(2,1)} async-done(((bf16[128,5,256]{2,1,0:T(8,128)(2,1)}), bf16[128,5,256]{2,1,0:T(8,128)(2,1)}, u32[]{:S(2)}, u32[]{:S(2)}) %all-to-all-start.2) | async-done | bytes 327712 | tf_op jit(solution)/shard_map/all_to_all | solution.py:97
  91.7 6.5 %all-to-all-start.1 = ((bf16[128,5,1024]{2,1,0:T(8,128)(2,1)}), bf16[128,5,1024]{2,1,0:T(8,128)(2,1)S(1)}, u32[]{:S(2)}, u32[]{:S(2)}) async-start(bf16[128,5,1024]{2,1,0:T(8,128)(2,1)} %bitcast.75), calls=%async_computation.1 | async-start | bytes 4194304 | tf_op jit(solution)/shard_map/all_to_all | solution.py:104
  98.2 1.9 all_to_all.51
  101.6 2.3 reshape.275
  103.9 10.1 %all-gather = bf16[1024,8]{0,1:T(8,128)(2,1)S(1)} all-gather(bf16[256,8]{0,1:T(8,128)(2,1)S(1)} %copy-done.10), channel_id=2, replica_groups=mesh['ep_0'=16,'ep_1'=4,'ep_2'=2,'tp'=4] {'ep_1'}, dimensions={0}, use_global_device_ids=true | all-gather | bytes 20480 | tf_op jit(solution)/shard_map/all_gather | solution.py:42
  114.0 94.1 %all-gather.1 = bf16[64,256,8]{1,2,0:T(8,128)(2,1)S(1)} all-gather(bf16[4,256,8]{1,2,0:T(8,128)(2,1)S(1)} %bitcast.83), channel_id=3, replica_groups=mesh['ep_0'=16,'ep_1'=4,'ep_2'=2,'tp'=4] {'ep_0'}, dimensions={0}, use_global_device_ids=true | all-gather | bytes 278528 | tf_op jit(solution)/shard_map/all_gather | solution.py:42
  208.1 8.0 %all-gather.2 = bf16[32,4,256,8]{2,3,1,0:T(8,128)(2,1)S(1)} all-gather(bf16[16,4,256,8]{2,3,1,0:T(8,128)(2,1)S(1)} %bitcast.81), channel_id=4, replica_groups=mesh['ep_0'=16,'ep_1'=4,'ep_2'=2,'tp'=4] {'ep_2'}, dimensions={0}, use_global_device_ids=true | all-gather | bytes 786432 | tf_op jit(solution)/shard_map/all_gather | solution.py:42
  216.9 2.0 copy.79
  220.3 21.9 %psum.36 = f32[1024]{0:T(1024)S(1)} all-reduce(f32[1024]{0:T(1024)S(1)} %fusion.3), channel_id=1, replica_groups=mesh['ep_0'=16,'ep_1'=4,'ep_2'=2,'tp'=4] {'ep_0'}, use_global_device_ids=true, to_apply=%region_13.14 | all-reduce | flops 1024 | bytes 8192 | tf_op jit(solution)/shard_map/psum | solution.py:54
  242.2 8.5 %psum.37 = f32[1024]{0:T(1024)S(1)} all-reduce(f32[1024]{0:T(1024)S(1)} %psum.36), channel_id=1, replica_groups=mesh['ep_0'=16,'ep_1'=4,'ep_2'=2,'tp'=4] {'ep_1'}, use_global_device_ids=true, to_apply=%region_14.15 | all-reduce | flops 1024 | bytes 8192 | tf_op jit(solution)/shard_map/psum | solution.py:54
  250.7 11.5 %psum.38 = f32[1024]{0:T(1024)S(1)} all-reduce(f32[1024]{0:T(1024)S(1)} %psum.37), channel_id=1, replica_groups=mesh['ep_0'=16,'ep_1'=4,'ep_2'=2,'tp'=4] {'ep_2'}, use_global_device_ids=true, to_apply=%region_15.16 | all-reduce | flops 1024 | bytes 8192 | tf_op jit(solution)/shard_map/psum | solution.py:54
  262.6 3.2 fusion.8
  265.8 1.7 fusion.11
  268.9 3.1 multiply_reduce_fusion
  272.2 14.3 %all-reduce = (f32[64,2,5]{2,1,0:T(2,128)S(1)}, f32[1024]{0:T(1024)S(1)}) all-reduce(f32[64,2,5]{2,1,0:T(2,128)S(1)} %reshape_reshape.7, f32[1024]{0:T(1024)S(1)} %psum.38), channel_id=1, replica_groups=mesh['ep_0'=16,'ep_1'=4,'ep_2'=2,'tp'=4] {'tp'}, use_global_device_ids=true, to_apply=%region_9.10 | all-reduce | flops 1664 | bytes 13312 | tf_op jit(solution)/shard_map/psum | solution.py:154
  287.3 7.3 %all-to-all-start.5 = ((f32[2,1,320]{2,1,0:T(1,128)}), f32[2,1,320]{2,1,0:T(1,128)S(1)}, u32[]{:S(2)}, u32[]{:S(2)}) async-start(f32[2,1,320]{2,1,0:T(1,128)} %reshape.331), calls=%async_computation.5 | async-start | bytes 6144 | tf_op jit(solution)/shard_map/all_to_all | solution.py:29
  297.7 3.5 all-to-all-start.3
  303.4 15.8 %all-to-all-done.3 = bf16[640,4,256]{2,0,1:T(8,128)(2,1)S(1)} async-done(((bf16[640,4,256]{2,0,1:T(8,128)(2,1)}), bf16[640,4,256]{2,0,1:T(8,128)(2,1)S(1)}, u32[]{:S(2)}, u32[]{:S(2)}) %all-to-all-start.3) | async-done | bytes 1310752 | tf_op jit(solution)/shard_map/all_to_all | solution.py:149
  319.2 11.2 %all-to-all-start.6 = ((f32[64,2,5]{2,1,0:T(2,128)}), f32[64,2,5]{2,1,0:T(2,128)S(1)}, u32[]{:S(2)}, u32[]{:S(2)}) async-start(f32[64,2,5]{2,1,0:T(2,128)} %copy.76), calls=%async_computation.6 | async-start | bytes 131072 | tf_op jit(solution)/shard_map/all_to_all | solution.py:29
  331.7 12.1 %all-to-all-done.6 = f32[64,2,5]{2,1,0:T(2,128)S(1)} async-done(((f32[64,2,5]{2,1,0:T(2,128)}), f32[64,2,5]{2,1,0:T(2,128)S(1)}, u32[]{:S(2)}, u32[]{:S(2)}) %all-to-all-start.6) | async-done | bytes 2592 | tf_op jit(solution)/shard_map/all_to_all | solution.py:29
  343.8 8.5 %all-to-all-start.4 = ((bf16[128,5,256]{2,1,0:T(8,128)(2,1)}), bf16[128,5,256]{2,1,0:T(8,128)(2,1)S(1)}, u32[]{:S(2)}, u32[]{:S(2)}) async-start(bf16[128,5,256]{2,1,0:T(8,128)(2,1)} %all_to_all.54), calls=%async_computation.4 | async-start | bytes 1048576 | tf_op jit(solution)/shard_map/all_to_all | solution.py:155
  352.5 6.0 %reduce-scatter.2.cloned.1.call-done = f32[16,128]{1,0:T(8,128)} async-done(((f32[2048,128]{1,0:T(8,128)}), f32[16,128]{1,0:T(8,128)}) %reduce-scatter.2.cloned.1.call-update) | async-done | bytes 8208 | tf_op jit(solution)/shard_map/reduce_scatter | solution.py:63
  360.4 3.1 fusion.1
  367.0 1.9 gather_fusion.4
  369.8 16.3 %all-to-all-done.4 = bf16[128,5,256]{2,1,0:T(8,128)(2,1)S(1)} async-done(((bf16[128,5,256]{2,1,0:T(8,128)(2,1)}), bf16[128,5,256]{2,1,0:T(8,128)(2,1)S(1)}, u32[]{:S(2)}, u32[]{:S(2)}) %all-to-all-start.4) | async-done | bytes 327712 | tf_op jit(solution)/shard_map/all_to_all | solution.py:155
  (105 shorter events, 29.6 us)
Async XLA Ops:
  8.0 254.6 %copy-start = (bf16[1,1024,352]{1,2,0:T(8,128)(2,1)S(1)}, bf16[1,1024,352]{1,2,0:T(8,128)(2,1)}, u32[]{:S(2)}) copy-start(bf16[1,1024,352]{1,2,0:T(8,128)(2,1)} %param.13) | copy-start | bytes 2162692
  8.0 26.2 %copy-start.1 = (bf16[128,256]{1,0:T(8,128)(2,1)S(1)}, bf16[128,256]{1,0:T(8,128)(2,1)}, u32[]{:S(2)}) copy-start(bf16[128,256]{1,0:T(8,128)(2,1)} %param.9) | copy-start | bytes 196612
  14.9 33.5 %all-to-all-start = ((bf16[128,5,1]{1,2,0:T(2,128)(2,1)}), bf16[128,5,1]{1,2,0:T(2,128)(2,1)S(1)}, u32[]{:S(2)}, u32[]{:S(2)}) async-start(bf16[128,5,1]{1,2,0:T(2,128)(2,1)} %copy.72), calls=%async_computation | async-start | bytes 131072 | tf_op jit(solution)/shard_map/all_to_all | solution.py:111
  36.3 20.4 %copy-start.8 = (bf16[128,256]{1,0:T(8,128)(2,1)S(1)}, bf16[128,256]{1,0:T(8,128)(2,1)}, u32[]{:S(2)}) copy-start(bf16[128,256]{1,0:T(8,128)(2,1)} %param.10) | copy-start | bytes 196612
  49.2 40.9 %all-to-all-start.2 = ((bf16[128,5,256]{2,1,0:T(8,128)(2,1)}), bf16[128,5,256]{2,1,0:T(8,128)(2,1)}, u32[]{:S(2)}, u32[]{:S(2)}) async-start(bf16[128,5,256]{2,1,0:T(8,128)(2,1)} %bitcast.4), calls=%async_computation.2 | async-start | bytes 1048576 | tf_op jit(solution)/shard_map/all_to_all | solution.py:97
  91.7 8.5 %copy-start.9 = (f32[1024]{0:T(1024)S(1)}, f32[1024]{0:T(1024)}, u32[]{:S(2)}) copy-start(f32[1024]{0:T(1024)} %param.17) | copy-start | bytes 12292
  91.7 175.7 %all-to-all-start.1 = ((bf16[128,5,1024]{2,1,0:T(8,128)(2,1)}), bf16[128,5,1024]{2,1,0:T(8,128)(2,1)S(1)}, u32[]{:S(2)}, u32[]{:S(2)}) async-start(bf16[128,5,1024]{2,1,0:T(8,128)(2,1)} %bitcast.75), calls=%async_computation.1 | async-start | bytes 4194304 | tf_op jit(solution)/shard_map/all_to_all | solution.py:104
  98.2 164.4 %all-gather.5.cloned.1.call-start = ((), (), s32[]{:S(2)}) async-start(), calls=%async_computation.8 | async-start | bytes 1638400 | tf_op jit(solution)/shard_map/all_gather | solution.py:113
  100.2 258.4 %reduce-scatter.2.cloned.1.call-start = ((), (), s32[]{:S(2)}) async-start(), calls=%async_computation.9 | async-start | bytes 1056768 | tf_op jit(solution)/shard_map/reduce_scatter | solution.py:63
  101.6 2.4 copy-start.10
  262.6 3.2 copy-start.4
  262.6 3.2 copy-start.11
  272.0 23.5 %copy-start.6 = (bf16[640,352]{0,1:T(8,128)(2,1)}, bf16[640,352]{0,1:T(8,128)(2,1)S(1)}, u32[]{:S(2)}) copy-start(bf16[640,352]{0,1:T(8,128)(2,1)S(1)} %get-tuple-element.59) | copy-start | bytes 1351684
  287.3 10.4 %all-to-all-start.5 = ((f32[2,1,320]{2,1,0:T(1,128)}), f32[2,1,320]{2,1,0:T(1,128)S(1)}, u32[]{:S(2)}, u32[]{:S(2)}) async-start(f32[2,1,320]{2,1,0:T(1,128)} %reshape.331), calls=%async_computation.5 | async-start | bytes 6144 | tf_op jit(solution)/shard_map/all_to_all | solution.py:29
  294.6 1.1 copy-start.5
  297.7 21.5 %all-to-all-start.3 = ((bf16[640,4,256]{2,0,1:T(8,128)(2,1)}), bf16[640,4,256]{2,0,1:T(8,128)(2,1)S(1)}, u32[]{:S(2)}, u32[]{:S(2)}) async-start(bf16[640,4,256]{2,0,1:T(8,128)(2,1)} %bitcast.77), calls=%async_computation.3 | async-start | bytes 2621440 | tf_op jit(solution)/shard_map/all_to_all | solution.py:149
  319.2 24.6 %all-to-all-start.6 = ((f32[64,2,5]{2,1,0:T(2,128)}), f32[64,2,5]{2,1,0:T(2,128)S(1)}, u32[]{:S(2)}, u32[]{:S(2)}) async-start(f32[64,2,5]{2,1,0:T(2,128)} %copy.76), calls=%async_computation.6 | async-start | bytes 131072 | tf_op jit(solution)/shard_map/all_to_all | solution.py:29
  343.8 42.3 %all-to-all-start.4 = ((bf16[128,5,256]{2,1,0:T(8,128)(2,1)}), bf16[128,5,256]{2,1,0:T(8,128)(2,1)S(1)}, u32[]{:S(2)}, u32[]{:S(2)}) async-start(bf16[128,5,256]{2,1,0:T(8,128)(2,1)} %all_to_all.54), calls=%async_computation.4 | async-start | bytes 1048576 | tf_op jit(solution)/shard_map/all_to_all | solution.py:155
  360.4 3.1 copy-start.7
  360.4 3.1 copy-start.12
  360.4 4.7 %copy-start.14 = (f32[640,352]{0,1:T(8,128)S(1)}, f32[640,352]{0,1:T(8,128)}, u32[]{:S(2)}) copy-start(f32[640,352]{0,1:T(8,128)} %fusion.11) | copy-start | bytes 2703364
  363.5 1.6 copy-start.3
  363.5 1.6 copy-start.13
  386.3 1.6 copy-start.2
Sparse Core Ops, SparseCore 0:
  101.7 34.7 all-gather.4
Sparse Core Ops, SparseCore 1:
  105.2 253.3 reduce-scatter.1
where the time goes:
time: 397 us; the launch traced here: 396 us
  blocking collectives  179 us (45%)
  waiting for transfers between devices  81.9 us (21%)
  starting transfers between devices  63.8 us (16%)
  local copies, waits for them, and re-layouts  31.7 us (8%)
  matrix products  19.6 us (5%)
  between operations  16 us (4%)
    all_gather x3, blocking collectives, stacked_from(): pieces = lax.all_gather(pieces, axes[k])  112 us
    psum x3, blocking collectives, over_axes(): return functools.reduce(lax.psum, axes, value)  41.9 us
    all_to_all x1, waiting for transfers between devices, local(): lax.all_to_all(spread(jnp.take(tokens, token_of, axis=0), experts, group_...  19.8 us
    all_to_all x1, starting transfers between devices, local(): lax.all_to_all(weight_out, EP, split_axis=0, concat_axis=0, tiled=True)  19.3 us
    all_to_all x2, starting transfers between devices, exchange_in_order(): lax.all_to_all(pieces, axes[k], split_axis=k, concat_axis=k, tiled=True)  18.4 us
    all_to_all x1, waiting for transfers between devices, local(): lax.all_to_all(column_sum, EP, split_axis=0, concat_axis=0, tiled=True)  16.3 us
    all_to_all x1, waiting for transfers between devices, local(): lax.all_to_all(partial_value, 'tp', split_axis=1, concat_axis=0, tiled=True)  15.8 us
    psum x1, blocking collectives, local(): route_sum = lax.psum(route_part, 'tp')  14.3 us
  transfers between devices with their start and end apart: 9, of which 6 were waited for; matrix products, arithmetic and copies ran while one was open for 10% of the time, Pallas kernels for 0%

commit v1 on v0

v1 whole, which is shorter than its diff:
```python
import jax
import jax.numpy as jnp
from jax import lax
from jax.experimental import pallas as pl
from jax.experimental.pallas import tpu as pltpu
from jax.sharding import Mesh
from jax.sharding import PartitionSpec as P

EP = ("ep_0", "ep_1", "ep_2")
CHIPS = ("ep_0", "ep_1")
F32 = jnp.float32
BF16 = jnp.bfloat16
EXPERTS = 64
CAP = 5
ROWS = EXPERTS * CAP
EXTRA = 16
TP = 4


def iota(shape, dim):
    return lax.broadcasted_iota(jnp.int32, shape, dim)


def dot(a, b):
    return jnp.dot(a, b, preferred_element_type=F32)


def dot_nt(a, b):
    return lax.dot_general(a, b, (((1,), (1,)), ((), ())), preferred_element_type=F32)


def dot_tn(a, b):
    return lax.dot_general(a, b, (((0,), (0,)), ((), ())), preferred_element_type=F32)


def onehot(cond):
    return jnp.where(cond, 1.0, 0.0).astype(BF16)


def call(kernel, outs, *args):
    return pl.pallas_call(
        kernel,
        out_shape=outs,
        compiler_params=pltpu.CompilerParams(vmem_limit_bytes=48 * 1024 * 1024),
    )(*args)


def pack_kernel(routes_ref, weights_ref, tok_ref, cot_ref, out_ref, keys_ref, cols_ref):
    tokens = 128
    r0 = routes_ref[0:1, :].astype(F32)
    r1 = routes_ref[1:2, :].astype(F32)
    w = weights_ref[...].astype(F32)
    row = iota((tokens, tokens), 0)
    lane = iota((tokens, tokens), 1)
    eye = row == lane

    def to_col(v):
        return jnp.sum(jnp.where(eye, v, 0.0), axis=1, keepdims=True)

    c0 = to_col(r0)
    c1 = to_col(r1)
    before = row < lane

    def rank_of(r):
        hit = jnp.where(c0 == r, 1.0, 0.0) + jnp.where(c1 == r, 1.0, 0.0)
        return jnp.sum(jnp.where(before, hit, 0.0), axis=0, keepdims=True)

    k0 = rank_of(r0)
    k1 = rank_of(r1)
    four = jnp.concatenate([(r0 * CAP + k0) * 4 + i for i in range(4)], axis=1)
    four_b = jnp.concatenate([(r1 * CAP + k1) * 4 + i for i in range(4)], axis=1)
    msgs = EXPERTS * 8
    m_row = iota((msgs, 512), 0)
    dest = m_row // 8
    sub = m_row % 8
    data = jnp.concatenate(
        [tok_ref[:, :128], tok_ref[:, 128:], cot_ref[:, :128], cot_ref[:, 128:]], axis=0
    )
    for j in range(3):
        cell = j * 8 + sub
        key = jnp.where(cell < 20, dest * 20 + cell, -1).astype(F32)
        block = dot(onehot((key == four) | (key == four_b)), data)
        if j == 2:
            both = jnp.concatenate([r0, r1], axis=1)
            there = onehot((m_row[:, :256].astype(F32) == both * 8 + 4))
            lane_f = lane.astype(F32)
            v0 = jnp.where(lane_f == to_col(k0), to_col(w[0:1, :]), 0.0)
            v1 = jnp.where(lane_f == to_col(k1), to_col(w[1:2, :]), 0.0)
            block = block + dot(there, jnp.concatenate([v0, v1], axis=0).astype(BF16))
        out_ref[:, j * 128 : (j + 1) * 128] = block.astype(BF16)
    eight = iota((8, tokens), 0)
    keys_ref[...] = jnp.where(
        eight == 0, r0, jnp.where(eight == 1, r1, jnp.where(eight == 2, k0, k1))
    )
    cols_ref[...] = jnp.where(
        lane == 0, to_col(r0 * 8 + k0), jnp.where(lane == 1, to_col(r1 * 8 + k1), 0.0)
    )


def unpack_kernel(in_ref, out_ref):
    msgs = EXPERTS * 8
    p_row = iota((512, msgs), 0)
    p_col = iota((512, msgs), 1)
    chunk = p_row // 128
    half = (p_row % 128) // 64
    src = p_row % 64
    perm = onehot(p_col == src * 8 + half * 4 + chunk)
    rows = dot(perm, in_ref[...])
    by_src = rows[64:128, 256:384]
    tall = jnp.concatenate([by_src] * CAP, axis=0)
    t_row = iota((ROWS, 128), 0)
    t_lane = iota((ROWS, 128), 1)
    tall = jnp.where(t_row // 64 == t_lane, tall, 0.0).astype(BF16)
    w_row = dot_nt(jnp.full((EXTRA, 128), 1.0, BF16), tall).astype(BF16)
    rows = rows.astype(BF16)
    for t in range(TP):
        for c in range(4):
            for j in range(3):
                n = 128 if j < 2 else 64
                out_ref[t, j * 128 : j * 128 + n, c * 128 : (c + 1) * 128] = rows[
                    c * 128 : c * 128 + n, j * 128 : (j + 1) * 128
                ]
        out_ref[t, ROWS : ROWS + EXTRA, :] = jnp.zeros((EXTRA, 512), BF16)
        out_ref[t, ROWS : ROWS + EXTRA, 0:ROWS] = w_row


def expert_kernel(in_ref, wg_ref, wu_ref, wd_ref, z_ref, dg_ref, du_ref, wt_ref):
    def summed(lo, w_ref):
        return sum(
            dot_nt(in_ref[t, 0:ROWS, lo : lo + 256], w_ref[:, t * 256 : (t + 1) * 256])
            for t in range(TP)
        )

    pre_gate = summed(0, wg_ref)
    pre_up = summed(0, wu_ref)
    projected = summed(256, wd_ref)
    w_row = in_ref[0, ROWS : ROWS + EXTRA, 0:ROWS].astype(F32)[0:1, :]
    eye = iota((ROWS, ROWS), 0) == iota((ROWS, ROWS), 1)
    weight = jnp.sum(jnp.where(eye, w_row, 0.0), axis=1, keepdims=True)
    sig = jax.nn.sigmoid(pre_gate)
    activated = pre_gate * sig
    hidden = activated * pre_up
    route = jnp.sum(hidden.astype(BF16).astype(F32) * projected, axis=1, keepdims=True)
    grad = weight * projected
    d_gate = (grad * pre_up * sig * (1.0 + pre_gate * (1.0 - sig))).astype(BF16)
    d_up = (grad * activated).astype(BF16)
    dg_ref[...] = d_gate
    du_ref[...] = d_up
    wt_ref[...] = (weight * hidden).astype(BF16)
    part = (dot(d_gate, wg_ref[...]) + dot(d_up, wu_ref[...])).astype(BF16)
    hi = route.astype(BF16).astype(F32)
    lo = route - hi
    lane = iota((ROWS, 128), 1)
    pair = jnp.where(lane == 0, hi, jnp.where(lane == 1, lo, 0.0))
    pair = jnp.concatenate([pair, jnp.zeros((512 - ROWS, 128), F32)], axis=0).astype(BF16)
    pick = onehot(iota((EXTRA, 128), 0) == iota((EXTRA, 128), 1))
    flat = dot_nt(pick, pair)
    extra = jnp.concatenate([flat[0:8, 0:256], flat[0:8, 256:512]], axis=0).astype(BF16)
    for t in range(TP):
        z_ref[t, 0:ROWS, :] = part[:, t * 256 : (t + 1) * 256]
        z_ref[t, ROWS : ROWS + EXTRA, :] = extra


def return_kernel(in_ref, mix_ref, out_ref):
    total = sum(in_ref[t].astype(F32) for t in range(TP))
    msgs = EXPERTS * 8
    rows = total[0:ROWS].astype(BF16)
    m_row = iota((msgs, 512), 0)
    m_col = iota((msgs, 512), 1)
    dest = m_row // 8
    sub = m_row % 8
    perm = onehot((m_col == sub * 64 + dest) & (sub < CAP))
    out = dot(perm[:, 0:ROWS], rows)
    first = total[ROWS : ROWS + 1] + total[ROWS + 1 : ROWS + 2]
    second = total[ROWS + 8 : ROWS + 9] + total[ROWS + 9 : ROWS + 10]
    route = jnp.concatenate([first, second], axis=1)
    hi = route.astype(BF16).astype(F32)
    lo = route - hi
    mine = (sub == CAP) & (m_col % 64 == dest)
    b_row = iota((512, 256), 0)
    b_col = iota((512, 256), 1)
    out = out + dot(jnp.where(mine, hi, 0.0).astype(BF16), onehot(b_row // 64 == b_col))
    out = out + dot(jnp.where(mine, lo, 0.0).astype(BF16), onehot(b_row // 64 == b_col - 128))
    out_sub = iota((msgs, 256), 0) % 8
    out = jnp.where(out_sub == CAP + 1, mix_ref[...], out)
    out_ref[...] = out.astype(BF16)


def final_kernel(in_ref, keys_ref, cols_ref, dense_ref, tok_ref, route_ref, mix_ref):
    msgs = EXPERTS * 8
    got = in_ref[...]
    lane = iota((128, msgs), 1).astype(F32)
    take = onehot((lane == cols_ref[:, 0:1]) | (lane == cols_ref[:, 1:2]))
    tok_ref[...] = (dot(take, got) + dense_ref[...]).astype(BF16)
    m_row = iota((msgs, 128), 0).astype(F32)
    l_row = iota((256, 128), 0).astype(F32)
    for a in range(2):
        expert = keys_ref[a : a + 1, :]
        rank = keys_ref[a + 2 : a + 3, :]
        cells = dot_tn(got, onehot(m_row == expert * 8 + CAP))
        keep = (l_row == rank) | (l_row == rank + 128)
        route_ref[a : a + 1, :] = jnp.sum(jnp.where(keep, cells, 0.0), axis=0, keepdims=True)
    e_row = iota((EXPERTS, msgs), 0)
    e_col = iota((EXPERTS, msgs), 1)
    mix = dot(onehot(e_col == e_row * 8 + CAP + 1), got)
    mix_ref[...] = mix[:, 0:128] + mix[:, 128:256]


def swap(value, axes):
    return lax.all_to_all(value, axes, split_axis=0, concat_axis=0, tiled=True)


def copies(value, n):
    return jnp.broadcast_to(value[None], (n,) + value.shape)


def local(tokens, cotangent, routes, route_weights, w_gate, w_up, w_down, dense_weight, mix_gate):
    ep_count = lax.axis_size(EP)
    wg = w_gate[0].T
    wu = w_up[0].T
    wd = w_down[0]
    dense_t = dense_weight.T
    packed, keys, cols = call(
        pack_kernel,
        (
            jax.ShapeDtypeStruct((512, 384), BF16),
            jax.ShapeDtypeStruct((8, 128), F32),
            jax.ShapeDtypeStruct((128, 128), F32),
        ),
        routes.T,
        route_weights.T,
        tokens,
        cotangent,
    )
    arrived = swap(packed.reshape(64, 8, 384), CHIPS)

    cot_all = swap(copies(cotangent, TP), "tp")
    moment = lax.dot_general(
        jnp.swapaxes(cot_all, 1, 2).reshape(1024, 128), tokens, (((1,), (0,)), ((), ())),
        preferred_element_type=F32,
    ).astype(BF16)
    moment = moment.reshape(16, 4, 2, 8, 256).transpose(2, 1, 0, 3, 4).reshape(2, 512, 256)
    moment = jnp.sum(swap(moment, "ep_2").astype(F32), axis=0).astype(BF16)
    moment = jnp.sum(swap(moment.reshape(4, 128, 256), "ep_1").astype(F32), axis=0).astype(BF16)
    both = jnp.concatenate([moment.reshape(16, 8, 256), copies(dense_t, 16)], axis=1)
    both = swap(both, "ep_0")
    moment = jnp.sum(both[:, 0:8].astype(F32), axis=0) * (1.0 / ep_count)
    gate = lax.dynamic_slice(mix_gate, (lax.axis_index(EP) * 8,), (8,))
    dense_grad = (moment * gate[:, None]).T
    share = jnp.sum(moment * dense_t.astype(F32), axis=1)
    share = jnp.pad(share[None, :], ((0, 0), (0, 120)))
    shares = swap(copies(share, 8), ("ep_2", "tp"))
    mix = jnp.sum(shares.reshape(2, TP, 128)[:, :, :8], axis=1).reshape(1, 16)
    mix_hi = mix.astype(BF16).astype(F32)
    mix_row = jnp.concatenate(
        [jnp.pad(mix_hi, ((0, 0), (0, 112))), jnp.pad(mix - mix_hi, ((0, 0), (0, 112)))], axis=1
    )
    dense_w = swap(copies(both[:, 8:16].reshape(128, 256), 4), "ep_1")
    dense_w = swap(copies(dense_w.reshape(512, 256), 2), "ep_2")
    dense_w = dense_w.reshape(2, 4, 16, 8, 256).transpose(2, 1, 0, 3, 4).reshape(TP, 256, 256)
    scaled = (mix_gate.reshape(TP, 1, 256) * cot_all.astype(F32)).astype(BF16)
    dense_dx = lax.dot_general(
        jnp.swapaxes(scaled, 0, 1).reshape(128, 1024), dense_w.reshape(1024, 256),
        (((1,), (0,)), ((), ())), preferred_element_type=F32,
    )

    own = call(
        unpack_kernel,
        jax.ShapeDtypeStruct((TP, ROWS + EXTRA, 512), BF16),
        arrived.reshape(512, 384),
    )
    own = swap(own, "tp")
    other = lax.ppermute(own, "ep_2", [(0, 1), (1, 0)])
    outs = (
        jax.ShapeDtypeStruct((TP, ROWS + EXTRA, 256), BF16),
        jax.ShapeDtypeStruct((ROWS, 352), BF16),
        jax.ShapeDtypeStruct((ROWS, 352), BF16),
        jax.ShapeDtypeStruct((ROWS, 352), BF16),
    )
    z_own, *act_own = call(expert_kernel, outs, own, wg, wu, wd)
    z_other, *act_other = call(expert_kernel, outs, other, wg, wu, wd)
    z_back = lax.ppermute(z_other, "ep_2", [(0, 1), (1, 0)])
    z_sum = (z_own.astype(F32) + z_back.astype(F32)).astype(BF16)
    z_all = swap(z_sum, "tp")
    back = call(return_kernel, jax.ShapeDtypeStruct((512, 256), BF16), z_all, mix_row)
    back = swap(back.reshape(64, 8, 256), CHIPS).reshape(512, 256)
    token_grad, route_t, mix_all = call(
        final_kernel,
        (
            jax.ShapeDtypeStruct((128, 256), BF16),
            jax.ShapeDtypeStruct((2, 128), F32),
            jax.ShapeDtypeStruct((EXPERTS, 128), F32),
        ),
        back,
        keys,
        cols,
        dense_dx,
    )
    mix_grad = mix_all[:, :16].reshape(1024)

    gate_grad, up_grad, down_grad = call(
        grads_kernel,
        tuple(jax.ShapeDtypeStruct((352, 1024), BF16) for _ in range(3)),
        own,
        other,
        *act_own,
        *act_other,
    )
    return (
        token_grad,
        route_t.T,
        gate_grad.T[None],
        up_grad.T[None],
        down_grad[None],
        dense_grad,
        mix_grad,
    )


def grads_kernel(own_ref, other_ref, dg0, du0, wt0, dg1, du1, wt1, gate_ref, up_ref, down_ref):
    for left0, left1, lo, out_ref in (
        (dg0, dg1, 0, gate_ref),
        (du0, du1, 0, up_ref),
        (wt0, wt1, 256, down_ref),
    ):
        left = jnp.concatenate([left0[...], left1[...]], axis=0)
        for t in range(TP):
            right = jnp.concatenate(
                [own_ref[t, 0:ROWS, lo : lo + 256], other_ref[t, 0:ROWS, lo : lo + 256]], axis=0
            )
            out_ref[:, t * 256 : (t + 1) * 256] = dot_tn(left, right).astype(BF16)


def solution(mesh):
    finer = Mesh(mesh.devices.reshape(16, 4, 2, mesh.shape["tp"]), ("ep_0", "ep_1", "ep_2", "tp"))
    in_specs = (
        P(EP, "tp"),
        P(EP, "tp"),
        P(EP, None),
        P(EP, None),
        P(EP, None, "tp"),
        P(EP, None, "tp"),
        P(EP, "tp", None),
        P("tp", EP),
        P(),
    )
    out_specs = (
        P(EP, "tp"),
        P(EP, None),
        P(EP, None, "tp"),
        P(EP, None, "tp"),
        P(EP, "tp", None),
        P("tp", EP),
        P(),
    )
    return jax.shard_map(local, mesh=finer, in_specs=in_specs, out_specs=out_specs, check_vma=False)
```

time: 397 us -> 209 us (0.53)
  the two profiles are of different devices: /device:TPU:33 before, /device:TPU:2 now
where the time goes in v1:
time: 209 us; the launch traced here: 207 us
  blocking collectives  92.8 us (44%)
  waiting for transfers between devices  35.7 us (17%)
  starting transfers between devices  34.2 us (16%)
  local copies, waits for them, and re-layouts  21.8 us (10%)
  Pallas kernels  10.8 us (5%)
  other arithmetic  10.4 us (5%)
    all_to_all x5, blocking collectives, swap(): return lax.all_to_all(value, axes, split_axis=0, concat_axis=0, tiled=True)  92.8 us
    all_to_all x6, waiting for transfers between devices, swap(): return lax.all_to_all(value, axes, split_axis=0, concat_axis=0, tiled=True)  35.7 us
    all_to_all x6, starting transfers between devices, swap(): return lax.all_to_all(value, axes, split_axis=0, concat_axis=0, tiled=True)  30.3 us
    unnamed x59, local copies, waits for them, and re-layouts  14.4 us
    pallas_call x7, Pallas kernels, call(): pl.pallas_call(kernel, out_shape=outs, compiler_params=pltpu.CompilerPara...  10.8 us
    broadcast_in_dim x7, local copies, waits for them, and re-layouts, copies(): return jnp.broadcast_to(value[None], (n,) + value.shape)  5.47 us
  transfers between devices with their start and end apart: 8, of which 5 were waited for; matrix products, arithmetic and copies ran while one was open for 8% of the time, Pallas kernels for 4%

profile of v1, /device:TPU:2, one launch (start us, length us, event | category | flops | bytes accessed | tf_op | source)
XLA Modules:
  0.0 207.1 jit_solution(12594497614635819222)
XLA Ops:
  4.6 45.5 %all_to_all.55 = bf16[64,8,384]{2,1,0:T(8,128)(2,1)S(1)} all-to-all(bf16[64,8,384]{2,1,0:T(8,128)(2,1)S(1)} %bitcast.62), channel_id=1, replica_groups=mesh['ep_0'=16,'ep_1'=4,'ep_2'=2,'tp'=4] {'ep_0','ep_1'}, dimensions={0} | all-to-all | bytes 786432 | tf_op jit(solution)/shard_map/all_to_all | solution.py:210
  50.7 21.1 %all_to_all.56.in_ref.own_ref = bf16[4,336,512]{2,1,0:T(8,128)(2,1)S(1)} all-to-all(bf16[4,336,512]{2,1,0:T(8,128)(2,1)S(1)} %shard_map.145), channel_id=1, replica_groups=mesh['ep_0'=16,'ep_1'=4,'ep_2'=2,'tp'=4] {'tp'}, dimensions={0} | all-to-all | bytes 2752512 | tf_op jit(solution)/shard_map/all_to_all | solution.py:210
  71.8 1.9 collective-permute-start
  73.9 10.0 %all_to_all.57 = bf16[4,128,256]{1,2,0:T(8,128)(2,1)S(1)} all-to-all(bf16[4,128,256]{1,2,0:T(8,128)(2,1)S(1)} %broadcast_in_dim.47), channel_id=1, replica_groups=mesh['ep_0'=16,'ep_1'=4,'ep_2'=2,'tp'=4] {'tp'}, dimensions={0} | all-to-all | bytes 524288 | tf_op jit(solution)/shard_map/all_to_all | solution.py:210
  84.6 4.9 %all_to_all.58 = bf16[2,512,256]{2,1,0:T(8,128)(2,1)} all-to-all(bf16[2,512,256]{2,1,0:T(8,128)(2,1)S(1)} %bitcast.68), channel_id=1, replica_groups=mesh['ep_0'=16,'ep_1'=4,'ep_2'=2,'tp'=4] {'ep_2'}, dimensions={0} | all-to-all | bytes 1048576 | tf_op jit(solution)/shard_map/all_to_all | solution.py:210
  89.4 2.0 reduce_sum.51
  91.4 11.3 %all_to_all.59 = bf16[4,128,256]{2,1,0:T(8,128)(2,1)} all-to-all(bf16[4,128,256]{2,1,0:T(8,128)(2,1)} %bitcast.72), channel_id=1, replica_groups=mesh['ep_0'=16,'ep_1'=4,'ep_2'=2,'tp'=4] {'ep_1'}, dimensions={0} | all-to-all | bytes 524288 | tf_op jit(solution)/shard_map/all_to_all | solution.py:210
  102.7 1.6 reduce_sum.52
  104.3 1.5 pad_maximum_fusion
  105.8 4.2 %all-to-all-start.6 = ((bf16[16,16,256]{2,1,0:T(8,128)(2,1)}), bf16[16,16,256]{2,1,0:T(8,128)(2,1)}, u32[]{:S(2)}, u32[]{:S(2)}) async-start(bf16[16,16,256]{2,1,0:T(8,128)(2,1)} %pad_maximum_fusion), calls=%async_computation.6 | async-start | bytes 262144 | tf_op jit(solution)/shard_map/all_to_all | solution.py:210
  110.0 1.1 copy-done.1
  111.1 1.1 copy-done.3
  112.2 2.9 %shard_map.147 = (bf16[4,336,256]{2,1,0:T(8,128)(2,1)}, bf16[320,352]{1,0:T(8,128)(2,1)S(1)}, bf16[320,352]{1,0:T(8,128)(2,1)S(1)}, bf16[320,352]{1,0:T(8,128)(2,1)S(1)}) custom-call(bf16[4,336,512]{2,1,0:T(8,128)(2,1)S(1)} %collective-permute-done.in_ref.other_ref, bf16[352,1024]{1,0:T(8,128)(2,1)S(1)} %bitcast.53, bf16[352,1024]{1,0:T(8,128)(2,1)S(1)} %bitcast.55, ...), custom_call_target="tpu_custom_call" | custom-call | tf_op jit(solution)/shard_map/pallas_call | solution.py:41
  117.2 1.9 collective-permute-start.1
  119.2 4.9 %all-to-all-done.6 = bf16[16,16,256]{2,1,0:T(8,128)(2,1)} async-done(((bf16[16,16,256]{2,1,0:T(8,128)(2,1)}), bf16[16,16,256]{2,1,0:T(8,128)(2,1)}, u32[]{:S(2)}, u32[]{:S(2)}) %all-to-all-start.6) | async-done | bytes 131104 | tf_op jit(solution)/shard_map/all_to_all | solution.py:210
  126.4 3.3 %all-to-all-start.7 = ((f32[8,1,128]{2,1,0:T(1,128)}), f32[8,1,128]{2,1,0:T(1,128)S(1)}, u32[]{:S(2)}, u32[]{:S(2)}) async-start(f32[8,1,128]{2,1,0:T(1,128)} %broadcast_in_dim.51), calls=%async_computation.7 | async-start | bytes 8192 | tf_op jit(solution)/shard_map/all_to_all | solution.py:210
  129.8 1.5 slice_bitcast_fusion
  131.2 1.1 copy-done.2
  132.3 1.1 copy-done.4
  133.5 2.0 shard_map.146
  138.5 1.6 broadcast_in_dim.53
  140.0 4.8 %all-to-all-start.9 = ((bf16[4,128,256]{2,1,0:T(8,128)(2,1)}), bf16[4,128,256]{2,1,0:T(8,128)(2,1)S(1)}, u32[]{:S(2)}, u32[]{:S(2)}) async-start(bf16[4,128,256]{2,1,0:T(8,128)(2,1)} %broadcast_in_dim.53), calls=%async_computation.9 | async-start | bytes 524288 | tf_op jit(solution)/shard_map/all_to_all | solution.py:210
  144.8 2.3 %add_convert_fusion = bf16[4,336,256]{2,1,0:T(8,128)(2,1)} fusion(bf16[4,336,256]{2,1,0:T(8,128)(2,1)} %collective-permute-done.1, bf16[4,336,256]{2,1,0:T(8,128)(2,1)} %copy-done.6), kind=kLoop, calls=%fused_computation | loop fusion | flops 1376256 | bytes 2064384 | tf_op jit(solution)/shard_map/convert_element_type | solution.py:283
  147.2 3.8 %all-to-all-done.9 = bf16[4,128,256]{2,1,0:T(8,128)(2,1)S(1)} async-done(((bf16[4,128,256]{2,1,0:T(8,128)(2,1)}), bf16[4,128,256]{2,1,0:T(8,128)(2,1)S(1)}, u32[]{:S(2)}, u32[]{:S(2)}) %all-to-all-start.9) | async-done | bytes 262176 | tf_op jit(solution)/shard_map/all_to_all | solution.py:210
  151.6 4.4 %all-to-all-start.2 = ((bf16[4,336,256]{2,1,0:T(8,128)(2,1)}), bf16[4,336,256]{2,1,0:T(8,128)(2,1)S(1)}, u32[]{:S(2)}, u32[]{:S(2)}) async-start(bf16[4,336,256]{2,1,0:T(8,128)(2,1)} %add_convert_fusion), calls=%async_computation.2 | async-start | bytes 1376256 | tf_op jit(solution)/shard_map/all_to_all | solution.py:210
  156.1 10.3 %all-to-all-done.2.in_ref = bf16[4,336,256]{2,1,0:T(8,128)(2,1)S(1)} async-done(((bf16[4,336,256]{2,1,0:T(8,128)(2,1)}), bf16[4,336,256]{2,1,0:T(8,128)(2,1)S(1)}, u32[]{:S(2)}, u32[]{:S(2)}) %all-to-all-start.2) | async-done | bytes 688160 | tf_op jit(solution)/shard_map/all_to_all | solution.py:210
  166.4 1.8 broadcast_in_dim.55
  168.2 4.2 %all-to-all-start.10 = ((bf16[2,512,256]{2,1,0:T(8,128)(2,1)}), bf16[2,512,256]{2,1,0:T(8,128)(2,1)}, u32[]{:S(2)}, u32[]{:S(2)}) async-start(bf16[2,512,256]{2,1,0:T(8,128)(2,1)} %broadcast_in_dim.55), calls=%async_computation.10 | async-start | bytes 1048576 | tf_op jit(solution)/shard_map/all_to_all | solution.py:210
  174.3 9.4 %all-to-all-start.8 = ((bf16[64,8,256]{2,1,0:T(8,128)(2,1)}), bf16[64,8,256]{2,1,0:T(8,128)(2,1)S(1)}, u32[]{:S(2)}, u32[]{:S(2)}) async-start(bf16[64,8,256]{2,1,0:T(8,128)(2,1)} %bitcast.60), calls=%async_computation.8 | async-start | bytes 524288 | tf_op jit(solution)/shard_map/all_to_all | solution.py:210
  183.8 1.3 multiply_convert_fusion
  186.5 2.7 %shard_map.150 = (bf16[352,1024]{1,0:T(8,128)(2,1)}, bf16[352,1024]{1,0:T(8,128)(2,1)}, bf16[352,1024]{1,0:T(8,128)(2,1)}) custom-call(bf16[4,336,512]{2,1,0:T(8,128)(2,1)S(1)} %all_to_all.56.in_ref.own_ref, bf16[4,336,512]{2,1,0:T(8,128)(2,1)S(1)} %collective-permute-done.in_ref.other_ref, bf16[320,352]{1,0:T(8,128)(2,1)S(1)} %copy-done.18, ...), custom_call_target="tpu_custom_call" | custom-call | tf_op jit(solution)/shard_map/pallas_call | solution.py:41
  189.2 16.3 %all-to-all-done.8 = bf16[64,8,256]{2,1,0:T(8,128)(2,1)S(1)} async-done(((bf16[64,8,256]{2,1,0:T(8,128)(2,1)}), bf16[64,8,256]{2,1,0:T(8,128)(2,1)S(1)}, u32[]{:S(2)}, u32[]{:S(2)}) %all-to-all-start.8) | async-done | bytes 262176 | tf_op jit(solution)/shard_map/all_to_all | solution.py:210
  (80 shorter events, 18.4 us)
Async XLA Ops:
  0.6 0.8 copy-start.7
  1.5 0.8 copy-start.9
  50.7 23.0 %copy-start.8 = (bf16[128,256]{1,0:T(8,128)(2,1)S(1)}, bf16[128,256]{1,0:T(8,128)(2,1)}, u32[]{:S(2)}) copy-start(bf16[128,256]{1,0:T(8,128)(2,1)} %cot_ref.1) | copy-start | bytes 196612
  50.7 33.2 %copy-start.10 = (bf16[128,256]{1,0:T(8,128)(2,1)S(1)}, bf16[128,256]{1,0:T(8,128)(2,1)}, u32[]{:S(2)}) copy-start(bf16[128,256]{1,0:T(8,128)(2,1)} %tok_ref.1) | copy-start | bytes 196612
  71.8 38.2 %collective-permute-start = (bf16[4,336,512]{2,1,0:T(8,128)(2,1)S(1)}, bf16[4,336,512]{2,1,0:T(8,128)(2,1)S(1)}, u32[]{:S(2)}, u32[]{:S(2)}) collective-permute-start(bf16[4,336,512]{2,1,0:T(8,128)(2,1)S(1)} %all_to_all.56.in_ref.own_ref), channel_id=1, source_target_pairs={{0,4},{4,0},{1,5},{5,1},{2,6},{6,2},{3,7},{7,3},{8,12},{12,8},{9,1... | collective-permute-start | bytes 4128776 | tf_op jit(solution)/shard_map/ppermute | solution.py:273
  83.9 0.7 copy-start.25
  84.2 20.1 %copy-start.27 = (bf16[256,8]{0,1:T(8,128)(2,1)S(1)}, bf16[256,8]{0,1:T(8,128)(2,1)}, u32[]{:S(2)}) copy-start(bf16[256,8]{0,1:T(8,128)(2,1)} %param.16) | copy-start | bytes 12292
  89.4 20.6 %copy-start = (bf16[1,1024,352]{1,2,0:T(8,128)(2,1)S(1)}, bf16[1,1024,352]{1,2,0:T(8,128)(2,1)}, u32[]{:S(2)}) copy-start(bf16[1,1024,352]{1,2,0:T(8,128)(2,1)} %param.13) | copy-start | bytes 2162692
  105.8 18.4 %all-to-all-start.6 = ((bf16[16,16,256]{2,1,0:T(8,128)(2,1)}), bf16[16,16,256]{2,1,0:T(8,128)(2,1)}, u32[]{:S(2)}, u32[]{:S(2)}) async-start(bf16[16,16,256]{2,1,0:T(8,128)(2,1)} %pad_maximum_fusion), calls=%async_computation.6 | async-start | bytes 262144 | tf_op jit(solution)/shard_map/all_to_all | solution.py:210
  110.0 1.1 copy-start.1
  111.1 1.1 copy-start.3
  112.2 6.9 %copy-start.28 = (f32[1024]{0:T(1024)S(1)}, f32[1024]{0:T(1024)}, u32[]{:S(2)}) copy-start(f32[1024]{0:T(1024)} %param.17) | copy-start | bytes 12292
  115.8 0.7 copy-start.13
  116.5 0.7 copy-start.15
  117.2 27.6 %collective-permute-start.1 = (bf16[4,336,256]{2,1,0:T(8,128)(2,1)}, bf16[4,336,256]{2,1,0:T(8,128)(2,1)}, u32[]{:S(2)}, u32[]{:S(2)}) collective-permute-start(bf16[4,336,256]{2,1,0:T(8,128)(2,1)} %get-tuple-element.26), channel_id=1, source_target_pairs={{0,4},{4,0},{1,5},{5,1},{2,6},{6,2},{3,7},{7,3},{8,12},{12,8},{9,1... | collective-permute-start | bytes 2064392 | tf_op jit(solution)/shard_map/ppermute | solution.py:282
  126.4 12.0 %all-to-all-start.7 = ((f32[8,1,128]{2,1,0:T(1,128)}), f32[8,1,128]{2,1,0:T(1,128)S(1)}, u32[]{:S(2)}, u32[]{:S(2)}) async-start(f32[8,1,128]{2,1,0:T(1,128)} %broadcast_in_dim.51), calls=%async_computation.7 | async-start | bytes 8192 | tf_op jit(solution)/shard_map/all_to_all | solution.py:210
  131.2 1.1 copy-start.2
  132.3 1.1 copy-start.4
  135.5 0.9 copy-start.6
  137.0 0.7 copy-start.19
  137.7 0.7 copy-start.21
  140.0 10.9 %all-to-all-start.9 = ((bf16[4,128,256]{2,1,0:T(8,128)(2,1)}), bf16[4,128,256]{2,1,0:T(8,128)(2,1)S(1)}, u32[]{:S(2)}, u32[]{:S(2)}) async-start(bf16[4,128,256]{2,1,0:T(8,128)(2,1)} %broadcast_in_dim.53), calls=%async_computation.9 | async-start | bytes 524288 | tf_op jit(solution)/shard_map/all_to_all | solution.py:210
  151.6 14.8 %all-to-all-start.2 = ((bf16[4,336,256]{2,1,0:T(8,128)(2,1)}), bf16[4,336,256]{2,1,0:T(8,128)(2,1)S(1)}, u32[]{:S(2)}, u32[]{:S(2)}) async-start(bf16[4,336,256]{2,1,0:T(8,128)(2,1)} %add_convert_fusion), calls=%async_computation.2 | async-start | bytes 1376256 | tf_op jit(solution)/shard_map/all_to_all | solution.py:210
  168.2 6.1 %all-to-all-start.10 = ((bf16[2,512,256]{2,1,0:T(8,128)(2,1)}), bf16[2,512,256]{2,1,0:T(8,128)(2,1)}, u32[]{:S(2)}, u32[]{:S(2)}) async-start(bf16[2,512,256]{2,1,0:T(8,128)(2,1)} %broadcast_in_dim.55), calls=%async_computation.10 | async-start | bytes 1048576 | tf_op jit(solution)/shard_map/all_to_all | solution.py:210
  173.1 0.7 copy-start.5
  174.3 31.2 %all-to-all-start.8 = ((bf16[64,8,256]{2,1,0:T(8,128)(2,1)}), bf16[64,8,256]{2,1,0:T(8,128)(2,1)S(1)}, u32[]{:S(2)}, u32[]{:S(2)}) async-start(bf16[64,8,256]{2,1,0:T(8,128)(2,1)} %bitcast.60), calls=%async_computation.8 | async-start | bytes 524288 | tf_op jit(solution)/shard_map/all_to_all | solution.py:210
  183.7 2.7 %copy-start.12 = (bf16[320,352]{1,0:T(8,128)(2,1)S(1)}, bf16[320,352]{1,0:T(8,128)(2,1)}, u32[]{:S(2)}) copy-start(bf16[320,352]{1,0:T(8,128)(2,1)} %copy-done.11) | copy-start | bytes 675844
  183.7 2.7 %copy-start.14 = (bf16[320,352]{1,0:T(8,128)(2,1)S(1)}, bf16[320,352]{1,0:T(8,128)(2,1)}, u32[]{:S(2)}) copy-start(bf16[320,352]{1,0:T(8,128)(2,1)} %copy-done.13) | copy-start | bytes 675844
  183.7 2.7 %copy-start.16 = (bf16[320,352]{1,0:T(8,128)(2,1)S(1)}, bf16[320,352]{1,0:T(8,128)(2,1)}, u32[]{:S(2)}) copy-start(bf16[320,352]{1,0:T(8,128)(2,1)} %copy-done.15) | copy-start | bytes 675844
  183.7 2.7 %copy-start.18 = (bf16[320,352]{1,0:T(8,128)(2,1)S(1)}, bf16[320,352]{1,0:T(8,128)(2,1)}, u32[]{:S(2)}) copy-start(bf16[320,352]{1,0:T(8,128)(2,1)} %copy-done.17) | copy-start | bytes 675844
  183.8 2.7 %copy-start.20 = (bf16[320,352]{1,0:T(8,128)(2,1)S(1)}, bf16[320,352]{1,0:T(8,128)(2,1)}, u32[]{:S(2)}) copy-start(bf16[320,352]{1,0:T(8,128)(2,1)} %copy-done.19) | copy-start | bytes 675844
  183.8 2.7 %copy-start.22 = (bf16[320,352]{1,0:T(8,128)(2,1)S(1)}, bf16[320,352]{1,0:T(8,128)(2,1)}, u32[]{:S(2)}) copy-start(bf16[320,352]{1,0:T(8,128)(2,1)} %copy-done.21) | copy-start | bytes 675844
  (5 other events, 3.4 us)

commit v2 on v1

--- a/solution.py
+++ b/solution.py
@@ -5,6 +5,7 @@
 from jax.experimental.pallas import tpu as pltpu
 from jax.sharding import Mesh
 from jax.sharding import PartitionSpec as P
+
 
 EP = ("ep_0", "ep_1", "ep_2")
 CHIPS = ("ep_0", "ep_1")
@@ -37,16 +38,40 @@
     return jnp.where(cond, 1.0, 0.0).astype(BF16)
 
 
-def call(kernel, outs, *args):
+def call(kernel, outs, *args, after=(), scratch=(), hbm=0, flops=0, out_specs=None):
+    whole = pl.BlockSpec(memory_space=pltpu.VMEM)
+    placed = pl.BlockSpec(memory_space=pl.ANY)
+    in_hbm = pl.BlockSpec(memory_space=pltpu.HBM)
+    count = len(args)
+
+    def body(*refs):
+        kernel(*refs[:count], *refs[count + len(after) :])
+
     return pl.pallas_call(
-        kernel,
+        body,
         out_shape=outs,
-        compiler_params=pltpu.CompilerParams(vmem_limit_bytes=48 * 1024 * 1024),
-    )(*args)
-
-
-def pack_kernel(routes_ref, weights_ref, tok_ref, cot_ref, out_ref, keys_ref, cols_ref):
+        in_specs=[in_hbm] * hbm + [whole] * (count - hbm) + [placed] * len(after),
+        out_specs=out_specs or jax.tree.map(lambda _: whole, outs),
+        scratch_shapes=list(scratch),
+        cost_estimate=pl.CostEstimate(
+            flops=flops or 200_000_000, bytes_accessed=1_000_000, transcendentals=0
+        ),
+        compiler_params=pltpu.CompilerParams(vmem_limit_bytes=20 * 1024 * 1024),
+    )(*args, *after)
+
+
+def struct(*shape, dtype=BF16):
+    return jax.ShapeDtypeStruct(shape, dtype)
+
+
+def pack_kernel(
+    tok_hbm, cot_hbm, routes_ref, weights_ref, out_ref, keys_ref, cols_ref, cot_ref, tok_ref, sems
+):
     tokens = 128
+    tok_copy = pltpu.make_async_copy(tok_hbm, tok_ref, sems.at[0])
+    cot_copy = pltpu.make_async_copy(cot_hbm, cot_ref, sems.at[1])
+    tok_copy.start()
+    cot_copy.start()
     r0 = routes_ref[0:1, :].astype(F32)
     r1 = routes_ref[1:2, :].astype(F32)
     w = weights_ref[...].astype(F32)
@@ -73,6 +98,8 @@
     m_row = iota((msgs, 512), 0)
     dest = m_row // 8
     sub = m_row % 8
+    tok_copy.wait()
+    cot_copy.wait()
     data = jnp.concatenate(
         [tok_ref[:, :128], tok_ref[:, 128:], cot_ref[:, :128], cot_ref[:, 128:]], axis=0
     )
@@ -124,7 +151,25 @@
         out_ref[t, ROWS : ROWS + EXTRA, 0:ROWS] = w_row
 
 
-def expert_kernel(in_ref, wg_ref, wu_ref, wd_ref, z_ref, dg_ref, du_ref, wt_ref):
+def expert_kernel(
+    in_hbm, wg_hbm, wu_hbm, wd_hbm, z_ref, dg_out, du_out, wt_out,
+    in_ref, wg_ref, wu_ref, wd_ref, dg_ref, du_ref, wt_ref, sems,
+):
+    inward = [
+        pltpu.make_async_copy(src, dst, sems.at[n])
+        for n, (src, dst) in enumerate(
+            ((in_hbm, in_ref), (wg_hbm, wg_ref), (wu_hbm, wu_ref), (wd_hbm, wd_ref))
+        )
+    ]
+    outward = [
+        pltpu.make_async_copy(src, dst, sems.at[4 + n])
+        for n, (src, dst) in enumerate(((dg_ref, dg_out), (du_ref, du_out), (wt_ref, wt_out)))
+    ]
+    for copy in inward:
+        copy.start()
+    inward[0].wait()
+    inward[1].wait()
+
     def summed(lo, w_ref):
         return sum(
             dot_nt(in_ref[t, 0:ROWS, lo : lo + 256], w_ref[:, t * 256 : (t + 1) * 256])
@@ -132,7 +177,9 @@
         )
 
     pre_gate = summed(0, wg_ref)
+    inward[2].wait()
     pre_up = summed(0, wu_ref)
+    inward[3].wait()
     projected = summed(256, wd_ref)
     w_row = in_ref[0, ROWS : ROWS + EXTRA, 0:ROWS].astype(F32)[0:1, :]
     eye = iota((ROWS, ROWS), 0) == iota((ROWS, ROWS), 1)
@@ -147,6 +194,8 @@
     dg_ref[...] = d_gate
     du_ref[...] = d_up
     wt_ref[...] = (weight * hidden).astype(BF16)
+    for copy in outward:
+        copy.start()
     part = (dot(d_gate, wg_ref[...]) + dot(d_up, wu_ref[...])).astype(BF16)
     hi = route.astype(BF16).astype(F32)
     lo = route - hi
@@ -159,9 +208,11 @@
     for t in range(TP):
         z_ref[t, 0:ROWS, :] = part[:, t * 256 : (t + 1) * 256]
         z_ref[t, ROWS : ROWS + EXTRA, :] = extra
-
-
-def return_kernel(in_ref, mix_ref, out_ref):
+    for copy in outward:
+        copy.wait()
+
+
+def return_kernel(in_ref, m0_ref, m1_ref, m2_ref, m3_ref, out_ref):
     total = sum(in_ref[t].astype(F32) for t in range(TP))
     msgs = EXPERTS * 8
     rows = total[0:ROWS].astype(BF16)
@@ -181,8 +232,19 @@
     b_col = iota((512, 256), 1)
     out = out + dot(jnp.where(mine, hi, 0.0).astype(BF16), onehot(b_row // 64 == b_col))
     out = out + dot(jnp.where(mine, lo, 0.0).astype(BF16), onehot(b_row // 64 == b_col - 128))
+    came = [m_ref[0:1, :] for m_ref in (m0_ref, m1_ref, m2_ref, m3_ref)]
+    here = lax.axis_index("tp")
+    mix = jnp.zeros((1, 128), F32)
+    for t in range(TP):
+        back = lax.rem(here - t + TP, TP)
+        pick = came[3]
+        for n in range(3):
+            pick = jnp.where(back == n, came[n], pick)
+        mix = mix + pick
+    mix_hi = mix.astype(BF16).astype(F32)
+    mix_row = jnp.concatenate([mix_hi, mix - mix_hi], axis=1)
     out_sub = iota((msgs, 256), 0) % 8
-    out = jnp.where(out_sub == CAP + 1, mix_ref[...], out)
+    out = jnp.where(out_sub == CAP + 1, mix_row, out)
     out_ref[...] = out.astype(BF16)
 
 
@@ -206,129 +268,245 @@
     mix_ref[...] = mix[:, 0:128] + mix[:, 128:256]
 
 
+def moment_kernel(cot_ref, tok_ref, keep_ref, send_ref):
+    moment = dot_tn(cot_ref[...], tok_ref[...])
+    north = lax.axis_index("ep_2") == 1
+    for x in range(4):
+        parts = []
+        for c in range(2):
+            starts = [(z * 8 + x * 2 + c) * 8 for z in range(16)]
+            parts.append(jnp.concatenate([moment[s : s + 8] for s in starts], axis=0))
+        span = slice(x * 128, (x + 1) * 128)
+        keep_ref[span, :] = jnp.where(north, parts[1], parts[0])
+        send_ref[span, :] = jnp.where(north, parts[0], parts[1]).astype(BF16)
+
+
+def core_sum_kernel(keep_ref, got_ref, own_ref, s1_ref, s2_ref, s3_ref, sum_ref):
+    sum_ref[...] = keep_ref[...] + got_ref[...].astype(F32)
+    here = lax.axis_index("ep_1")
+
+    def part(shift):
+        start = pl.multiple_of(lax.rem(here + shift, 4) * 128, 128)
+        return sum_ref[pl.ds(start, 128), :]
+
+    own_ref[...] = part(0)
+    s1_ref[...] = part(1).astype(BF16)
+    s2_ref[...] = part(2).astype(BF16)
+    s3_ref[...] = part(3).astype(BF16)
+
+
+def x_sum_kernel(own_ref, r1_ref, r2_ref, r3_ref, dense_ref, out_ref):
+    total = own_ref[...] + r1_ref[...].astype(F32)
+    total = total + (r2_ref[...].astype(F32) + r3_ref[...].astype(F32))
+    dense = dense_ref[...].astype(F32)
+    pieces = []
+    for z in range(16):
+        pieces += [total[z * 8 : z * 8 + 8], dense]
+    out_ref[...] = jnp.concatenate(pieces, axis=0).astype(BF16)
+
+
+def z_sum_kernel(in_ref, gate_ref, dense_ref, grad_ref, share_ref, w_ref):
+    got = in_ref[...].astype(F32)
+    moment = sum(got[z * 16 : z * 16 + 8] for z in range(16)) * (1.0 / 128)
+    w_ref[...] = jnp.concatenate(
+        [got[z * 16 + 8 : z * 16 + 16] for z in range(16)], axis=0
+    ).astype(BF16)
+    core = lax.axis_index("ep_2")
+    first = (lax.axis_index("ep_0") * 8 + lax.axis_index("ep_1") * 2 + core) * 8
+    at = iota((8, 1024), 1) == first + iota((8, 1024), 0)
+    gate = jnp.sum(jnp.where(at, gate_ref[...], 0.0), axis=1, keepdims=True)
+    grad_ref[...] = moment * gate
+    share = jnp.sum(moment * dense_ref[...].astype(F32), axis=1, keepdims=True)
+    spot = iota((8, 128), 1) == core * 8 + iota((8, 128), 0)
+    row = jnp.sum(jnp.where(spot, share, 0.0), axis=0, keepdims=True)
+    share_ref[...] = jnp.broadcast_to(row, (8, 128))
+
+
+def dense_kernel(cot_ref, gate_ref, own_ref, other_ref, out_ref):
+    north = lax.axis_index("ep_2") == 1
+    own = own_ref[...].astype(F32)
+    other = other_ref[...].astype(F32)
+    south_w = jnp.where(north, other, own)
+    north_w = jnp.where(north, own, other)
+    pieces = []
+    for z in range(16):
+        for x in range(4):
+            s = (x * 16 + z) * 8
+            pieces += [south_w[s : s + 8], north_w[s : s + 8]]
+    weight = jnp.concatenate(pieces, axis=0).astype(BF16)
+    scaled = (gate_ref[...] * cot_ref[...].astype(F32)).astype(BF16)
+    out_ref[...] = dot(scaled, weight)
+
+
+def add_kernel(a_ref, b_ref, out_ref):
+    out_ref[...] = (a_ref[...].astype(F32) + b_ref[...].astype(F32)).astype(BF16)
+
+
+def share_kernel(a_ref, b_ref, out_ref):
+    out_ref[...] = a_ref[...] + b_ref[...]
+
+
+def in_place(*arrays):
+    return [pltpu.with_memory_space_constraint(a, pltpu.HBM) for a in arrays]
+
+
 def swap(value, axes):
     return lax.all_to_all(value, axes, split_axis=0, concat_axis=0, tiled=True)
 
 
-def copies(value, n):
-    return jnp.broadcast_to(value[None], (n,) + value.shape)
+def shift(value, axis, by):
+    n = lax.axis_size(axis)
+    return lax.ppermute(value, axis, [(i, (i + by) % n) for i in range(n)])
 
 
 def local(tokens, cotangent, routes, route_weights, w_gate, w_up, w_down, dense_weight, mix_gate):
-    ep_count = lax.axis_size(EP)
     wg = w_gate[0].T
     wu = w_up[0].T
     wd = w_down[0]
     dense_t = dense_weight.T
-    packed, keys, cols = call(
+    gate_row = mix_gate[None, :]
+    tokens, cotangent, wg, wu, wd, routes_t, weights_t = in_place(
+        tokens, cotangent, wg, wu, wd, routes.T, route_weights.T
+    )
+    packed, keys, cols, cot_here = call(
         pack_kernel,
         (
-            jax.ShapeDtypeStruct((512, 384), BF16),
-            jax.ShapeDtypeStruct((8, 128), F32),
-            jax.ShapeDtypeStruct((128, 128), F32),
+            struct(512, 384),
+            struct(8, 128, dtype=F32),
+            struct(128, 128, dtype=F32),
+            struct(128, 256),
         ),
-        routes.T,
-        route_weights.T,
         tokens,
         cotangent,
+        routes_t,
+        weights_t,
+        hbm=2,
+        scratch=(
+            pltpu.VMEM((128, 256), BF16),
+            pltpu.SemaphoreType.DMA((2,)),
+        ),
     )
     arrived = swap(packed.reshape(64, 8, 384), CHIPS)
 
-    cot_all = swap(copies(cotangent, TP), "tp")
-    moment = lax.dot_general(
-        jnp.swapaxes(cot_all, 1, 2).reshape(1024, 128), tokens, (((1,), (0,)), ((), ())),
-        preferred_element_type=F32,
-    ).astype(BF16)
-    moment = moment.reshape(16, 4, 2, 8, 256).transpose(2, 1, 0, 3, 4).reshape(2, 512, 256)
-    moment = jnp.sum(swap(moment, "ep_2").astype(F32), axis=0).astype(BF16)
-    moment = jnp.sum(swap(moment.reshape(4, 128, 256), "ep_1").astype(F32), axis=0).astype(BF16)
-    both = jnp.concatenate([moment.reshape(16, 8, 256), copies(dense_t, 16)], axis=1)
-    both = swap(both, "ep_0")
-    moment = jnp.sum(both[:, 0:8].astype(F32), axis=0) * (1.0 / ep_count)
-    gate = lax.dynamic_slice(mix_gate, (lax.axis_index(EP) * 8,), (8,))
-    dense_grad = (moment * gate[:, None]).T
-    share = jnp.sum(moment * dense_t.astype(F32), axis=1)
-    share = jnp.pad(share[None, :], ((0, 0), (0, 120)))
-    shares = swap(copies(share, 8), ("ep_2", "tp"))
-    mix = jnp.sum(shares.reshape(2, TP, 128)[:, :, :8], axis=1).reshape(1, 16)
-    mix_hi = mix.astype(BF16).astype(F32)
-    mix_row = jnp.concatenate(
-        [jnp.pad(mix_hi, ((0, 0), (0, 112))), jnp.pad(mix - mix_hi, ((0, 0), (0, 112)))], axis=1
-    )
-    dense_w = swap(copies(both[:, 8:16].reshape(128, 256), 4), "ep_1")
-    dense_w = swap(copies(dense_w.reshape(512, 256), 2), "ep_2")
-    dense_w = dense_w.reshape(2, 4, 16, 8, 256).transpose(2, 1, 0, 3, 4).reshape(TP, 256, 256)
-    scaled = (mix_gate.reshape(TP, 1, 256) * cot_all.astype(F32)).astype(BF16)
-    dense_dx = lax.dot_general(
-        jnp.swapaxes(scaled, 0, 1).reshape(128, 1024), dense_w.reshape(1024, 256),
-        (((1,), (0,)), ((), ())), preferred_element_type=F32,
+    cot_all = lax.all_gather(cot_here, "tp", axis=1, tiled=True)
+    keep, send = call(
+        moment_kernel, (struct(512, 256, dtype=F32), struct(512, 256)), cot_all, tokens
+    )
+    here, *away = call(
+        core_sum_kernel,
+        (struct(128, 256, dtype=F32),) + (struct(128, 256),) * 3,
+        keep,
+        shift(send, "ep_2", 1),
+        scratch=(pltpu.VMEM((512, 256), F32),),
+    )
+    both = call(
+        x_sum_kernel,
+        struct(256, 256),
+        here,
+        *(shift(piece, "ep_1", i + 1) for i, piece in enumerate(away)),
+        dense_t,
     )
 
     own = call(
-        unpack_kernel,
-        jax.ShapeDtypeStruct((TP, ROWS + EXTRA, 512), BF16),
-        arrived.reshape(512, 384),
-    )
-    own = swap(own, "tp")
-    other = lax.ppermute(own, "ep_2", [(0, 1), (1, 0)])
-    outs = (
-        jax.ShapeDtypeStruct((TP, ROWS + EXTRA, 256), BF16),
-        jax.ShapeDtypeStruct((ROWS, 352), BF16),
-        jax.ShapeDtypeStruct((ROWS, 352), BF16),
-        jax.ShapeDtypeStruct((ROWS, 352), BF16),
-    )
-    z_own, *act_own = call(expert_kernel, outs, own, wg, wu, wd)
-    z_other, *act_other = call(expert_kernel, outs, other, wg, wu, wd)
-    z_back = lax.ppermute(z_other, "ep_2", [(0, 1), (1, 0)])
-    z_sum = (z_own.astype(F32) + z_back.astype(F32)).astype(BF16)
+        unpack_kernel, struct(TP, ROWS + EXTRA, 512), arrived.reshape(512, 384), after=(here,)
+    )
+    own, both = lax.optimization_barrier((swap(own, "tp"), both))
+    other = shift(own, "ep_2", 1)
+    outs = (struct(TP, ROWS + EXTRA, 256),) + (pltpu.HBM((ROWS, 352), BF16),) * 3
+    hbm_spec = pl.BlockSpec(memory_space=pltpu.HBM)
+    vmem_spec = pl.BlockSpec(memory_space=pltpu.VMEM)
+    expert = dict(
+        hbm=4,
+        flops=1_150_000_000,
+        out_specs=(vmem_spec,) + (hbm_spec,) * 3,
+        scratch=(pltpu.VMEM((TP, ROWS + EXTRA, 512), BF16),)
+        + (pltpu.VMEM((352, 1024), BF16),) * 3
+        + (pltpu.VMEM((ROWS, 352), BF16),) * 3
+        + (pltpu.SemaphoreType.DMA((7,)),),
+    )
+    z_own, *act_own = call(expert_kernel, outs, own, wg, wu, wd, **expert)
+    z_got = swap(both.reshape(16, 16, 256), "ep_0").reshape(256, 256)
+    z_other, *act_other = call(expert_kernel, outs, other, wg, wu, wd, **expert)
+    z_back = shift(z_other, "ep_2", 1)
+    z_back, z_got = lax.optimization_barrier((z_back, z_got))
+    dense_grad, share, dense_w = call(
+        z_sum_kernel,
+        (struct(8, 256, dtype=F32), struct(8, 128, dtype=F32), struct(128, 256)),
+        z_got,
+        gate_row,
+        dense_t,
+    )
+    z_sum = call(add_kernel, outs[0], z_own, z_back)
     z_all = swap(z_sum, "tp")
-    back = call(return_kernel, jax.ShapeDtypeStruct((512, 256), BF16), z_all, mix_row)
-    back = swap(back.reshape(64, 8, 256), CHIPS).reshape(512, 256)
+    share = call(
+        share_kernel, struct(8, 128, dtype=F32), share, shift(share, "ep_2", 1), after=(z_sum,)
+    )
+    shares = [share] + [shift(share, "tp", by) for by in (1, 2, 3)]
+    back_ready = call(return_kernel, struct(512, 256), z_all, *shares)
+    gate_grad, up_grad, down_grad, grads_done = call(
+        grads_kernel,
+        (struct(352, 1024),) * 3 + (struct(8, 128, dtype=F32),),
+        own,
+        other,
+        *in_place(*act_own, *act_other),
+        after=(back_ready,),
+        scratch=(pltpu.VMEM((352, 1024), BF16),) * 3 + (pltpu.SemaphoreType.DMA((3,)),),
+        out_specs=(hbm_spec,) * 3 + (vmem_spec,),
+        flops=1_400_000_000,
+    )
+    back = swap(back_ready.reshape(64, 8, 256), CHIPS).reshape(512, 256)
+
+    dense_w = lax.all_gather(dense_w, "ep_1", axis=0, tiled=True)
+    dense_dx = call(
+        dense_kernel,
+        struct(128, 256, dtype=F32),
+        cot_all,
+        gate_row,
+        dense_w,
+        shift(dense_w, "ep_2", 1),
+    )
     token_grad, route_t, mix_all = call(
         final_kernel,
-        (
-            jax.ShapeDtypeStruct((128, 256), BF16),
-            jax.ShapeDtypeStruct((2, 128), F32),
-            jax.ShapeDtypeStruct((EXPERTS, 128), F32),
-        ),
+        (struct(128, 256), struct(2, 128, dtype=F32), struct(EXPERTS, 128, dtype=F32)),
         back,
         keys,
         cols,
         dense_dx,
+        after=(grads_done,),
     )
     mix_grad = mix_all[:, :16].reshape(1024)
-
-    gate_grad, up_grad, down_grad = call(
-        grads_kernel,
-        tuple(jax.ShapeDtypeStruct((352, 1024), BF16) for _ in range(3)),
-        own,
-        other,
-        *act_own,
-        *act_other,
-    )
     return (
         token_grad,
         route_t.T,
         gate_grad.T[None],
         up_grad.T[None],
         down_grad[None],
-        dense_grad,
+        dense_grad.T,
         mix_grad,
     )
 
 
-def grads_kernel(own_ref, other_ref, dg0, du0, wt0, dg1, du1, wt1, gate_ref, up_ref, down_ref):
-    for left0, left1, lo, out_ref in (
-        (dg0, dg1, 0, gate_ref),
-        (du0, du1, 0, up_ref),
-        (wt0, wt1, 256, down_ref),
-    ):
+def grads_kernel(
+    own_ref, other_ref, dg0, du0, wt0, dg1, du1, wt1,
+    gate_ref, up_ref, down_ref, done_ref, gate_tmp, up_tmp, down_tmp, sems,
+):
+    copies = []
+    for n, (left0, left1, lo, out_ref, tmp) in enumerate((
+        (dg0, dg1, 0, gate_ref, gate_tmp),
+        (du0, du1, 0, up_ref, up_tmp),
+        (wt0, wt1, 256, down_ref, down_tmp),
+    )):
         left = jnp.concatenate([left0[...], left1[...]], axis=0)
         for t in range(TP):
             right = jnp.concatenate(
                 [own_ref[t, 0:ROWS, lo : lo + 256], other_ref[t, 0:ROWS, lo : lo + 256]], axis=0
             )
-            out_ref[:, t * 256 : (t + 1) * 256] = dot_tn(left, right).astype(BF16)
+            tmp[:, t * 256 : (t + 1) * 256] = dot_tn(left, right).astype(BF16)
+        copies.append(pltpu.make_async_copy(tmp, out_ref, sems.at[n]))
+        copies[-1].start()
+    done_ref[...] = jnp.zeros((8, 128), F32)
+    for copy in copies:
+        copy.wait()
 
 
 def solution(mesh):

time: 209 us -> 162 us (0.78)
  the two profiles are of different devices: /device:TPU:2 before, /device:TPU:1 now
where the time goes in v2:
time: 162 us; the launch traced here: 161 us
  starting transfers between devices  85.8 us (53%)
  waiting for transfers between devices  27.2 us (17%)
  Pallas kernels  24.6 us (15%)
  blocking collectives  20.8 us (13%)
  local copies, waits for them, and re-layouts  2.01 us (1%)
    ppermute x11, starting transfers between devices, shift(): return lax.ppermute(value, axis, [(i, (i + by) % n) for i in range(n)])  46.3 us
    all_to_all x5, starting transfers between devices, swap(): return lax.all_to_all(value, axes, split_axis=0, concat_axis=0, tiled=True)  39.5 us
    pallas_call x14, Pallas kernels, call(): pl.pallas_call(body, out_shape=outs, in_specs=[in_hbm] * hbm + [whole] *...  24.6 us
    all_to_all x5, waiting for transfers between devices, swap(): return lax.all_to_all(value, axes, split_axis=0, concat_axis=0, tiled=True)  15 us
    ppermute x11, waiting for transfers between devices, shift(): return lax.ppermute(value, axis, [(i, (i + by) % n) for i in range(n)])  12.2 us
    all_gather x1, blocking collectives, local(): cot_all = lax.all_gather(cot_here, 'tp', axis=1, tiled=True)  10.7 us
    all_gather x1, blocking collectives, local(): dense_w = lax.all_gather(dense_w, 'ep_1', axis=0, tiled=True)  10.1 us
  transfers between devices with their start and end apart: 16, of which 9 were waited for; matrix products, arithmetic and copies ran while one was open for 0% of the time, Pallas kernels for 7%

profile of v2, /device:TPU:1, one launch (start us, length us, event | category | flops | bytes accessed | tf_op | source)
XLA Modules:
  0.0 161.3 jit_solution(4923946386215891614)
XLA Ops:
  0.6 3.1 %shard_map.144 = (bf16[512,384]{1,0:T(8,128)(2,1)}, f32[8,128]{1,0:T(8,128)S(1)}, f32[128,128]{1,0:T(8,128)S(1)}, bf16[128,256]{1,0:T(8,128)(2,1)S(1)}) custom-call(bf16[128,256]{1,0:T(8,128)(2,1)} %refs_1_.3, bf16[128,256]{1,0:T(8,128)(2,1)} %refs_1_.2, s32[2,128]{1,0:T(2,128)} %bitcast.41, bf16[2,128]{1,0:T(2,128)(2,1)} %bitcast.42), custom_call_target="tpu_custom_call" | custom-call | flops 200000000 | bytes 1000000 | tf_op jit(solution)/shard_map/pallas_call | solution.py:50
  3.8 19.1 %all-to-all-start = ((bf16[64,8,384]{2,1,0:T(8,128)(2,1)}), bf16[64,8,384]{2,1,0:T(8,128)(2,1)S(1)}, u32[]{:S(2)}, u32[]{:S(2)}) async-start(bf16[64,8,384]{2,1,0:T(8,128)(2,1)} %bitcast.2), calls=%async_computation | async-start | bytes 786432 | tf_op jit(solution)/shard_map/all_to_all | solution.py:354
  22.9 10.7 %all_gather.6.refs_0_ = bf16[128,1024]{1,0:T(8,128)(2,1)S(1)} all-gather(bf16[128,256]{1,0:T(8,128)(2,1)S(1)} %get-tuple-element.40), channel_id=1, replica_groups=mesh['ep_0'=16,'ep_1'=4,'ep_2'=2,'tp'=4] {'tp'}, dimensions={1}, use_global_device_ids=true | all-gather | bytes 327680 | tf_op jit(solution)/shard_map/all_gather | solution.py:391
  33.6 1.2 shard_map.145
  34.8 4.9 %collective-permute-start = (bf16[512,256]{1,0:T(8,128)(2,1)S(1)}, bf16[512,256]{1,0:T(8,128)(2,1)S(1)}, u32[]{:S(2)}, u32[]{:S(2)}) collective-permute-start(bf16[512,256]{1,0:T(8,128)(2,1)S(1)} %get-tuple-element.42), channel_id=1, source_target_pairs={{0,4},{4,0},{1,5},{5,1},{2,6},{6,2},{3,7},{7,3},{8,12},{12,8},{9,1... | collective-permute-start | bytes 786440 | tf_op jit(solution)/shard_map/ppermute | solution.py:359
  39.7 1.1 collective-permute-done.refs_1_
  40.9 6.8 %all-to-all-done = bf16[64,8,384]{2,1,0:T(8,128)(2,1)S(1)} async-done(((bf16[64,8,384]{2,1,0:T(8,128)(2,1)}), bf16[64,8,384]{2,1,0:T(8,128)(2,1)S(1)}, u32[]{:S(2)}, u32[]{:S(2)}) %all-to-all-start) | async-done | bytes 393248 | tf_op jit(solution)/shard_map/all_to_all | solution.py:354
  47.8 1.7 %shard_map.147 = bf16[4,336,512]{2,1,0:T(8,128)(2,1)} custom-call(bf16[512,384]{1,0:T(8,128)(2,1)S(1)} %bitcast.27, f32[128,256]{1,0:T(8,128)S(1)} %get-tuple-element.43.refs_1_.refs_0_), custom_call_target="tpu_custom_call" | custom-call | flops 200000000 | bytes 1000000 | tf_op jit(solution)/shard_map/pallas_call | solution.py:50
  49.4 4.3 %all-to-all-start.1 = ((bf16[4,336,512]{2,1,0:T(8,128)(2,1)}), bf16[4,336,512]{2,1,0:T(8,128)(2,1)S(1)}, u32[]{:S(2)}, u32[]{:S(2)}) async-start(bf16[4,336,512]{2,1,0:T(8,128)(2,1)} %shard_map.147), calls=%async_computation.1 | async-start | bytes 2752512 | tf_op jit(solution)/shard_map/all_to_all | solution.py:354
  53.8 3.8 %collective-permute-start.1 = (bf16[128,256]{1,0:T(8,128)(2,1)S(1)}, bf16[128,256]{1,0:T(8,128)(2,1)S(1)}, u32[]{:S(2)}, u32[]{:S(2)}) collective-permute-start(bf16[128,256]{1,0:T(8,128)(2,1)S(1)} %get-tuple-element.44), channel_id=1, source_target_pairs={{0,8},{8,16},{16,24},{24,0},{1,9},{9,17},{17,25},{25,1},{2,10},{10... | collective-permute-start | bytes 196616 | tf_op jit(solution)/shard_map/ppermute | solution.py:359
  57.5 5.4 %collective-permute-start.2 = (bf16[128,256]{1,0:T(8,128)(2,1)S(1)}, bf16[128,256]{1,0:T(8,128)(2,1)S(1)}, u32[]{:S(2)}, u32[]{:S(2)}) collective-permute-start(bf16[128,256]{1,0:T(8,128)(2,1)S(1)} %get-tuple-element.45), channel_id=1, source_target_pairs={{0,16},{8,24},{16,0},{24,8},{1,17},{9,25},{17,1},{25,9},{2,18},{10... | collective-permute-start | bytes 196616 | tf_op jit(solution)/shard_map/ppermute | solution.py:359
  62.9 2.0 %collective-permute-start.3 = (bf16[128,256]{1,0:T(8,128)(2,1)S(1)}, bf16[128,256]{1,0:T(8,128)(2,1)S(1)}, u32[]{:S(2)}, u32[]{:S(2)}) collective-permute-start(bf16[128,256]{1,0:T(8,128)(2,1)S(1)} %get-tuple-element.46), channel_id=1, source_target_pairs={{0,24},{8,0},{16,8},{24,16},{1,25},{9,1},{17,9},{25,17},{2,26},{10... | collective-permute-start | bytes 196616 | tf_op jit(solution)/shard_map/ppermute | solution.py:359
  64.9 3.3 %collective-permute-done.3.refs_3_ = bf16[128,256]{1,0:T(8,128)(2,1)S(1)} collective-permute-done((bf16[128,256]{1,0:T(8,128)(2,1)S(1)}, bf16[128,256]{1,0:T(8,128)(2,1)S(1)}, u32[]{:S(2)}, u32[]{:S(2)}) %collective-permute-start.3) | collective-permute-done | bytes 65568 | tf_op jit(solution)/shard_map/ppermute | solution.py:359
  68.9 6.3 %collective-permute-start.4 = (bf16[4,336,512]{2,1,0:T(8,128)(2,1)S(1)}, bf16[4,336,512]{2,1,0:T(8,128)(2,1)S(1)}, u32[]{:S(2)}, u32[]{:S(2)}) collective-permute-start(bf16[4,336,512]{2,1,0:T(8,128)(2,1)S(1)} %all-to-all-done.1.refs_0_), channel_id=1, source_target_pairs={{0,4},{4,0},{1,5},{5,1},{2,6},{6,2},{3,7},{7,3},{8,12},{12,8},{9,1... | collective-permute-start | bytes 4128776 | tf_op jit(solution)/shard_map/ppermute | solution.py:359
  75.2 2.7 %collective-permute-done.4.refs_0_.refs_1_ = bf16[4,336,512]{2,1,0:T(8,128)(2,1)S(1)} collective-permute-done((bf16[4,336,512]{2,1,0:T(8,128)(2,1)S(1)}, bf16[4,336,512]{2,1,0:T(8,128)(2,1)S(1)}, u32[]{:S(2)}, u32[]{:S(2)}) %collective-permute-start.4) | collective-permute-done | bytes 1376288 | tf_op jit(solution)/shard_map/ppermute | solution.py:359
  78.0 5.1 %shard_map.150 = (bf16[4,336,256]{2,1,0:T(8,128)(2,1)}, bf16[320,352]{1,0:T(8,128)(2,1)}, bf16[320,352]{1,0:T(8,128)(2,1)}, bf16[320,352]{1,0:T(8,128)(2,1)}) custom-call(bf16[4,336,512]{2,1,0:T(8,128)(2,1)S(1)} %collective-permute-done.4.refs_0_.refs_1_, bf16[352,1024]{1,0:T(8,128)(2,1)} %bitcast.35, bf16[352,1024]{1,0:T(8,128)(2,1)} %bitcast.37, ...), custom_call_target="tpu_custom_call" | custom-call | flops 1150000000 | bytes 1000000 | tf_op jit(solution)/shard_map/pallas_call | solution.py:50
  83.1 2.3 %collective-permute-start.5 = (bf16[4,336,256]{2,1,0:T(8,128)(2,1)}, bf16[4,336,256]{2,1,0:T(8,128)(2,1)S(1)}, u32[]{:S(2)}, u32[]{:S(2)}) collective-permute-start(bf16[4,336,256]{2,1,0:T(8,128)(2,1)} %get-tuple-element.49), channel_id=1, source_target_pairs={{0,4},{4,0},{1,5},{5,1},{2,6},{6,2},{3,7},{7,3},{8,12},{12,8},{9,1... | collective-permute-start | bytes 2064392 | tf_op jit(solution)/shard_map/ppermute | solution.py:359
  85.4 5.2 %all-to-all-start.2 = ((bf16[16,16,256]{2,1,0:T(8,128)(2,1)}), bf16[16,16,256]{2,1,0:T(8,128)(2,1)S(1)}, u32[]{:S(2)}, u32[]{:S(2)}) async-start(bf16[16,16,256]{2,1,0:T(8,128)(2,1)} %bitcast.12), calls=%async_computation.2 | async-start | bytes 262144 | tf_op jit(solution)/shard_map/all_to_all | solution.py:354
  90.6 4.0 %shard_map.149 = (bf16[4,336,256]{2,1,0:T(8,128)(2,1)S(1)}, bf16[320,352]{1,0:T(8,128)(2,1)}, bf16[320,352]{1,0:T(8,128)(2,1)}, bf16[320,352]{1,0:T(8,128)(2,1)}) custom-call(bf16[4,336,512]{2,1,0:T(8,128)(2,1)S(1)} %all-to-all-done.1.refs_0_, bf16[352,1024]{1,0:T(8,128)(2,1)} %bitcast.36, bf16[352,1024]{1,0:T(8,128)(2,1)} %bitcast.38, ...), custom_call_target="tpu_custom_call" | custom-call | flops 1150000000 | bytes 1000000 | tf_op jit(solution)/shard_map/pallas_call | solution.py:50
  94.6 8.1 %all-to-all-done.2 = bf16[16,16,256]{2,1,0:T(8,128)(2,1)S(1)} async-done(((bf16[16,16,256]{2,1,0:T(8,128)(2,1)}), bf16[16,16,256]{2,1,0:T(8,128)(2,1)S(1)}, u32[]{:S(2)}, u32[]{:S(2)}) %all-to-all-start.2) | async-done | bytes 131104 | tf_op jit(solution)/shard_map/all_to_all | solution.py:354
  103.7 3.5 %all-to-all-start.3 = ((bf16[4,336,256]{2,1,0:T(8,128)(2,1)}), bf16[4,336,256]{2,1,0:T(8,128)(2,1)S(1)}, u32[]{:S(2)}, u32[]{:S(2)}) async-start(bf16[4,336,256]{2,1,0:T(8,128)(2,1)} %shard_map.151.refs_2_), calls=%async_computation.3 | async-start | bytes 1376256 | tf_op jit(solution)/shard_map/all_to_all | solution.py:354
  107.9 4.6 %collective-permute-start.6 = (f32[8,128]{1,0:T(8,128)S(1)}, f32[8,128]{1,0:T(8,128)S(1)}, u32[]{:S(2)}, u32[]{:S(2)}) collective-permute-start(f32[8,128]{1,0:T(8,128)S(1)} %get-tuple-element.53.refs_0_), channel_id=1, source_target_pairs={{0,4},{4,0},{1,5},{5,1},{2,6},{6,2},{3,7},{7,3},{8,12},{12,8},{9,1... | collective-permute-start | bytes 12296 | tf_op jit(solution)/shard_map/ppermute | solution.py:359
  113.4 4.8 %collective-permute-start.9 = (f32[8,128]{1,0:T(8,128)S(1)}, f32[8,128]{1,0:T(8,128)S(1)}, u32[]{:S(2)}, u32[]{:S(2)}) collective-permute-start(f32[8,128]{1,0:T(8,128)S(1)} %shard_map.153.refs_1_), channel_id=1, source_target_pairs={{0,3},{1,0},{2,1},{3,2},{4,7},{5,4},{6,5},{7,6},{8,11},{9,8},{10,9... | collective-permute-start | bytes 12296 | tf_op jit(solution)/shard_map/ppermute | solution.py:359
  118.2 2.5 %collective-permute-start.8 = (f32[8,128]{1,0:T(8,128)S(1)}, f32[8,128]{1,0:T(8,128)S(1)}, u32[]{:S(2)}, u32[]{:S(2)}) collective-permute-start(f32[8,128]{1,0:T(8,128)S(1)} %shard_map.153.refs_1_), channel_id=1, source_target_pairs={{0,2},{1,3},{2,0},{3,1},{4,6},{5,7},{6,4},{7,5},{8,10},{9,11},{10,... | collective-permute-start | bytes 12296 | tf_op jit(solution)/shard_map/ppermute | solution.py:359
  120.7 2.5 %collective-permute-start.7 = (f32[8,128]{1,0:T(8,128)S(1)}, f32[8,128]{1,0:T(8,128)S(1)}, u32[]{:S(2)}, u32[]{:S(2)}) collective-permute-start(f32[8,128]{1,0:T(8,128)S(1)} %shard_map.153.refs_1_), channel_id=1, source_target_pairs={{0,1},{1,2},{2,3},{3,0},{4,5},{5,6},{6,7},{7,4},{8,9},{9,10},{10,1... | collective-permute-start | bytes 12296 | tf_op jit(solution)/shard_map/ppermute | solution.py:359
  124.0 2.2 %collective-permute-done.7.refs_2_ = f32[8,128]{1,0:T(8,128)S(1)} collective-permute-done((f32[8,128]{1,0:T(8,128)S(1)}, f32[8,128]{1,0:T(8,128)S(1)}, u32[]{:S(2)}, u32[]{:S(2)}) %collective-permute-start.7) | collective-permute-done | bytes 4128 | tf_op jit(solution)/shard_map/ppermute | solution.py:359
  126.2 1.4 shard_map.154.refs_8_
  127.6 7.4 %all-to-all-start.4 = ((bf16[64,8,256]{2,1,0:T(8,128)(2,1)}), bf16[64,8,256]{2,1,0:T(8,128)(2,1)S(1)}, u32[]{:S(2)}, u32[]{:S(2)}) async-start(bf16[64,8,256]{2,1,0:T(8,128)(2,1)} %bitcast.15), calls=%async_computation.4 | async-start | bytes 524288 | tf_op jit(solution)/shard_map/all_to_all | solution.py:354
  135.0 10.1 %all_gather.7.refs_2_ = bf16[512,256]{1,0:T(8,128)(2,1)S(1)} all-gather(bf16[128,256]{1,0:T(8,128)(2,1)S(1)} %get-tuple-element.56), channel_id=1, replica_groups=mesh['ep_0'=16,'ep_1'=4,'ep_2'=2,'tp'=4] {'ep_1'}, dimensions={0}, use_global_device_ids=true | all-gather | bytes 327680 | tf_op jit(solution)/shard_map/all_gather | solution.py:459
  145.1 7.3 %collective-permute-start.10 = (bf16[512,256]{1,0:T(8,128)(2,1)S(1)}, bf16[512,256]{1,0:T(8,128)(2,1)S(1)}, u32[]{:S(2)}, u32[]{:S(2)}) collective-permute-start(bf16[512,256]{1,0:T(8,128)(2,1)S(1)} %all_gather.7.refs_2_), channel_id=1, source_target_pairs={{0,4},{4,0},{1,5},{5,1},{2,6},{6,2},{3,7},{7,3},{8,12},{12,8},{9,1... | collective-permute-start | bytes 786440 | tf_op jit(solution)/shard_map/ppermute | solution.py:359
  153.9 1.3 copy-done.2
  155.2 4.4 %shard_map.156 = (bf16[352,1024]{1,0:T(8,128)(2,1)}, bf16[352,1024]{1,0:T(8,128)(2,1)}, bf16[352,1024]{1,0:T(8,128)(2,1)}, f32[8,128]{1,0:T(8,128)S(1)}) custom-call(bf16[4,336,512]{2,1,0:T(8,128)(2,1)S(1)} %all-to-all-done.1.refs_0_, bf16[4,336,512]{2,1,0:T(8,128)(2,1)S(1)} %copy-done.2, bf16[320,352]{1,0:T(8,128)(2,1)} %get-tuple-element.57.refs_2_, ...), custom_call_target="tpu_custom_call" | custom-call | flops 1400000000 | bytes 1000000 | tf_op jit(solution)/shard_map/pallas_call | solution.py:50
  (25 shorter events, 7.3 us)
Async XLA Ops:
  3.8 44.0 %all-to-all-start = ((bf16[64,8,384]{2,1,0:T(8,128)(2,1)}), bf16[64,8,384]{2,1,0:T(8,128)(2,1)S(1)}, u32[]{:S(2)}, u32[]{:S(2)}) async-start(bf16[64,8,384]{2,1,0:T(8,128)(2,1)} %bitcast.2), calls=%async_computation | async-start | bytes 786432 | tf_op jit(solution)/shard_map/all_to_all | solution.py:354
  34.8 6.1 %collective-permute-start = (bf16[512,256]{1,0:T(8,128)(2,1)S(1)}, bf16[512,256]{1,0:T(8,128)(2,1)S(1)}, u32[]{:S(2)}, u32[]{:S(2)}) collective-permute-start(bf16[512,256]{1,0:T(8,128)(2,1)S(1)} %get-tuple-element.42), channel_id=1, source_target_pairs={{0,4},{4,0},{1,5},{5,1},{2,6},{6,2},{3,7},{7,3},{8,12},{12,8},{9,1... | collective-permute-start | bytes 786440 | tf_op jit(solution)/shard_map/ppermute | solution.py:359
  49.4 18.8 %copy-start.3 = (bf16[256,8]{0,1:T(8,128)(2,1)S(1)}, bf16[256,8]{0,1:T(8,128)(2,1)}, u32[]{:S(2)}) copy-start(bf16[256,8]{0,1:T(8,128)(2,1)} %param.16) | copy-start | bytes 12292
  49.4 19.5 %all-to-all-start.1 = ((bf16[4,336,512]{2,1,0:T(8,128)(2,1)}), bf16[4,336,512]{2,1,0:T(8,128)(2,1)S(1)}, u32[]{:S(2)}, u32[]{:S(2)}) async-start(bf16[4,336,512]{2,1,0:T(8,128)(2,1)} %shard_map.147), calls=%async_computation.1 | async-start | bytes 2752512 | tf_op jit(solution)/shard_map/all_to_all | solution.py:354
  53.8 11.1 %collective-permute-start.1 = (bf16[128,256]{1,0:T(8,128)(2,1)S(1)}, bf16[128,256]{1,0:T(8,128)(2,1)S(1)}, u32[]{:S(2)}, u32[]{:S(2)}) collective-permute-start(bf16[128,256]{1,0:T(8,128)(2,1)S(1)} %get-tuple-element.44), channel_id=1, source_target_pairs={{0,8},{8,16},{16,24},{24,0},{1,9},{9,17},{17,25},{25,1},{2,10},{10... | collective-permute-start | bytes 196616 | tf_op jit(solution)/shard_map/ppermute | solution.py:359
  57.5 7.4 %collective-permute-start.2 = (bf16[128,256]{1,0:T(8,128)(2,1)S(1)}, bf16[128,256]{1,0:T(8,128)(2,1)S(1)}, u32[]{:S(2)}, u32[]{:S(2)}) collective-permute-start(bf16[128,256]{1,0:T(8,128)(2,1)S(1)} %get-tuple-element.45), channel_id=1, source_target_pairs={{0,16},{8,24},{16,0},{24,8},{1,17},{9,25},{17,1},{25,9},{2,18},{10... | collective-permute-start | bytes 196616 | tf_op jit(solution)/shard_map/ppermute | solution.py:359
  62.9 5.3 %collective-permute-start.3 = (bf16[128,256]{1,0:T(8,128)(2,1)S(1)}, bf16[128,256]{1,0:T(8,128)(2,1)S(1)}, u32[]{:S(2)}, u32[]{:S(2)}) collective-permute-start(bf16[128,256]{1,0:T(8,128)(2,1)S(1)} %get-tuple-element.46), channel_id=1, source_target_pairs={{0,24},{8,0},{16,8},{24,16},{1,25},{9,1},{17,9},{25,17},{2,26},{10... | collective-permute-start | bytes 196616 | tf_op jit(solution)/shard_map/ppermute | solution.py:359
  68.9 9.1 %collective-permute-start.4 = (bf16[4,336,512]{2,1,0:T(8,128)(2,1)S(1)}, bf16[4,336,512]{2,1,0:T(8,128)(2,1)S(1)}, u32[]{:S(2)}, u32[]{:S(2)}) collective-permute-start(bf16[4,336,512]{2,1,0:T(8,128)(2,1)S(1)} %all-to-all-done.1.refs_0_), channel_id=1, source_target_pairs={{0,4},{4,0},{1,5},{5,1},{2,6},{6,2},{3,7},{7,3},{8,12},{12,8},{9,1... | collective-permute-start | bytes 4128776 | tf_op jit(solution)/shard_map/ppermute | solution.py:359
  78.0 5.1 %copy-start.1 = (bf16[4,336,512]{2,1,0:T(8,128)(2,1)}, bf16[4,336,512]{2,1,0:T(8,128)(2,1)S(1)}, u32[]{:S(2)}) copy-start(bf16[4,336,512]{2,1,0:T(8,128)(2,1)S(1)} %collective-permute-done.4.refs_0_.refs_1_) | copy-start | bytes 4128772
  83.1 19.6 %collective-permute-start.5 = (bf16[4,336,256]{2,1,0:T(8,128)(2,1)}, bf16[4,336,256]{2,1,0:T(8,128)(2,1)S(1)}, u32[]{:S(2)}, u32[]{:S(2)}) collective-permute-start(bf16[4,336,256]{2,1,0:T(8,128)(2,1)} %get-tuple-element.49), channel_id=1, source_target_pairs={{0,4},{4,0},{1,5},{5,1},{2,6},{6,2},{3,7},{7,3},{8,12},{12,8},{9,1... | collective-permute-start | bytes 2064392 | tf_op jit(solution)/shard_map/ppermute | solution.py:359
  85.4 17.3 %all-to-all-start.2 = ((bf16[16,16,256]{2,1,0:T(8,128)(2,1)}), bf16[16,16,256]{2,1,0:T(8,128)(2,1)S(1)}, u32[]{:S(2)}, u32[]{:S(2)}) async-start(bf16[16,16,256]{2,1,0:T(8,128)(2,1)} %bitcast.12), calls=%async_computation.2 | async-start | bytes 262144 | tf_op jit(solution)/shard_map/all_to_all | solution.py:354
  102.7 4.5 %copy-start = (f32[1024]{0:T(1024)S(1)}, f32[1024]{0:T(1024)}, u32[]{:S(2)}) copy-start(f32[1024]{0:T(1024)} %param.17) | copy-start | bytes 12292
  103.7 22.5 %all-to-all-start.3 = ((bf16[4,336,256]{2,1,0:T(8,128)(2,1)}), bf16[4,336,256]{2,1,0:T(8,128)(2,1)S(1)}, u32[]{:S(2)}, u32[]{:S(2)}) async-start(bf16[4,336,256]{2,1,0:T(8,128)(2,1)} %shard_map.151.refs_2_), calls=%async_computation.3 | async-start | bytes 1376256 | tf_op jit(solution)/shard_map/all_to_all | solution.py:354
  107.9 5.4 %collective-permute-start.6 = (f32[8,128]{1,0:T(8,128)S(1)}, f32[8,128]{1,0:T(8,128)S(1)}, u32[]{:S(2)}, u32[]{:S(2)}) collective-permute-start(f32[8,128]{1,0:T(8,128)S(1)} %get-tuple-element.53.refs_0_), channel_id=1, source_target_pairs={{0,4},{4,0},{1,5},{5,1},{2,6},{6,2},{3,7},{7,3},{8,12},{12,8},{9,1... | collective-permute-start | bytes 12296 | tf_op jit(solution)/shard_map/ppermute | solution.py:359
  113.4 9.8 %collective-permute-start.9 = (f32[8,128]{1,0:T(8,128)S(1)}, f32[8,128]{1,0:T(8,128)S(1)}, u32[]{:S(2)}, u32[]{:S(2)}) collective-permute-start(f32[8,128]{1,0:T(8,128)S(1)} %shard_map.153.refs_1_), channel_id=1, source_target_pairs={{0,3},{1,0},{2,1},{3,2},{4,7},{5,4},{6,5},{7,6},{8,11},{9,8},{10,9... | collective-permute-start | bytes 12296 | tf_op jit(solution)/shard_map/ppermute | solution.py:359
  118.2 5.9 %collective-permute-start.8 = (f32[8,128]{1,0:T(8,128)S(1)}, f32[8,128]{1,0:T(8,128)S(1)}, u32[]{:S(2)}, u32[]{:S(2)}) collective-permute-start(f32[8,128]{1,0:T(8,128)S(1)} %shard_map.153.refs_1_), channel_id=1, source_target_pairs={{0,2},{1,3},{2,0},{3,1},{4,6},{5,7},{6,4},{7,5},{8,10},{9,11},{10,... | collective-permute-start | bytes 12296 | tf_op jit(solution)/shard_map/ppermute | solution.py:359
  120.7 5.6 %collective-permute-start.7 = (f32[8,128]{1,0:T(8,128)S(1)}, f32[8,128]{1,0:T(8,128)S(1)}, u32[]{:S(2)}, u32[]{:S(2)}) collective-permute-start(f32[8,128]{1,0:T(8,128)S(1)} %shard_map.153.refs_1_), channel_id=1, source_target_pairs={{0,1},{1,2},{2,3},{3,0},{4,5},{5,6},{6,7},{7,4},{8,9},{9,10},{10,1... | collective-permute-start | bytes 12296 | tf_op jit(solution)/shard_map/ppermute | solution.py:359
  127.6 32.0 %all-to-all-start.4 = ((bf16[64,8,256]{2,1,0:T(8,128)(2,1)}), bf16[64,8,256]{2,1,0:T(8,128)(2,1)S(1)}, u32[]{:S(2)}, u32[]{:S(2)}) async-start(bf16[64,8,256]{2,1,0:T(8,128)(2,1)} %bitcast.15), calls=%async_computation.4 | async-start | bytes 524288 | tf_op jit(solution)/shard_map/all_to_all | solution.py:354
  145.1 8.4 %collective-permute-start.10 = (bf16[512,256]{1,0:T(8,128)(2,1)S(1)}, bf16[512,256]{1,0:T(8,128)(2,1)S(1)}, u32[]{:S(2)}, u32[]{:S(2)}) collective-permute-start(bf16[512,256]{1,0:T(8,128)(2,1)S(1)} %all_gather.7.refs_2_), channel_id=1, source_target_pairs={{0,4},{4,0},{1,5},{5,1},{2,6},{6,2},{3,7},{7,3},{8,12},{12,8},{9,1... | collective-permute-start | bytes 786440 | tf_op jit(solution)/shard_map/ppermute | solution.py:359
  153.9 1.3 copy-start.2

commit v3 on v2

--- a/solution.py
+++ b/solution.py
@@ -152,23 +152,12 @@
 
 
 def expert_kernel(
-    in_hbm, wg_hbm, wu_hbm, wd_hbm, z_ref, dg_out, du_out, wt_out,
-    in_ref, wg_ref, wu_ref, wd_ref, dg_ref, du_ref, wt_ref, sems,
+    in_ref, wg_ref, wu_ref, wd_ref, z_ref, dg_out, du_out, wt_out, dg_ref, du_ref, wt_ref, sems
 ):
-    inward = [
+    outward = [
         pltpu.make_async_copy(src, dst, sems.at[n])
-        for n, (src, dst) in enumerate(
-            ((in_hbm, in_ref), (wg_hbm, wg_ref), (wu_hbm, wu_ref), (wd_hbm, wd_ref))
-        )
-    ]
-    outward = [
-        pltpu.make_async_copy(src, dst, sems.at[4 + n])
         for n, (src, dst) in enumerate(((dg_ref, dg_out), (du_ref, du_out), (wt_ref, wt_out)))
     ]
-    for copy in inward:
-        copy.start()
-    inward[0].wait()
-    inward[1].wait()
 
     def summed(lo, w_ref):
         return sum(
@@ -177,9 +166,7 @@
         )
 
     pre_gate = summed(0, wg_ref)
-    inward[2].wait()
     pre_up = summed(0, wu_ref)
-    inward[3].wait()
     projected = summed(256, wd_ref)
     w_row = in_ref[0, ROWS : ROWS + EXTRA, 0:ROWS].astype(F32)[0:1, :]
     eye = iota((ROWS, ROWS), 0) == iota((ROWS, ROWS), 1)
@@ -212,7 +199,18 @@
         copy.wait()
 
 
-def return_kernel(in_ref, m0_ref, m1_ref, m2_ref, m3_ref, out_ref):
+def load_kernel(*refs):
+    count = (len(refs) - 1) // 2
+    copies = [
+        pltpu.make_async_copy(refs[n], refs[count + n], refs[-1].at[n]) for n in range(count)
+    ]
+    for copy in copies:
+        copy.start()
+    for copy in copies:
+        copy.wait()
+
+
+def return_kernel(in_ref, out_ref):
     total = sum(in_ref[t].astype(F32) for t in range(TP))
     msgs = EXPERTS * 8
     rows = total[0:ROWS].astype(BF16)
@@ -232,15 +230,7 @@
     b_col = iota((512, 256), 1)
     out = out + dot(jnp.where(mine, hi, 0.0).astype(BF16), onehot(b_row // 64 == b_col))
     out = out + dot(jnp.where(mine, lo, 0.0).astype(BF16), onehot(b_row // 64 == b_col - 128))
-    came = [m_ref[0:1, :] for m_ref in (m0_ref, m1_ref, m2_ref, m3_ref)]
-    here = lax.axis_index("tp")
-    mix = jnp.zeros((1, 128), F32)
-    for t in range(TP):
-        back = lax.rem(here - t + TP, TP)
-        pick = came[3]
-        for n in range(3):
-            pick = jnp.where(back == n, came[n], pick)
-        mix = mix + pick
+    mix = total[ROWS + 2 : ROWS + 3, 0:128] + total[ROWS + 3 : ROWS + 4, 0:128]
     mix_hi = mix.astype(BF16).astype(F32)
     mix_row = jnp.concatenate([mix_hi, mix - mix_hi], axis=1)
     out_sub = iota((msgs, 256), 0) % 8
@@ -338,12 +328,25 @@
     out_ref[...] = dot(scaled, weight)
 
 
-def add_kernel(a_ref, b_ref, out_ref):
-    out_ref[...] = (a_ref[...].astype(F32) + b_ref[...].astype(F32)).astype(BF16)
-
-
-def share_kernel(a_ref, b_ref, out_ref):
-    out_ref[...] = a_ref[...] + b_ref[...]
+def add_kernel(a_ref, b_ref, m0_ref, m1_ref, out_ref):
+    def parts(value):
+        hi = value.astype(BF16).astype(F32)
+        return hi, value - hi
+
+    mix = parts(jnp.concatenate([m0_ref[0:1, :] + m1_ref[0:1, :], jnp.zeros((1, 128), F32)], axis=1))
+    sub = iota((8, 256), 0)
+    extra = []
+    both = a_ref[0, ROWS : ROWS + EXTRA, :].astype(F32) + b_ref[0, ROWS : ROWS + EXTRA, :].astype(F32)
+    for at in (0, 8):
+        block = jnp.zeros((8, 256), F32)
+        for n, row in enumerate(parts(both[at : at + 1] + both[at + 1 : at + 2]) + mix):
+            block = jnp.where(sub == n, row, block)
+        extra.append(block)
+    extra = jnp.concatenate(extra, axis=0).astype(BF16)
+    for t in range(TP):
+        total = a_ref[t, 0:ROWS, :].astype(F32) + b_ref[t, 0:ROWS, :].astype(F32)
+        out_ref[t, 0:ROWS, :] = total.astype(BF16)
+        out_ref[t, ROWS : ROWS + EXTRA, :] = extra
 
 
 def in_place(*arrays):
@@ -416,17 +419,22 @@
     hbm_spec = pl.BlockSpec(memory_space=pltpu.HBM)
     vmem_spec = pl.BlockSpec(memory_space=pltpu.VMEM)
     expert = dict(
-        hbm=4,
         flops=1_150_000_000,
         out_specs=(vmem_spec,) + (hbm_spec,) * 3,
-        scratch=(pltpu.VMEM((TP, ROWS + EXTRA, 512), BF16),)
-        + (pltpu.VMEM((352, 1024), BF16),) * 3
-        + (pltpu.VMEM((ROWS, 352), BF16),) * 3
-        + (pltpu.SemaphoreType.DMA((7,)),),
-    )
-    z_own, *act_own = call(expert_kernel, outs, own, wg, wu, wd, **expert)
+        scratch=(pltpu.VMEM((ROWS, 352), BF16),) * 3 + (pltpu.SemaphoreType.DMA((3,)),),
+    )
+    weights = call(
+        load_kernel,
+        (struct(352, 1024),) * 3,
+        wg,
+        wu,
+        wd,
+        hbm=3,
+        scratch=(pltpu.SemaphoreType.DMA((3,)),),
+    )
+    z_own, *act_own = call(expert_kernel, outs, own, *weights, **expert)
     z_got = swap(both.reshape(16, 16, 256), "ep_0").reshape(256, 256)
-    z_other, *act_other = call(expert_kernel, outs, other, wg, wu, wd, **expert)
+    z_other, *act_other = call(expert_kernel, outs, other, *weights, **expert)
     z_back = shift(z_other, "ep_2", 1)
     z_back, z_got = lax.optimization_barrier((z_back, z_got))
     dense_grad, share, dense_w = call(
@@ -436,13 +444,11 @@
         gate_row,
         dense_t,
     )
-    z_sum = call(add_kernel, outs[0], z_own, z_back)
+    z_sum = call(add_kernel, outs[0], z_own, z_back, share, shift(share, "ep_2", 1))
     z_all = swap(z_sum, "tp")
-    share = call(
-        share_kernel, struct(8, 128, dtype=F32), share, shift(share, "ep_2", 1), after=(z_sum,)
-    )
-    shares = [share] + [shift(share, "tp", by) for by in (1, 2, 3)]
-    back_ready = call(return_kernel, struct(512, 256), z_all, *shares)
+    dense_w = lax.all_gather(dense_w, "ep_1", axis=0, tiled=True)
+    z_all, dense_w = lax.optimization_barrier((z_all, dense_w))
+    back_ready = call(return_kernel, struct(512, 256), z_all)
     gate_grad, up_grad, down_grad, grads_done = call(
         grads_kernel,
         (struct(352, 1024),) * 3 + (struct(8, 128, dtype=F32),),
@@ -456,7 +462,6 @@
     )
     back = swap(back_ready.reshape(64, 8, 256), CHIPS).reshape(512, 256)
 
-    dense_w = lax.all_gather(dense_w, "ep_1", axis=0, tiled=True)
     dense_dx = call(
         dense_kernel,
         struct(128, 256, dtype=F32),

time: 162 us -> 156 us (0.963)
  the two profiles are of different devices: /device:TPU:1 before, /device:TPU:8 now
where the time goes in v3:
time: 156 us; the launch traced here: 155 us
  starting transfers between devices  56.3 us (36%)
  blocking collectives  44.6 us (29%)
  waiting for transfers between devices  29.3 us (19%)
  Pallas kernels  21.7 us (14%)
  local copies, waits for them, and re-layouts  2.01 us (1%)
    all_to_all x4, starting transfers between devices, swap(): return lax.all_to_all(value, axes, split_axis=0, concat_axis=0, tiled=True)  35.3 us
    all_to_all x4, waiting for transfers between devices, swap(): return lax.all_to_all(value, axes, split_axis=0, concat_axis=0, tiled=True)  23.5 us
    pallas_call x14, Pallas kernels, call(): pl.pallas_call(body, out_shape=outs, in_specs=[in_hbm] * hbm + [whole] *...  21.7 us
    ppermute x8, starting transfers between devices, shift(): return lax.ppermute(value, axis, [(i, (i + by) % n) for i in range(n)])  21 us
    all_to_all x1, blocking collectives, swap(): return lax.all_to_all(value, axes, split_axis=0, concat_axis=0, tiled=True)  19.7 us
    all_gather x1, blocking collectives, local(): cot_all = lax.all_gather(cot_here, 'tp', axis=1, tiled=True)  12.5 us
    all_gather x1, blocking collectives, local(): dense_w = lax.all_gather(dense_w, 'ep_1', axis=0, tiled=True)  12.4 us
    ppermute x8, waiting for transfers between devices, shift(): return lax.ppermute(value, axis, [(i, (i + by) % n) for i in range(n)])  5.79 us
  transfers between devices with their start and end apart: 12, of which 6 were waited for; matrix products, arithmetic and copies ran while one was open for 0% of the time, Pallas kernels for 7%

profile of v3, /device:TPU:8, one launch (start us, length us, event | category | flops | bytes accessed | tf_op | source)
XLA Modules:
  0.0 154.8 jit_solution(14420768660440920733)
XLA Ops:
  0.6 3.1 %shard_map.144 = (bf16[512,384]{1,0:T(8,128)(2,1)}, f32[8,128]{1,0:T(8,128)S(1)}, f32[128,128]{1,0:T(8,128)S(1)}, bf16[128,256]{1,0:T(8,128)(2,1)S(1)}) custom-call(bf16[128,256]{1,0:T(8,128)(2,1)} %refs_1_.3, bf16[128,256]{1,0:T(8,128)(2,1)} %refs_1_.2, s32[2,128]{1,0:T(2,128)} %bitcast.39, bf16[2,128]{1,0:T(2,128)(2,1)} %bitcast.40), custom_call_target="tpu_custom_call" | custom-call | flops 200000000 | bytes 1000000 | tf_op jit(solution)/shard_map/pallas_call | solution.py:50
  3.8 18.6 %all-to-all-start = ((bf16[64,8,384]{2,1,0:T(8,128)(2,1)}), bf16[64,8,384]{2,1,0:T(8,128)(2,1)S(1)}, u32[]{:S(2)}, u32[]{:S(2)}) async-start(bf16[64,8,384]{2,1,0:T(8,128)(2,1)} %bitcast.2), calls=%async_computation | async-start | bytes 786432 | tf_op jit(solution)/shard_map/all_to_all | solution.py:357
  22.4 12.5 %all_gather.6.refs_0_ = bf16[128,1024]{1,0:T(8,128)(2,1)S(1)} all-gather(bf16[128,256]{1,0:T(8,128)(2,1)S(1)} %get-tuple-element.45), channel_id=1, replica_groups=mesh['ep_0'=16,'ep_1'=4,'ep_2'=2,'tp'=4] {'tp'}, dimensions={1}, use_global_device_ids=true | all-gather | bytes 327680 | tf_op jit(solution)/shard_map/all_gather | solution.py:394
  34.9 1.2 shard_map.145
  36.1 1.9 %collective-permute-start = (bf16[512,256]{1,0:T(8,128)(2,1)S(1)}, bf16[512,256]{1,0:T(8,128)(2,1)S(1)}, u32[]{:S(2)}, u32[]{:S(2)}) collective-permute-start(bf16[512,256]{1,0:T(8,128)(2,1)S(1)} %get-tuple-element.47), channel_id=1, source_target_pairs={{0,4},{4,0},{1,5},{5,1},{2,6},{6,2},{3,7},{7,3},{8,12},{12,8},{9,1... | collective-permute-start | bytes 786440 | tf_op jit(solution)/shard_map/ppermute | solution.py:362
  38.0 1.5 collective-permute-done.refs_1_
  39.6 10.0 %all-to-all-done = bf16[64,8,384]{2,1,0:T(8,128)(2,1)S(1)} async-done(((bf16[64,8,384]{2,1,0:T(8,128)(2,1)}), bf16[64,8,384]{2,1,0:T(8,128)(2,1)S(1)}, u32[]{:S(2)}, u32[]{:S(2)}) %all-to-all-start) | async-done | bytes 393248 | tf_op jit(solution)/shard_map/all_to_all | solution.py:357
  49.6 1.7 %shard_map.147 = bf16[4,336,512]{2,1,0:T(8,128)(2,1)} custom-call(bf16[512,384]{1,0:T(8,128)(2,1)S(1)} %bitcast.27, f32[128,256]{1,0:T(8,128)S(1)} %get-tuple-element.48.refs_1_.refs_0_), custom_call_target="tpu_custom_call" | custom-call | flops 200000000 | bytes 1000000 | tf_op jit(solution)/shard_map/pallas_call | solution.py:50
  51.3 5.0 %all-to-all-start.1 = ((bf16[4,336,512]{2,1,0:T(8,128)(2,1)}), bf16[4,336,512]{2,1,0:T(8,128)(2,1)S(1)}, u32[]{:S(2)}, u32[]{:S(2)}) async-start(bf16[4,336,512]{2,1,0:T(8,128)(2,1)} %shard_map.147), calls=%async_computation.1 | async-start | bytes 2752512 | tf_op jit(solution)/shard_map/all_to_all | solution.py:357
  56.3 3.3 %collective-permute-start.1 = (bf16[128,256]{1,0:T(8,128)(2,1)S(1)}, bf16[128,256]{1,0:T(8,128)(2,1)S(1)}, u32[]{:S(2)}, u32[]{:S(2)}) collective-permute-start(bf16[128,256]{1,0:T(8,128)(2,1)S(1)} %get-tuple-element.49), channel_id=1, source_target_pairs={{0,8},{8,16},{16,24},{24,0},{1,9},{9,17},{17,25},{25,1},{2,10},{10... | collective-permute-start | bytes 196616 | tf_op jit(solution)/shard_map/ppermute | solution.py:362
  59.6 4.6 %collective-permute-start.2 = (bf16[128,256]{1,0:T(8,128)(2,1)S(1)}, bf16[128,256]{1,0:T(8,128)(2,1)S(1)}, u32[]{:S(2)}, u32[]{:S(2)}) collective-permute-start(bf16[128,256]{1,0:T(8,128)(2,1)S(1)} %get-tuple-element.50), channel_id=1, source_target_pairs={{0,16},{8,24},{16,0},{24,8},{1,17},{9,25},{17,1},{25,9},{2,18},{10... | collective-permute-start | bytes 196616 | tf_op jit(solution)/shard_map/ppermute | solution.py:362
  64.2 3.4 %collective-permute-start.3 = (bf16[128,256]{1,0:T(8,128)(2,1)S(1)}, bf16[128,256]{1,0:T(8,128)(2,1)S(1)}, u32[]{:S(2)}, u32[]{:S(2)}) collective-permute-start(bf16[128,256]{1,0:T(8,128)(2,1)S(1)} %get-tuple-element.51), channel_id=1, source_target_pairs={{0,24},{8,0},{16,8},{24,16},{1,25},{9,1},{17,9},{25,17},{2,26},{10... | collective-permute-start | bytes 196616 | tf_op jit(solution)/shard_map/ppermute | solution.py:362
  67.6 2.8 %collective-permute-done.3.refs_3_ = bf16[128,256]{1,0:T(8,128)(2,1)S(1)} collective-permute-done((bf16[128,256]{1,0:T(8,128)(2,1)S(1)}, bf16[128,256]{1,0:T(8,128)(2,1)S(1)}, u32[]{:S(2)}, u32[]{:S(2)}) %collective-permute-start.3) | collective-permute-done | bytes 65568 | tf_op jit(solution)/shard_map/ppermute | solution.py:362
  70.8 1.9 %collective-permute-start.4 = (bf16[4,336,512]{2,1,0:T(8,128)(2,1)S(1)}, bf16[4,336,512]{2,1,0:T(8,128)(2,1)S(1)}, u32[]{:S(2)}, u32[]{:S(2)}) collective-permute-start(bf16[4,336,512]{2,1,0:T(8,128)(2,1)S(1)} %all-to-all-done.1.refs_0_), channel_id=1, source_target_pairs={{0,4},{4,0},{1,5},{5,1},{2,6},{6,2},{3,7},{7,3},{8,12},{12,8},{9,1... | collective-permute-start | bytes 4128776 | tf_op jit(solution)/shard_map/ppermute | solution.py:362
  72.7 1.6 %shard_map.149 = (bf16[352,1024]{1,0:T(8,128)(2,1)S(1)}, bf16[352,1024]{1,0:T(8,128)(2,1)S(1)}, bf16[352,1024]{1,0:T(8,128)(2,1)S(1)}) custom-call(bf16[352,1024]{1,0:T(8,128)(2,1)} %bitcast.36, bf16[352,1024]{1,0:T(8,128)(2,1)} %bitcast.37, bf16[352,1024]{1,0:T(8,128)(2,1)} %bitcast.38), custom_call_target="tpu_custom_call" | custom-call | flops 200000000 | bytes 1000000 | tf_op jit(solution)/shard_map/pallas_call | solution.py:50
  74.3 1.5 collective-permute-done.4.refs_0_.refs_1_
  75.8 2.6 %shard_map.151 = (bf16[4,336,256]{2,1,0:T(8,128)(2,1)S(1)}, bf16[320,352]{1,0:T(8,128)(2,1)}, bf16[320,352]{1,0:T(8,128)(2,1)}, bf16[320,352]{1,0:T(8,128)(2,1)}) custom-call(bf16[4,336,512]{2,1,0:T(8,128)(2,1)S(1)} %collective-permute-done.4.refs_0_.refs_1_, bf16[352,1024]{1,0:T(8,128)(2,1)S(1)} %get-tuple-element.53.refs_1_, ...), custom_call_target="tpu_custom_call" | custom-call | flops 1150000000 | bytes 1000000 | tf_op jit(solution)/shard_map/pallas_call | solution.py:50
  78.5 2.0 %collective-permute-start.5 = (bf16[4,336,256]{2,1,0:T(8,128)(2,1)S(1)}, bf16[4,336,256]{2,1,0:T(8,128)(2,1)S(1)}, u32[]{:S(2)}, u32[]{:S(2)}) collective-permute-start(bf16[4,336,256]{2,1,0:T(8,128)(2,1)S(1)} %get-tuple-element.57), channel_id=1, source_target_pairs={{0,4},{4,0},{1,5},{5,1},{2,6},{6,2},{3,7},{7,3},{8,12},{12,8},{9,1... | collective-permute-start | bytes 2064392 | tf_op jit(solution)/shard_map/ppermute | solution.py:362
  80.5 19.7 %all_to_all.25 = bf16[16,16,256]{2,1,0:T(8,128)(2,1)S(1)} all-to-all(bf16[16,16,256]{2,1,0:T(8,128)(2,1)S(1)} %bitcast.29), channel_id=1, replica_groups=mesh['ep_0'=16,'ep_1'=4,'ep_2'=2,'tp'=4] {'ep_0'}, dimensions={0} | all-to-all | bytes 262144 | tf_op jit(solution)/shard_map/all_to_all | solution.py:357
  100.2 0.7 shard_map.152
  100.9 1.9 %collective-permute-start.6 = (f32[8,128]{1,0:T(8,128)S(1)}, f32[8,128]{1,0:T(8,128)S(1)}, u32[]{:S(2)}, u32[]{:S(2)}) collective-permute-start(f32[8,128]{1,0:T(8,128)S(1)} %get-tuple-element.61.refs_2_), channel_id=1, source_target_pairs={{0,4},{4,0},{1,5},{5,1},{2,6},{6,2},{3,7},{7,3},{8,12},{12,8},{9,1... | collective-permute-start | bytes 12296 | tf_op jit(solution)/shard_map/ppermute | solution.py:362
  102.9 2.7 %shard_map.150 = (bf16[4,336,256]{2,1,0:T(8,128)(2,1)S(1)}, bf16[320,352]{1,0:T(8,128)(2,1)}, bf16[320,352]{1,0:T(8,128)(2,1)}, bf16[320,352]{1,0:T(8,128)(2,1)}) custom-call(bf16[4,336,512]{2,1,0:T(8,128)(2,1)S(1)} %all-to-all-done.1.refs_0_, bf16[352,1024]{1,0:T(8,128)(2,1)S(1)} %get-tuple-element.53.refs_1_, ...), custom_call_target="tpu_custom_call" | custom-call | flops 1150000000 | bytes 1000000 | tf_op jit(solution)/shard_map/pallas_call | solution.py:50
  105.5 1.0 shard_map.153
  106.5 4.9 %all-to-all-start.3 = ((bf16[4,336,256]{2,1,0:T(8,128)(2,1)}), bf16[4,336,256]{2,1,0:T(8,128)(2,1)S(1)}, u32[]{:S(2)}, u32[]{:S(2)}) async-start(bf16[4,336,256]{2,1,0:T(8,128)(2,1)} %shard_map.153), calls=%async_computation.3 | async-start | bytes 1376256 | tf_op jit(solution)/shard_map/all_to_all | solution.py:357
  111.5 12.4 %all_gather.7.refs_2_ = bf16[512,256]{1,0:T(8,128)(2,1)S(1)} all-gather(bf16[128,256]{1,0:T(8,128)(2,1)S(1)} %get-tuple-element.62), channel_id=1, replica_groups=mesh['ep_0'=16,'ep_1'=4,'ep_2'=2,'tp'=4] {'ep_1'}, dimensions={0}, use_global_device_ids=true | all-gather | bytes 327680 | tf_op jit(solution)/shard_map/all_gather | solution.py:449
  123.9 1.4 shard_map.154.refs_8_
  125.2 6.8 %all-to-all-start.4 = ((bf16[64,8,256]{2,1,0:T(8,128)(2,1)}), bf16[64,8,256]{2,1,0:T(8,128)(2,1)S(1)}, u32[]{:S(2)}, u32[]{:S(2)}) async-start(bf16[64,8,256]{2,1,0:T(8,128)(2,1)} %bitcast.13), calls=%async_computation.4 | async-start | bytes 524288 | tf_op jit(solution)/shard_map/all_to_all | solution.py:357
  132.0 1.9 %collective-permute-start.7 = (bf16[512,256]{1,0:T(8,128)(2,1)S(1)}, bf16[512,256]{1,0:T(8,128)(2,1)S(1)}, u32[]{:S(2)}, u32[]{:S(2)}) collective-permute-start(bf16[512,256]{1,0:T(8,128)(2,1)S(1)} %all_gather.7.refs_2_), channel_id=1, source_target_pairs={{0,4},{4,0},{1,5},{5,1},{2,6},{6,2},{3,7},{7,3},{8,12},{12,8},{9,1... | collective-permute-start | bytes 786440 | tf_op jit(solution)/shard_map/ppermute | solution.py:362
  134.0 1.3 copy-done.2
  135.3 4.4 %shard_map.156 = (bf16[352,1024]{1,0:T(8,128)(2,1)}, bf16[352,1024]{1,0:T(8,128)(2,1)}, bf16[352,1024]{1,0:T(8,128)(2,1)}, f32[8,128]{1,0:T(8,128)S(1)}) custom-call(bf16[4,336,512]{2,1,0:T(8,128)(2,1)S(1)} %all-to-all-done.1.refs_0_, bf16[4,336,512]{2,1,0:T(8,128)(2,1)S(1)} %copy-done.2, bf16[320,352]{1,0:T(8,128)(2,1)} %get-tuple-element.67.refs_2_, ...), custom_call_target="tpu_custom_call" | custom-call | flops 1400000000 | bytes 1000000 | tf_op jit(solution)/shard_map/pallas_call | solution.py:50
  140.0 13.1 %all-to-all-done.4 = bf16[64,8,256]{2,1,0:T(8,128)(2,1)S(1)} async-done(((bf16[64,8,256]{2,1,0:T(8,128)(2,1)}), bf16[64,8,256]{2,1,0:T(8,128)(2,1)S(1)}, u32[]{:S(2)}, u32[]{:S(2)}) %all-to-all-start.4) | async-done | bytes 262176 | tf_op jit(solution)/shard_map/all_to_all | solution.py:357
  153.1 1.0 shard_map.157
  (18 shorter events, 1.5 us)
Async XLA Ops:
  3.8 45.8 %all-to-all-start = ((bf16[64,8,384]{2,1,0:T(8,128)(2,1)}), bf16[64,8,384]{2,1,0:T(8,128)(2,1)S(1)}, u32[]{:S(2)}, u32[]{:S(2)}) async-start(bf16[64,8,384]{2,1,0:T(8,128)(2,1)} %bitcast.2), calls=%async_computation | async-start | bytes 786432 | tf_op jit(solution)/shard_map/all_to_all | solution.py:357
  36.1 3.4 %collective-permute-start = (bf16[512,256]{1,0:T(8,128)(2,1)S(1)}, bf16[512,256]{1,0:T(8,128)(2,1)S(1)}, u32[]{:S(2)}, u32[]{:S(2)}) collective-permute-start(bf16[512,256]{1,0:T(8,128)(2,1)S(1)} %get-tuple-element.47), channel_id=1, source_target_pairs={{0,4},{4,0},{1,5},{5,1},{2,6},{6,2},{3,7},{7,3},{8,12},{12,8},{9,1... | collective-permute-start | bytes 786440 | tf_op jit(solution)/shard_map/ppermute | solution.py:362
  51.3 19.1 %copy-start.3 = (bf16[256,8]{0,1:T(8,128)(2,1)S(1)}, bf16[256,8]{0,1:T(8,128)(2,1)}, u32[]{:S(2)}) copy-start(bf16[256,8]{0,1:T(8,128)(2,1)} %param.16) | copy-start | bytes 12292
  51.3 19.6 %all-to-all-start.1 = ((bf16[4,336,512]{2,1,0:T(8,128)(2,1)}), bf16[4,336,512]{2,1,0:T(8,128)(2,1)S(1)}, u32[]{:S(2)}, u32[]{:S(2)}) async-start(bf16[4,336,512]{2,1,0:T(8,128)(2,1)} %shard_map.147), calls=%async_computation.1 | async-start | bytes 2752512 | tf_op jit(solution)/shard_map/all_to_all | solution.py:357
  56.3 11.3 %collective-permute-start.1 = (bf16[128,256]{1,0:T(8,128)(2,1)S(1)}, bf16[128,256]{1,0:T(8,128)(2,1)S(1)}, u32[]{:S(2)}, u32[]{:S(2)}) collective-permute-start(bf16[128,256]{1,0:T(8,128)(2,1)S(1)} %get-tuple-element.49), channel_id=1, source_target_pairs={{0,8},{8,16},{16,24},{24,0},{1,9},{9,17},{17,25},{25,1},{2,10},{10... | collective-permute-start | bytes 196616 | tf_op jit(solution)/shard_map/ppermute | solution.py:362
  59.6 8.0 %collective-permute-start.2 = (bf16[128,256]{1,0:T(8,128)(2,1)S(1)}, bf16[128,256]{1,0:T(8,128)(2,1)S(1)}, u32[]{:S(2)}, u32[]{:S(2)}) collective-permute-start(bf16[128,256]{1,0:T(8,128)(2,1)S(1)} %get-tuple-element.50), channel_id=1, source_target_pairs={{0,16},{8,24},{16,0},{24,8},{1,17},{9,25},{17,1},{25,9},{2,18},{10... | collective-permute-start | bytes 196616 | tf_op jit(solution)/shard_map/ppermute | solution.py:362
  64.2 6.2 %collective-permute-start.3 = (bf16[128,256]{1,0:T(8,128)(2,1)S(1)}, bf16[128,256]{1,0:T(8,128)(2,1)S(1)}, u32[]{:S(2)}, u32[]{:S(2)}) collective-permute-start(bf16[128,256]{1,0:T(8,128)(2,1)S(1)} %get-tuple-element.51), channel_id=1, source_target_pairs={{0,24},{8,0},{16,8},{24,16},{1,25},{9,1},{17,9},{25,17},{2,26},{10... | collective-permute-start | bytes 196616 | tf_op jit(solution)/shard_map/ppermute | solution.py:362
  70.8 5.0 %collective-permute-start.4 = (bf16[4,336,512]{2,1,0:T(8,128)(2,1)S(1)}, bf16[4,336,512]{2,1,0:T(8,128)(2,1)S(1)}, u32[]{:S(2)}, u32[]{:S(2)}) collective-permute-start(bf16[4,336,512]{2,1,0:T(8,128)(2,1)S(1)} %all-to-all-done.1.refs_0_), channel_id=1, source_target_pairs={{0,4},{4,0},{1,5},{5,1},{2,6},{6,2},{3,7},{7,3},{8,12},{12,8},{9,1... | collective-permute-start | bytes 4128776 | tf_op jit(solution)/shard_map/ppermute | solution.py:362
  75.8 2.6 %copy-start.1 = (bf16[4,336,512]{2,1,0:T(8,128)(2,1)}, bf16[4,336,512]{2,1,0:T(8,128)(2,1)S(1)}, u32[]{:S(2)}) copy-start(bf16[4,336,512]{2,1,0:T(8,128)(2,1)S(1)} %collective-permute-done.4.refs_0_.refs_1_) | copy-start | bytes 4128772
  75.8 24.4 %copy-start = (f32[1024]{0:T(1024)S(1)}, f32[1024]{0:T(1024)}, u32[]{:S(2)}) copy-start(f32[1024]{0:T(1024)} %param.17) | copy-start | bytes 12292
  78.5 21.7 %collective-permute-start.5 = (bf16[4,336,256]{2,1,0:T(8,128)(2,1)S(1)}, bf16[4,336,256]{2,1,0:T(8,128)(2,1)S(1)}, u32[]{:S(2)}, u32[]{:S(2)}) collective-permute-start(bf16[4,336,256]{2,1,0:T(8,128)(2,1)S(1)} %get-tuple-element.57), channel_id=1, source_target_pairs={{0,4},{4,0},{1,5},{5,1},{2,6},{6,2},{3,7},{7,3},{8,12},{12,8},{9,1... | collective-permute-start | bytes 2064392 | tf_op jit(solution)/shard_map/ppermute | solution.py:362
  100.9 4.6 %collective-permute-start.6 = (f32[8,128]{1,0:T(8,128)S(1)}, f32[8,128]{1,0:T(8,128)S(1)}, u32[]{:S(2)}, u32[]{:S(2)}) collective-permute-start(f32[8,128]{1,0:T(8,128)S(1)} %get-tuple-element.61.refs_2_), channel_id=1, source_target_pairs={{0,4},{4,0},{1,5},{5,1},{2,6},{6,2},{3,7},{7,3},{8,12},{12,8},{9,1... | collective-permute-start | bytes 12296 | tf_op jit(solution)/shard_map/ppermute | solution.py:362
  106.5 17.3 %all-to-all-start.3 = ((bf16[4,336,256]{2,1,0:T(8,128)(2,1)}), bf16[4,336,256]{2,1,0:T(8,128)(2,1)S(1)}, u32[]{:S(2)}, u32[]{:S(2)}) async-start(bf16[4,336,256]{2,1,0:T(8,128)(2,1)} %shard_map.153), calls=%async_computation.3 | async-start | bytes 1376256 | tf_op jit(solution)/shard_map/all_to_all | solution.py:357
  125.2 27.9 %all-to-all-start.4 = ((bf16[64,8,256]{2,1,0:T(8,128)(2,1)}), bf16[64,8,256]{2,1,0:T(8,128)(2,1)S(1)}, u32[]{:S(2)}, u32[]{:S(2)}) async-start(bf16[64,8,256]{2,1,0:T(8,128)(2,1)} %bitcast.13), calls=%async_computation.4 | async-start | bytes 524288 | tf_op jit(solution)/shard_map/all_to_all | solution.py:357
  132.0 7.7 %collective-permute-start.7 = (bf16[512,256]{1,0:T(8,128)(2,1)S(1)}, bf16[512,256]{1,0:T(8,128)(2,1)S(1)}, u32[]{:S(2)}, u32[]{:S(2)}) collective-permute-start(bf16[512,256]{1,0:T(8,128)(2,1)S(1)} %all_gather.7.refs_2_), channel_id=1, source_target_pairs={{0,4},{4,0},{1,5},{5,1},{2,6},{6,2},{3,7},{7,3},{8,12},{12,8},{9,1... | collective-permute-start | bytes 786440 | tf_op jit(solution)/shard_map/ppermute | solution.py:362
  134.0 1.3 copy-start.2

commit v4 on v3

--- a/solution.py
+++ b/solution.py
@@ -8,7 +8,7 @@
 
 
 EP = ("ep_0", "ep_1", "ep_2")
-CHIPS = ("ep_0", "ep_1")
+CHIPS = ("ep_1", "ep_0")
 F32 = jnp.float32
 BF16 = jnp.bfloat16
 EXPERTS = 64
@@ -64,16 +64,17 @@
     return jax.ShapeDtypeStruct(shape, dtype)
 
 
+def peer_of(expert):
+    return (expert & 3) * 16 + (expert >> 2)
+
+
 def pack_kernel(
-    tok_hbm, cot_hbm, routes_ref, weights_ref, out_ref, keys_ref, cols_ref, cot_ref, tok_ref, sems
+    tok_ref, cot_ref, routes_ref, weights_ref, out_ref, keys_ref, cols_ref, cot_out
 ):
     tokens = 128
-    tok_copy = pltpu.make_async_copy(tok_hbm, tok_ref, sems.at[0])
-    cot_copy = pltpu.make_async_copy(cot_hbm, cot_ref, sems.at[1])
-    tok_copy.start()
-    cot_copy.start()
-    r0 = routes_ref[0:1, :].astype(F32)
-    r1 = routes_ref[1:2, :].astype(F32)
+    cot_out[...] = cot_ref[...]
+    r0 = peer_of(routes_ref[0:1, :]).astype(F32)
+    r1 = peer_of(routes_ref[1:2, :]).astype(F32)
     w = weights_ref[...].astype(F32)
     row = iota((tokens, tokens), 0)
     lane = iota((tokens, tokens), 1)
@@ -98,8 +99,6 @@
     m_row = iota((msgs, 512), 0)
     dest = m_row // 8
     sub = m_row % 8
-    tok_copy.wait()
-    cot_copy.wait()
     data = jnp.concatenate(
         [tok_ref[:, :128], tok_ref[:, 128:], cot_ref[:, :128], cot_ref[:, 128:]], axis=0
     )
@@ -254,7 +253,7 @@
         route_ref[a : a + 1, :] = jnp.sum(jnp.where(keep, cells, 0.0), axis=0, keepdims=True)
     e_row = iota((EXPERTS, msgs), 0)
     e_col = iota((EXPERTS, msgs), 1)
-    mix = dot(onehot(e_col == e_row * 8 + CAP + 1), got)
+    mix = dot(onehot(e_col == peer_of(e_row) * 8 + CAP + 1), got)
     mix_ref[...] = mix[:, 0:128] + mix[:, 128:256]
 
 
@@ -383,11 +382,6 @@
         cotangent,
         routes_t,
         weights_t,
-        hbm=2,
-        scratch=(
-            pltpu.VMEM((128, 256), BF16),
-            pltpu.SemaphoreType.DMA((2,)),
-        ),
     )
     arrived = swap(packed.reshape(64, 8, 384), CHIPS)
 

time: 156 us -> 154 us (0.987)
  the two profiles are of different devices: /device:TPU:8 before, /device:TPU:6 now
where the time goes in v4:
time: 154 us
  starting transfers between devices  53.2 us (35%)
  blocking collectives  43.9 us (29%)
  waiting for transfers between devices  32.4 us (21%)
  Pallas kernels  21.1 us (14%)
  local copies, waits for them, and re-layouts  2.01 us (1%)
    all_to_all x4, starting transfers between devices, swap(): return lax.all_to_all(value, axes, split_axis=0, concat_axis=0, tiled=True)  34.9 us
    all_to_all x4, waiting for transfers between devices, swap(): return lax.all_to_all(value, axes, split_axis=0, concat_axis=0, tiled=True)  24 us
    pallas_call x14, Pallas kernels, call(): pl.pallas_call(body, out_shape=outs, in_specs=[in_hbm] * hbm + [whole] *...  21.1 us
    all_to_all x1, blocking collectives, swap(): return lax.all_to_all(value, axes, split_axis=0, concat_axis=0, tiled=True)  18.9 us
    ppermute x8, starting transfers between devices, shift(): return lax.ppermute(value, axis, [(i, (i + by) % n) for i in range(n)])  18.2 us
    all_gather x1, blocking collectives, local(): cot_all = lax.all_gather(cot_here, 'tp', axis=1, tiled=True)  12.8 us
    all_gather x1, blocking collectives, local(): dense_w = lax.all_gather(dense_w, 'ep_1', axis=0, tiled=True)  12.3 us
    ppermute x8, waiting for transfers between devices, shift(): return lax.ppermute(value, axis, [(i, (i + by) % n) for i in range(n)])  8.46 us
  transfers between devices with their start and end apart: 12, of which 7 were waited for; matrix products, arithmetic and copies ran while one was open for 0% of the time, Pallas kernels for 7%

profile of v4, /device:TPU:6, one launch (start us, length us, event | category | flops | bytes accessed | tf_op | source)
XLA Modules:
  0.0 153.5 jit_solution(11643409682758532063)
XLA Ops:
  0.6 2.6 %shard_map.144 = (bf16[512,384]{1,0:T(8,128)(2,1)}, f32[8,128]{1,0:T(8,128)S(1)}, f32[128,128]{1,0:T(8,128)S(1)}, bf16[128,256]{1,0:T(8,128)(2,1)S(1)}) custom-call(bf16[128,256]{1,0:T(8,128)(2,1)} %refs_1_.3, bf16[128,256]{1,0:T(8,128)(2,1)} %refs_1_.2, s32[2,128]{1,0:T(2,128)} %bitcast.39, bf16[2,128]{1,0:T(2,128)(2,1)} %bitcast.40), custom_call_target="tpu_custom_call" | custom-call | flops 200000000 | bytes 1000000 | tf_op jit(solution)/shard_map/pallas_call | solution.py:50
  3.2 18.8 %all-to-all-start = ((bf16[64,8,384]{2,1,0:T(8,128)(2,1)}), bf16[64,8,384]{2,1,0:T(8,128)(2,1)S(1)}, u32[]{:S(2)}, u32[]{:S(2)}) async-start(bf16[64,8,384]{2,1,0:T(8,128)(2,1)} %bitcast.2), calls=%async_computation | async-start | bytes 786432 | tf_op jit(solution)/shard_map/all_to_all | solution.py:356
  22.0 12.8 %all_gather.6.refs_0_ = bf16[128,1024]{1,0:T(8,128)(2,1)S(1)} all-gather(bf16[128,256]{1,0:T(8,128)(2,1)S(1)} %get-tuple-element.45), channel_id=1, replica_groups=mesh['ep_0'=16,'ep_1'=4,'ep_2'=2,'tp'=4] {'tp'}, dimensions={1}, use_global_device_ids=true | all-gather | bytes 327680 | tf_op jit(solution)/shard_map/all_gather | solution.py:388
  34.8 1.2 shard_map.145
  35.9 1.9 %collective-permute-start = (bf16[512,256]{1,0:T(8,128)(2,1)S(1)}, bf16[512,256]{1,0:T(8,128)(2,1)S(1)}, u32[]{:S(2)}, u32[]{:S(2)}) collective-permute-start(bf16[512,256]{1,0:T(8,128)(2,1)S(1)} %get-tuple-element.47), channel_id=1, source_target_pairs={{0,4},{4,0},{1,5},{5,1},{2,6},{6,2},{3,7},{7,3},{8,12},{12,8},{9,1... | collective-permute-start | bytes 786440 | tf_op jit(solution)/shard_map/ppermute | solution.py:361
  37.9 1.5 collective-permute-done.refs_1_
  39.5 8.8 %all-to-all-done = bf16[64,8,384]{2,1,0:T(8,128)(2,1)S(1)} async-done(((bf16[64,8,384]{2,1,0:T(8,128)(2,1)}), bf16[64,8,384]{2,1,0:T(8,128)(2,1)S(1)}, u32[]{:S(2)}, u32[]{:S(2)}) %all-to-all-start) | async-done | bytes 393248 | tf_op jit(solution)/shard_map/all_to_all | solution.py:356
  48.3 1.7 %shard_map.147 = bf16[4,336,512]{2,1,0:T(8,128)(2,1)} custom-call(bf16[512,384]{1,0:T(8,128)(2,1)S(1)} %bitcast.27, f32[128,256]{1,0:T(8,128)S(1)} %get-tuple-element.48.refs_1_.refs_0_), custom_call_target="tpu_custom_call" | custom-call | flops 200000000 | bytes 1000000 | tf_op jit(solution)/shard_map/pallas_call | solution.py:50
  49.9 4.6 %all-to-all-start.1 = ((bf16[4,336,512]{2,1,0:T(8,128)(2,1)}), bf16[4,336,512]{2,1,0:T(8,128)(2,1)S(1)}, u32[]{:S(2)}, u32[]{:S(2)}) async-start(bf16[4,336,512]{2,1,0:T(8,128)(2,1)} %shard_map.147), calls=%async_computation.1 | async-start | bytes 2752512 | tf_op jit(solution)/shard_map/all_to_all | solution.py:356
  54.5 2.2 %collective-permute-start.1 = (bf16[128,256]{1,0:T(8,128)(2,1)S(1)}, bf16[128,256]{1,0:T(8,128)(2,1)S(1)}, u32[]{:S(2)}, u32[]{:S(2)}) collective-permute-start(bf16[128,256]{1,0:T(8,128)(2,1)S(1)} %get-tuple-element.49), channel_id=1, source_target_pairs={{0,8},{8,16},{16,24},{24,0},{1,9},{9,17},{17,25},{25,1},{2,10},{10... | collective-permute-start | bytes 196616 | tf_op jit(solution)/shard_map/ppermute | solution.py:361
  56.7 4.4 %collective-permute-start.2 = (bf16[128,256]{1,0:T(8,128)(2,1)S(1)}, bf16[128,256]{1,0:T(8,128)(2,1)S(1)}, u32[]{:S(2)}, u32[]{:S(2)}) collective-permute-start(bf16[128,256]{1,0:T(8,128)(2,1)S(1)} %get-tuple-element.50), channel_id=1, source_target_pairs={{0,16},{8,24},{16,0},{24,8},{1,17},{9,25},{17,1},{25,9},{2,18},{10... | collective-permute-start | bytes 196616 | tf_op jit(solution)/shard_map/ppermute | solution.py:361
  61.2 1.9 %collective-permute-start.3 = (bf16[128,256]{1,0:T(8,128)(2,1)S(1)}, bf16[128,256]{1,0:T(8,128)(2,1)S(1)}, u32[]{:S(2)}, u32[]{:S(2)}) collective-permute-start(bf16[128,256]{1,0:T(8,128)(2,1)S(1)} %get-tuple-element.51), channel_id=1, source_target_pairs={{0,24},{8,0},{16,8},{24,16},{1,25},{9,1},{17,9},{25,17},{2,26},{10... | collective-permute-start | bytes 196616 | tf_op jit(solution)/shard_map/ppermute | solution.py:361
  63.1 1.8 %collective-permute-done.2.refs_2_ = bf16[128,256]{1,0:T(8,128)(2,1)S(1)} collective-permute-done((bf16[128,256]{1,0:T(8,128)(2,1)S(1)}, bf16[128,256]{1,0:T(8,128)(2,1)S(1)}, u32[]{:S(2)}, u32[]{:S(2)}) %collective-permute-start.2) | collective-permute-done | bytes 65568 | tf_op jit(solution)/shard_map/ppermute | solution.py:361
  64.9 3.6 %collective-permute-done.3.refs_3_ = bf16[128,256]{1,0:T(8,128)(2,1)S(1)} collective-permute-done((bf16[128,256]{1,0:T(8,128)(2,1)S(1)}, bf16[128,256]{1,0:T(8,128)(2,1)S(1)}, u32[]{:S(2)}, u32[]{:S(2)}) %collective-permute-start.3) | collective-permute-done | bytes 65568 | tf_op jit(solution)/shard_map/ppermute | solution.py:361
  68.6 2.5 %all-to-all-done.1.refs_0_ = bf16[4,336,512]{2,1,0:T(8,128)(2,1)S(1)} async-done(((bf16[4,336,512]{2,1,0:T(8,128)(2,1)}), bf16[4,336,512]{2,1,0:T(8,128)(2,1)S(1)}, u32[]{:S(2)}, u32[]{:S(2)}) %all-to-all-start.1) | async-done | bytes 1376288 | tf_op jit(solution)/shard_map/all_to_all | solution.py:356
  71.1 1.9 %collective-permute-start.4 = (bf16[4,336,512]{2,1,0:T(8,128)(2,1)S(1)}, bf16[4,336,512]{2,1,0:T(8,128)(2,1)S(1)}, u32[]{:S(2)}, u32[]{:S(2)}) collective-permute-start(bf16[4,336,512]{2,1,0:T(8,128)(2,1)S(1)} %all-to-all-done.1.refs_0_), channel_id=1, source_target_pairs={{0,4},{4,0},{1,5},{5,1},{2,6},{6,2},{3,7},{7,3},{8,12},{12,8},{9,1... | collective-permute-start | bytes 4128776 | tf_op jit(solution)/shard_map/ppermute | solution.py:361
  73.0 1.6 %shard_map.149 = (bf16[352,1024]{1,0:T(8,128)(2,1)S(1)}, bf16[352,1024]{1,0:T(8,128)(2,1)S(1)}, bf16[352,1024]{1,0:T(8,128)(2,1)S(1)}) custom-call(bf16[352,1024]{1,0:T(8,128)(2,1)} %bitcast.36, bf16[352,1024]{1,0:T(8,128)(2,1)} %bitcast.37, bf16[352,1024]{1,0:T(8,128)(2,1)} %bitcast.38), custom_call_target="tpu_custom_call" | custom-call | flops 200000000 | bytes 1000000 | tf_op jit(solution)/shard_map/pallas_call | solution.py:50
  74.6 1.5 collective-permute-done.4.refs_0_.refs_1_
  76.1 2.6 %shard_map.151 = (bf16[4,336,256]{2,1,0:T(8,128)(2,1)S(1)}, bf16[320,352]{1,0:T(8,128)(2,1)}, bf16[320,352]{1,0:T(8,128)(2,1)}, bf16[320,352]{1,0:T(8,128)(2,1)}) custom-call(bf16[4,336,512]{2,1,0:T(8,128)(2,1)S(1)} %collective-permute-done.4.refs_0_.refs_1_, bf16[352,1024]{1,0:T(8,128)(2,1)S(1)} %get-tuple-element.53.refs_1_, ...), custom_call_target="tpu_custom_call" | custom-call | flops 1150000000 | bytes 1000000 | tf_op jit(solution)/shard_map/pallas_call | solution.py:50
  78.8 2.0 %collective-permute-start.5 = (bf16[4,336,256]{2,1,0:T(8,128)(2,1)S(1)}, bf16[4,336,256]{2,1,0:T(8,128)(2,1)S(1)}, u32[]{:S(2)}, u32[]{:S(2)}) collective-permute-start(bf16[4,336,256]{2,1,0:T(8,128)(2,1)S(1)} %get-tuple-element.57), channel_id=1, source_target_pairs={{0,4},{4,0},{1,5},{5,1},{2,6},{6,2},{3,7},{7,3},{8,12},{12,8},{9,1... | collective-permute-start | bytes 2064392 | tf_op jit(solution)/shard_map/ppermute | solution.py:361
  80.8 18.9 %all_to_all.25 = bf16[16,16,256]{2,1,0:T(8,128)(2,1)S(1)} all-to-all(bf16[16,16,256]{2,1,0:T(8,128)(2,1)S(1)} %bitcast.29), channel_id=1, replica_groups=mesh['ep_0'=16,'ep_1'=4,'ep_2'=2,'tp'=4] {'ep_0'}, dimensions={0} | all-to-all | bytes 262144 | tf_op jit(solution)/shard_map/all_to_all | solution.py:356
  100.4 1.9 %collective-permute-start.6 = (f32[8,128]{1,0:T(8,128)S(1)}, f32[8,128]{1,0:T(8,128)S(1)}, u32[]{:S(2)}, u32[]{:S(2)}) collective-permute-start(f32[8,128]{1,0:T(8,128)S(1)} %get-tuple-element.61.refs_2_), channel_id=1, source_target_pairs={{0,4},{4,0},{1,5},{5,1},{2,6},{6,2},{3,7},{7,3},{8,12},{12,8},{9,1... | collective-permute-start | bytes 12296 | tf_op jit(solution)/shard_map/ppermute | solution.py:361
  102.4 2.7 %shard_map.150 = (bf16[4,336,256]{2,1,0:T(8,128)(2,1)S(1)}, bf16[320,352]{1,0:T(8,128)(2,1)}, bf16[320,352]{1,0:T(8,128)(2,1)}, bf16[320,352]{1,0:T(8,128)(2,1)}) custom-call(bf16[4,336,512]{2,1,0:T(8,128)(2,1)S(1)} %all-to-all-done.1.refs_0_, bf16[352,1024]{1,0:T(8,128)(2,1)S(1)} %get-tuple-element.53.refs_1_, ...), custom_call_target="tpu_custom_call" | custom-call | flops 1150000000 | bytes 1000000 | tf_op jit(solution)/shard_map/pallas_call | solution.py:50
  105.0 1.0 shard_map.153
  106.0 3.5 %all-to-all-start.3 = ((bf16[4,336,256]{2,1,0:T(8,128)(2,1)}), bf16[4,336,256]{2,1,0:T(8,128)(2,1)S(1)}, u32[]{:S(2)}, u32[]{:S(2)}) async-start(bf16[4,336,256]{2,1,0:T(8,128)(2,1)} %shard_map.153), calls=%async_computation.3 | async-start | bytes 1376256 | tf_op jit(solution)/shard_map/all_to_all | solution.py:356
  109.5 12.3 %all_gather.7.refs_2_ = bf16[512,256]{1,0:T(8,128)(2,1)S(1)} all-gather(bf16[128,256]{1,0:T(8,128)(2,1)S(1)} %get-tuple-element.62), channel_id=1, replica_groups=mesh['ep_0'=16,'ep_1'=4,'ep_2'=2,'tp'=4] {'ep_1'}, dimensions={0}, use_global_device_ids=true | all-gather | bytes 327680 | tf_op jit(solution)/shard_map/all_gather | solution.py:443
  121.8 1.4 shard_map.154.refs_8_
  123.2 8.1 %all-to-all-start.4 = ((bf16[64,8,256]{2,1,0:T(8,128)(2,1)}), bf16[64,8,256]{2,1,0:T(8,128)(2,1)S(1)}, u32[]{:S(2)}, u32[]{:S(2)}) async-start(bf16[64,8,256]{2,1,0:T(8,128)(2,1)} %bitcast.13), calls=%async_computation.4 | async-start | bytes 524288 | tf_op jit(solution)/shard_map/all_to_all | solution.py:356
  131.2 1.9 %collective-permute-start.7 = (bf16[512,256]{1,0:T(8,128)(2,1)S(1)}, bf16[512,256]{1,0:T(8,128)(2,1)S(1)}, u32[]{:S(2)}, u32[]{:S(2)}) collective-permute-start(bf16[512,256]{1,0:T(8,128)(2,1)S(1)} %all_gather.7.refs_2_), channel_id=1, source_target_pairs={{0,4},{4,0},{1,5},{5,1},{2,6},{6,2},{3,7},{7,3},{8,12},{12,8},{9,1... | collective-permute-start | bytes 786440 | tf_op jit(solution)/shard_map/ppermute | solution.py:361
  133.2 1.3 copy-done.2
  134.5 4.4 %shard_map.156 = (bf16[352,1024]{1,0:T(8,128)(2,1)}, bf16[352,1024]{1,0:T(8,128)(2,1)}, bf16[352,1024]{1,0:T(8,128)(2,1)}, f32[8,128]{1,0:T(8,128)S(1)}) custom-call(bf16[4,336,512]{2,1,0:T(8,128)(2,1)S(1)} %all-to-all-done.1.refs_0_, bf16[4,336,512]{2,1,0:T(8,128)(2,1)S(1)} %copy-done.2, bf16[320,352]{1,0:T(8,128)(2,1)} %get-tuple-element.67.refs_2_, ...), custom_call_target="tpu_custom_call" | custom-call | flops 1400000000 | bytes 1000000 | tf_op jit(solution)/shard_map/pallas_call | solution.py:50
  139.2 12.7 %all-to-all-done.4 = bf16[64,8,256]{2,1,0:T(8,128)(2,1)S(1)} async-done(((bf16[64,8,256]{2,1,0:T(8,128)(2,1)}), bf16[64,8,256]{2,1,0:T(8,128)(2,1)S(1)}, u32[]{:S(2)}, u32[]{:S(2)}) %all-to-all-start.4) | async-done | bytes 262176 | tf_op jit(solution)/shard_map/all_to_all | solution.py:356
  (18 shorter events, 2.8 us)
Async XLA Ops:
  3.2 45.1 %all-to-all-start = ((bf16[64,8,384]{2,1,0:T(8,128)(2,1)}), bf16[64,8,384]{2,1,0:T(8,128)(2,1)S(1)}, u32[]{:S(2)}, u32[]{:S(2)}) async-start(bf16[64,8,384]{2,1,0:T(8,128)(2,1)} %bitcast.2), calls=%async_computation | async-start | bytes 786432 | tf_op jit(solution)/shard_map/all_to_all | solution.py:356
  35.9 3.4 %collective-permute-start = (bf16[512,256]{1,0:T(8,128)(2,1)S(1)}, bf16[512,256]{1,0:T(8,128)(2,1)S(1)}, u32[]{:S(2)}, u32[]{:S(2)}) collective-permute-start(bf16[512,256]{1,0:T(8,128)(2,1)S(1)} %get-tuple-element.47), channel_id=1, source_target_pairs={{0,4},{4,0},{1,5},{5,1},{2,6},{6,2},{3,7},{7,3},{8,12},{12,8},{9,1... | collective-permute-start | bytes 786440 | tf_op jit(solution)/shard_map/ppermute | solution.py:361
  49.9 18.6 %copy-start.3 = (bf16[256,8]{0,1:T(8,128)(2,1)S(1)}, bf16[256,8]{0,1:T(8,128)(2,1)}, u32[]{:S(2)}) copy-start(bf16[256,8]{0,1:T(8,128)(2,1)} %param.16) | copy-start | bytes 12292
  49.9 21.2 %all-to-all-start.1 = ((bf16[4,336,512]{2,1,0:T(8,128)(2,1)}), bf16[4,336,512]{2,1,0:T(8,128)(2,1)S(1)}, u32[]{:S(2)}, u32[]{:S(2)}) async-start(bf16[4,336,512]{2,1,0:T(8,128)(2,1)} %shard_map.147), calls=%async_computation.1 | async-start | bytes 2752512 | tf_op jit(solution)/shard_map/all_to_all | solution.py:356
  54.5 8.6 %collective-permute-start.1 = (bf16[128,256]{1,0:T(8,128)(2,1)S(1)}, bf16[128,256]{1,0:T(8,128)(2,1)S(1)}, u32[]{:S(2)}, u32[]{:S(2)}) collective-permute-start(bf16[128,256]{1,0:T(8,128)(2,1)S(1)} %get-tuple-element.49), channel_id=1, source_target_pairs={{0,8},{8,16},{16,24},{24,0},{1,9},{9,17},{17,25},{25,1},{2,10},{10... | collective-permute-start | bytes 196616 | tf_op jit(solution)/shard_map/ppermute | solution.py:361
  56.7 8.1 %collective-permute-start.2 = (bf16[128,256]{1,0:T(8,128)(2,1)S(1)}, bf16[128,256]{1,0:T(8,128)(2,1)S(1)}, u32[]{:S(2)}, u32[]{:S(2)}) collective-permute-start(bf16[128,256]{1,0:T(8,128)(2,1)S(1)} %get-tuple-element.50), channel_id=1, source_target_pairs={{0,16},{8,24},{16,0},{24,8},{1,17},{9,25},{17,1},{25,9},{2,18},{10... | collective-permute-start | bytes 196616 | tf_op jit(solution)/shard_map/ppermute | solution.py:361
  61.2 7.4 %collective-permute-start.3 = (bf16[128,256]{1,0:T(8,128)(2,1)S(1)}, bf16[128,256]{1,0:T(8,128)(2,1)S(1)}, u32[]{:S(2)}, u32[]{:S(2)}) collective-permute-start(bf16[128,256]{1,0:T(8,128)(2,1)S(1)} %get-tuple-element.51), channel_id=1, source_target_pairs={{0,24},{8,0},{16,8},{24,16},{1,25},{9,1},{17,9},{25,17},{2,26},{10... | collective-permute-start | bytes 196616 | tf_op jit(solution)/shard_map/ppermute | solution.py:361
  71.1 5.0 %collective-permute-start.4 = (bf16[4,336,512]{2,1,0:T(8,128)(2,1)S(1)}, bf16[4,336,512]{2,1,0:T(8,128)(2,1)S(1)}, u32[]{:S(2)}, u32[]{:S(2)}) collective-permute-start(bf16[4,336,512]{2,1,0:T(8,128)(2,1)S(1)} %all-to-all-done.1.refs_0_), channel_id=1, source_target_pairs={{0,4},{4,0},{1,5},{5,1},{2,6},{6,2},{3,7},{7,3},{8,12},{12,8},{9,1... | collective-permute-start | bytes 4128776 | tf_op jit(solution)/shard_map/ppermute | solution.py:361
  76.1 2.6 %copy-start.1 = (bf16[4,336,512]{2,1,0:T(8,128)(2,1)}, bf16[4,336,512]{2,1,0:T(8,128)(2,1)S(1)}, u32[]{:S(2)}) copy-start(bf16[4,336,512]{2,1,0:T(8,128)(2,1)S(1)} %collective-permute-done.4.refs_0_.refs_1_) | copy-start | bytes 4128772
  76.1 23.6 %copy-start = (f32[1024]{0:T(1024)S(1)}, f32[1024]{0:T(1024)}, u32[]{:S(2)}) copy-start(f32[1024]{0:T(1024)} %param.17) | copy-start | bytes 12292
  78.8 21.0 %collective-permute-start.5 = (bf16[4,336,256]{2,1,0:T(8,128)(2,1)S(1)}, bf16[4,336,256]{2,1,0:T(8,128)(2,1)S(1)}, u32[]{:S(2)}, u32[]{:S(2)}) collective-permute-start(bf16[4,336,256]{2,1,0:T(8,128)(2,1)S(1)} %get-tuple-element.57), channel_id=1, source_target_pairs={{0,4},{4,0},{1,5},{5,1},{2,6},{6,2},{3,7},{7,3},{8,12},{12,8},{9,1... | collective-permute-start | bytes 2064392 | tf_op jit(solution)/shard_map/ppermute | solution.py:361
  100.4 4.6 %collective-permute-start.6 = (f32[8,128]{1,0:T(8,128)S(1)}, f32[8,128]{1,0:T(8,128)S(1)}, u32[]{:S(2)}, u32[]{:S(2)}) collective-permute-start(f32[8,128]{1,0:T(8,128)S(1)} %get-tuple-element.61.refs_2_), channel_id=1, source_target_pairs={{0,4},{4,0},{1,5},{5,1},{2,6},{6,2},{3,7},{7,3},{8,12},{12,8},{9,1... | collective-permute-start | bytes 12296 | tf_op jit(solution)/shard_map/ppermute | solution.py:361
  106.0 15.8 %all-to-all-start.3 = ((bf16[4,336,256]{2,1,0:T(8,128)(2,1)}), bf16[4,336,256]{2,1,0:T(8,128)(2,1)S(1)}, u32[]{:S(2)}, u32[]{:S(2)}) async-start(bf16[4,336,256]{2,1,0:T(8,128)(2,1)} %shard_map.153), calls=%async_computation.3 | async-start | bytes 1376256 | tf_op jit(solution)/shard_map/all_to_all | solution.py:356
  123.2 28.7 %all-to-all-start.4 = ((bf16[64,8,256]{2,1,0:T(8,128)(2,1)}), bf16[64,8,256]{2,1,0:T(8,128)(2,1)S(1)}, u32[]{:S(2)}, u32[]{:S(2)}) async-start(bf16[64,8,256]{2,1,0:T(8,128)(2,1)} %bitcast.13), calls=%async_computation.4 | async-start | bytes 524288 | tf_op jit(solution)/shard_map/all_to_all | solution.py:356
  131.2 7.7 %collective-permute-start.7 = (bf16[512,256]{1,0:T(8,128)(2,1)S(1)}, bf16[512,256]{1,0:T(8,128)(2,1)S(1)}, u32[]{:S(2)}, u32[]{:S(2)}) collective-permute-start(bf16[512,256]{1,0:T(8,128)(2,1)S(1)} %all_gather.7.refs_2_), channel_id=1, source_target_pairs={{0,4},{4,0},{1,5},{5,1},{2,6},{6,2},{3,7},{7,3},{8,12},{12,8},{9,1... | collective-permute-start | bytes 786440 | tf_op jit(solution)/shard_map/ppermute | solution.py:361
  133.2 1.3 copy-start.2

commit v5 on v4

--- a/solution.py
+++ b/solution.py
@@ -257,26 +257,22 @@
     mix_ref[...] = mix[:, 0:128] + mix[:, 128:256]
 
 
-def moment_kernel(cot_ref, tok_ref, keep_ref, send_ref):
+def moment_kernel(cot_ref, tok_ref, out_ref):
     moment = dot_tn(cot_ref[...], tok_ref[...])
-    north = lax.axis_index("ep_2") == 1
     for x in range(4):
-        parts = []
-        for c in range(2):
-            starts = [(z * 8 + x * 2 + c) * 8 for z in range(16)]
-            parts.append(jnp.concatenate([moment[s : s + 8] for s in starts], axis=0))
-        span = slice(x * 128, (x + 1) * 128)
-        keep_ref[span, :] = jnp.where(north, parts[1], parts[0])
-        send_ref[span, :] = jnp.where(north, parts[0], parts[1]).astype(BF16)
+        starts = [(z * 8 + x * 2) * 8 for z in range(16)]
+        out_ref[x * 256 : (x + 1) * 256, :] = jnp.concatenate(
+            [moment[s : s + 16] for s in starts], axis=0
+        )
 
 
 def core_sum_kernel(keep_ref, got_ref, own_ref, s1_ref, s2_ref, s3_ref, sum_ref):
-    sum_ref[...] = keep_ref[...] + got_ref[...].astype(F32)
+    sum_ref[...] = keep_ref[...] + got_ref[...]
     here = lax.axis_index("ep_1")
 
     def part(shift):
-        start = pl.multiple_of(lax.rem(here + shift, 4) * 128, 128)
-        return sum_ref[pl.ds(start, 128), :]
+        start = pl.multiple_of(lax.rem(here + shift, 4) * 256, 256)
+        return sum_ref[pl.ds(start, 256), :]
 
     own_ref[...] = part(0)
     s1_ref[...] = part(1).astype(BF16)
@@ -290,23 +286,28 @@
     dense = dense_ref[...].astype(F32)
     pieces = []
     for z in range(16):
-        pieces += [total[z * 8 : z * 8 + 8], dense]
+        pieces += [total[z * 16 : z * 16 + 16], dense]
     out_ref[...] = jnp.concatenate(pieces, axis=0).astype(BF16)
 
 
-def z_sum_kernel(in_ref, gate_ref, dense_ref, grad_ref, share_ref, w_ref):
+def z_sum_kernel(in_ref, gate_ref, dense_ref, dense_other_ref, grad_ref, share_ref, w_ref):
     got = in_ref[...].astype(F32)
-    moment = sum(got[z * 16 : z * 16 + 8] for z in range(16)) * (1.0 / 128)
+    moment = sum(got[z * 24 : z * 24 + 16] for z in range(16)) * (1.0 / 128)
     w_ref[...] = jnp.concatenate(
-        [got[z * 16 + 8 : z * 16 + 16] for z in range(16)], axis=0
+        [got[z * 24 + 16 : z * 24 + 24] for z in range(16)], axis=0
     ).astype(BF16)
     core = lax.axis_index("ep_2")
     first = (lax.axis_index("ep_0") * 8 + lax.axis_index("ep_1") * 2 + core) * 8
     at = iota((8, 1024), 1) == first + iota((8, 1024), 0)
     gate = jnp.sum(jnp.where(at, gate_ref[...], 0.0), axis=1, keepdims=True)
-    grad_ref[...] = moment * gate
-    share = jnp.sum(moment * dense_ref[...].astype(F32), axis=1, keepdims=True)
-    spot = iota((8, 128), 1) == core * 8 + iota((8, 128), 0)
+    grad_ref[...] = jnp.where(core == 0, moment[0:8], moment[8:16]) * gate
+    own = dense_ref[...].astype(F32)
+    other = dense_other_ref[...].astype(F32)
+    dense = jnp.concatenate(
+        [jnp.where(core == 0, own, other), jnp.where(core == 0, other, own)], axis=0
+    )
+    share = jnp.sum(moment * dense, axis=1, keepdims=True)
+    spot = iota((16, 128), 1) == iota((16, 128), 0)
     row = jnp.sum(jnp.where(spot, share, 0.0), axis=0, keepdims=True)
     share_ref[...] = jnp.broadcast_to(row, (8, 128))
 
@@ -327,12 +328,12 @@
     out_ref[...] = dot(scaled, weight)
 
 
-def add_kernel(a_ref, b_ref, m0_ref, m1_ref, out_ref):
+def add_kernel(a_ref, b_ref, mix_ref, out_ref):
     def parts(value):
         hi = value.astype(BF16).astype(F32)
         return hi, value - hi
 
-    mix = parts(jnp.concatenate([m0_ref[0:1, :] + m1_ref[0:1, :], jnp.zeros((1, 128), F32)], axis=1))
+    mix = parts(jnp.concatenate([mix_ref[0:1, :], jnp.zeros((1, 128), F32)], axis=1))
     sub = iota((8, 256), 0)
     extra = []
     both = a_ref[0, ROWS : ROWS + EXTRA, :].astype(F32) + b_ref[0, ROWS : ROWS + EXTRA, :].astype(F32)
@@ -386,19 +387,19 @@
     arrived = swap(packed.reshape(64, 8, 384), CHIPS)
 
     cot_all = lax.all_gather(cot_here, "tp", axis=1, tiled=True)
-    keep, send = call(
-        moment_kernel, (struct(512, 256, dtype=F32), struct(512, 256)), cot_all, tokens
-    )
+    dense_other = shift(lax.optimization_barrier((dense_t, cot_all))[0], "ep_2", 1)
+    keep = call(moment_kernel, struct(1024, 256, dtype=F32), cot_all, tokens)
     here, *away = call(
         core_sum_kernel,
-        (struct(128, 256, dtype=F32),) + (struct(128, 256),) * 3,
+        (struct(256, 256, dtype=F32),) + (struct(256, 256),) * 3,
         keep,
-        shift(send, "ep_2", 1),
-        scratch=(pltpu.VMEM((512, 256), F32),),
+        shift(keep, "ep_2", 1),
+        scratch=(pltpu.VMEM((1024, 256), F32),),
+        after=(dense_other,),
     )
     both = call(
         x_sum_kernel,
-        struct(256, 256),
+        struct(384, 256),
         here,
         *(shift(piece, "ep_1", i + 1) for i, piece in enumerate(away)),
         dense_t,
@@ -427,7 +428,7 @@
         scratch=(pltpu.SemaphoreType.DMA((3,)),),
     )
     z_own, *act_own = call(expert_kernel, outs, own, *weights, **expert)
-    z_got = swap(both.reshape(16, 16, 256), "ep_0").reshape(256, 256)
+    z_got = swap(both.reshape(16, 24, 256), "ep_0").reshape(384, 256)
     z_other, *act_other = call(expert_kernel, outs, other, *weights, **expert)
     z_back = shift(z_other, "ep_2", 1)
     z_back, z_got = lax.optimization_barrier((z_back, z_got))
@@ -437,8 +438,9 @@
         z_got,
         gate_row,
         dense_t,
-    )
-    z_sum = call(add_kernel, outs[0], z_own, z_back, share, shift(share, "ep_2", 1))
+        dense_other,
+    )
+    z_sum = call(add_kernel, outs[0], z_own, z_back, share)
     z_all = swap(z_sum, "tp")
     dense_w = lax.all_gather(dense_w, "ep_1", axis=0, tiled=True)
     z_all, dense_w = lax.optimization_barrier((z_all, dense_w))

time: 154 us -> 154 us (level)
  blocking collectives: 43.9 us -> 25 us
  starting transfers between devices: 53.2 us -> 64.7 us
  local copies, waits for them, and re-layouts: 2.01 us -> 6.57 us
  Pallas kernels: 21.1 us -> 24.3 us
    all_to_all x1 -> x0, blocking collectives: 18.9 us -> none  [swap(): return lax.all_to_all(value, axes, split_axis=0, concat_axis=0, tiled=True)]
    all_to_all x4 -> x5, starting transfers between devices: 34.9 us -> 45.8 us  [swap(): return lax.all_to_all(value, axes, split_axis=0, concat_axis=0, tiled=True)]
    unnamed x8 -> x16, local copies, waits for them, and re-layouts: 1.34 us -> 5.9 us
    pallas_call x14, Pallas kernels: 21.1 us -> 24.3 us  [call(): pl.pallas_call(body, out_shape=outs, in_specs=[in_hbm] * hbm + [whole] *...]
    all_to_all x4 -> x5, waiting for transfers between devices: 24 us -> 24.8 us  [swap(): return lax.all_to_all(value, axes, split_axis=0, concat_axis=0, tiled=True)]
  transfers between devices with their start and end apart: 12 -> 13, of which waited for: 7 -> 7; matrix products, arithmetic and copies ran while one was open for 0% -> 0% of each run, Pallas kernels for 7% -> 10%
where the time goes in v5:
time: 154 us; the launch traced here: 153 us
  starting transfers between devices  64.7 us (42%)
  waiting for transfers between devices  31.8 us (21%)
  blocking collectives  25 us (16%)
  Pallas kernels  24.3 us (16%)
  local copies, waits for them, and re-layouts  6.57 us (4%)
    all_to_all x5, starting transfers between devices, swap(): return lax.all_to_all(value, axes, split_axis=0, concat_axis=0, tiled=True)  45.8 us
    all_to_all x5, waiting for transfers between devices, swap(): return lax.all_to_all(value, axes, split_axis=0, concat_axis=0, tiled=True)  24.8 us
    pallas_call x14, Pallas kernels, call(): pl.pallas_call(body, out_shape=outs, in_specs=[in_hbm] * hbm + [whole] *...  24.3 us
    ppermute x8, starting transfers between devices, shift(): return lax.ppermute(value, axis, [(i, (i + by) % n) for i in range(n)])  18.8 us
    all_gather x1, blocking collectives, local(): cot_all = lax.all_gather(cot_here, 'tp', axis=1, tiled=True)  12.8 us
    all_gather x1, blocking collectives, local(): dense_w = lax.all_gather(dense_w, 'ep_1', axis=0, tiled=True)  12.3 us
    ppermute x8, waiting for transfers between devices, shift(): return lax.ppermute(value, axis, [(i, (i + by) % n) for i in range(n)])  6.95 us
    unnamed x16, local copies, waits for them, and re-layouts  5.9 us
  transfers between devices with their start and end apart: 13, of which 7 were waited for; matrix products, arithmetic and copies ran while one was open for 0% of the time, Pallas kernels for 10%

profile of v5, /device:TPU:6, one launch (start us, length us, event | category | flops | bytes accessed | tf_op | source)
XLA Modules:
  0.0 153.2 jit_solution(16071083447463468705)
XLA Ops:
  0.6 2.6 %shard_map.144 = (bf16[512,384]{1,0:T(8,128)(2,1)}, f32[8,128]{1,0:T(8,128)S(1)}, f32[128,128]{1,0:T(8,128)S(1)}, bf16[128,256]{1,0:T(8,128)(2,1)S(1)}) custom-call(bf16[128,256]{1,0:T(8,128)(2,1)} %refs_1_.3, bf16[128,256]{1,0:T(8,128)(2,1)} %refs_1_.2, s32[2,128]{1,0:T(2,128)} %bitcast.39, bf16[2,128]{1,0:T(2,128)(2,1)} %bitcast.40), custom_call_target="tpu_custom_call" | custom-call | flops 200000000 | bytes 1000000 | tf_op jit(solution)/shard_map/pallas_call | solution.py:50
  3.2 18.9 %all-to-all-start = ((bf16[64,8,384]{2,1,0:T(8,128)(2,1)}), bf16[64,8,384]{2,1,0:T(8,128)(2,1)S(1)}, u32[]{:S(2)}, u32[]{:S(2)}) async-start(bf16[64,8,384]{2,1,0:T(8,128)(2,1)} %bitcast.2), calls=%async_computation | async-start | bytes 786432 | tf_op jit(solution)/shard_map/all_to_all | solution.py:357
  22.1 12.8 %all_gather.6.refs_0_ = bf16[128,1024]{1,0:T(8,128)(2,1)S(1)} all-gather(bf16[128,256]{1,0:T(8,128)(2,1)S(1)} %get-tuple-element.44), channel_id=1, replica_groups=mesh['ep_0'=16,'ep_1'=4,'ep_2'=2,'tp'=4] {'tp'}, dimensions={1}, use_global_device_ids=true | all-gather | bytes 327680 | tf_op jit(solution)/shard_map/all_gather | solution.py:389
  34.9 1.2 shard_map.145.refs_0_
  36.1 1.9 %collective-permute-start = (f32[1024,256]{1,0:T(8,128)S(1)}, f32[1024,256]{1,0:T(8,128)S(1)}, u32[]{:S(2)}, u32[]{:S(2)}) collective-permute-start(f32[1024,256]{1,0:T(8,128)S(1)} %shard_map.145.refs_0_), channel_id=1, source_target_pairs={{0,4},{4,0},{1,5},{5,1},{2,6},{6,2},{3,7},{7,3},{8,12},{12,8},{9,1... | collective-permute-start | bytes 3145736 | tf_op jit(solution)/shard_map/ppermute | solution.py:362
  38.0 2.4 %collective-permute-start.1 = (bf16[8,256]{1,0:T(8,128)(2,1)S(1)}, bf16[8,256]{1,0:T(8,128)(2,1)S(1)}, u32[]{:S(2)}, u32[]{:S(2)}) collective-permute-start(bf16[8,256]{1,0:T(8,128)(2,1)S(1)} %bitcast.31), channel_id=1, source_target_pairs={{0,4},{4,0},{1,5},{5,1},{2,6},{6,2},{3,7},{7,3},{8,12},{12,8},{9,1... | collective-permute-start | bytes 12296 | tf_op jit(solution)/shard_map/ppermute | solution.py:362
  41.4 7.0 %all-to-all-done = bf16[64,8,384]{2,1,0:T(8,128)(2,1)S(1)} async-done(((bf16[64,8,384]{2,1,0:T(8,128)(2,1)}), bf16[64,8,384]{2,1,0:T(8,128)(2,1)S(1)}, u32[]{:S(2)}, u32[]{:S(2)}) %all-to-all-start) | async-done | bytes 393248 | tf_op jit(solution)/shard_map/all_to_all | solution.py:357
  48.4 1.6 %shard_map.147 = bf16[4,336,512]{2,1,0:T(8,128)(2,1)} custom-call(bf16[512,384]{1,0:T(8,128)(2,1)S(1)} %bitcast.27, f32[256,256]{1,0:T(8,128)S(1)} %get-tuple-element.46.refs_1_.refs_0_), custom_call_target="tpu_custom_call" | custom-call | flops 200000000 | bytes 1000000 | tf_op jit(solution)/shard_map/pallas_call | solution.py:50
  50.0 4.5 %all-to-all-start.1 = ((bf16[4,336,512]{2,1,0:T(8,128)(2,1)}), bf16[4,336,512]{2,1,0:T(8,128)(2,1)S(1)}, u32[]{:S(2)}, u32[]{:S(2)}) async-start(bf16[4,336,512]{2,1,0:T(8,128)(2,1)} %shard_map.147), calls=%async_computation.1 | async-start | bytes 2752512 | tf_op jit(solution)/shard_map/all_to_all | solution.py:357
  54.5 2.2 %collective-permute-start.2 = (bf16[256,256]{1,0:T(8,128)(2,1)S(1)}, bf16[256,256]{1,0:T(8,128)(2,1)S(1)}, u32[]{:S(2)}, u32[]{:S(2)}) collective-permute-start(bf16[256,256]{1,0:T(8,128)(2,1)S(1)} %get-tuple-element.47), channel_id=1, source_target_pairs={{0,8},{8,16},{16,24},{24,0},{1,9},{9,17},{17,25},{25,1},{2,10},{10... | collective-permute-start | bytes 393224 | tf_op jit(solution)/shard_map/ppermute | solution.py:362
  56.7 4.4 %collective-permute-start.3 = (bf16[256,256]{1,0:T(8,128)(2,1)S(1)}, bf16[256,256]{1,0:T(8,128)(2,1)S(1)}, u32[]{:S(2)}, u32[]{:S(2)}) collective-permute-start(bf16[256,256]{1,0:T(8,128)(2,1)S(1)} %get-tuple-element.48), channel_id=1, source_target_pairs={{0,16},{8,24},{16,0},{24,8},{1,17},{9,25},{17,1},{25,9},{2,18},{10... | collective-permute-start | bytes 393224 | tf_op jit(solution)/shard_map/ppermute | solution.py:362
  61.2 1.9 %collective-permute-start.4 = (bf16[256,256]{1,0:T(8,128)(2,1)S(1)}, bf16[256,256]{1,0:T(8,128)(2,1)S(1)}, u32[]{:S(2)}, u32[]{:S(2)}) collective-permute-start(bf16[256,256]{1,0:T(8,128)(2,1)S(1)} %get-tuple-element.49), channel_id=1, source_target_pairs={{0,24},{8,0},{16,8},{24,16},{1,25},{9,1},{17,9},{25,17},{2,26},{10... | collective-permute-start | bytes 393224 | tf_op jit(solution)/shard_map/ppermute | solution.py:362
  63.1 3.2 %collective-permute-done.3.refs_2_ = bf16[256,256]{1,0:T(8,128)(2,1)S(1)} collective-permute-done((bf16[256,256]{1,0:T(8,128)(2,1)S(1)}, bf16[256,256]{1,0:T(8,128)(2,1)S(1)}, u32[]{:S(2)}, u32[]{:S(2)}) %collective-permute-start.3) | collective-permute-done | bytes 131104 | tf_op jit(solution)/shard_map/ppermute | solution.py:362
  66.3 2.9 %collective-permute-done.4.refs_3_ = bf16[256,256]{1,0:T(8,128)(2,1)S(1)} collective-permute-done((bf16[256,256]{1,0:T(8,128)(2,1)S(1)}, bf16[256,256]{1,0:T(8,128)(2,1)S(1)}, u32[]{:S(2)}, u32[]{:S(2)}) %collective-permute-start.4) | collective-permute-done | bytes 131104 | tf_op jit(solution)/shard_map/ppermute | solution.py:362
  70.0 1.1 all-to-all-done.1.refs_0_
  71.1 1.9 %collective-permute-start.5 = (bf16[4,336,512]{2,1,0:T(8,128)(2,1)S(1)}, bf16[4,336,512]{2,1,0:T(8,128)(2,1)}, u32[]{:S(2)}, u32[]{:S(2)}) collective-permute-start(bf16[4,336,512]{2,1,0:T(8,128)(2,1)S(1)} %all-to-all-done.1.refs_0_), channel_id=1, source_target_pairs={{0,4},{4,0},{1,5},{5,1},{2,6},{6,2},{3,7},{7,3},{8,12},{12,8},{9,1... | collective-permute-start | bytes 4128776 | tf_op jit(solution)/shard_map/ppermute | solution.py:362
  73.0 1.6 %shard_map.149 = (bf16[352,1024]{1,0:T(8,128)(2,1)S(1)}, bf16[352,1024]{1,0:T(8,128)(2,1)S(1)}, bf16[352,1024]{1,0:T(8,128)(2,1)S(1)}) custom-call(bf16[352,1024]{1,0:T(8,128)(2,1)} %bitcast.36, bf16[352,1024]{1,0:T(8,128)(2,1)} %bitcast.37, bf16[352,1024]{1,0:T(8,128)(2,1)} %bitcast.38), custom_call_target="tpu_custom_call" | custom-call | flops 200000000 | bytes 1000000 | tf_op jit(solution)/shard_map/pallas_call | solution.py:50
  77.1 6.7 %all-to-all-start.2 = ((bf16[16,24,256]{2,1,0:T(8,128)(2,1)}), bf16[16,24,256]{2,1,0:T(8,128)(2,1)S(1)}, u32[]{:S(2)}, u32[]{:S(2)}) async-start(bf16[16,24,256]{2,1,0:T(8,128)(2,1)} %bitcast.10), calls=%async_computation.2 | async-start | bytes 393216 | tf_op jit(solution)/shard_map/all_to_all | solution.py:357
  83.9 1.1 copy-done.3
  85.0 1.1 copy-done.5
  86.1 1.1 copy-done.7
  87.2 4.8 %shard_map.151 = (bf16[4,336,256]{2,1,0:T(8,128)(2,1)}, bf16[320,352]{1,0:T(8,128)(2,1)}, bf16[320,352]{1,0:T(8,128)(2,1)}, bf16[320,352]{1,0:T(8,128)(2,1)}) custom-call(bf16[4,336,512]{2,1,0:T(8,128)(2,1)} %collective-permute-done.5.refs_0_.refs_1_, bf16[352,1024]{1,0:T(8,128)(2,1)S(1)} %copy-done.3, bf16[352,1024]{1,0:T(8,128)(2,1)S(1)} %copy-done.5, ...), custom_call_target="tpu_custom_call" | custom-call | flops 1150000000 | bytes 1000000 | tf_op jit(solution)/shard_map/pallas_call | solution.py:50
  92.0 2.1 %collective-permute-start.6 = (bf16[4,336,256]{2,1,0:T(8,128)(2,1)}, bf16[4,336,256]{2,1,0:T(8,128)(2,1)S(1)}, u32[]{:S(2)}, u32[]{:S(2)}) collective-permute-start(bf16[4,336,256]{2,1,0:T(8,128)(2,1)} %get-tuple-element.55), channel_id=1, source_target_pairs={{0,4},{4,0},{1,5},{5,1},{2,6},{6,2},{3,7},{7,3},{8,12},{12,8},{9,1... | collective-permute-start | bytes 2064392 | tf_op jit(solution)/shard_map/ppermute | solution.py:362
  94.2 2.6 %shard_map.150 = (bf16[4,336,256]{2,1,0:T(8,128)(2,1)S(1)}, bf16[320,352]{1,0:T(8,128)(2,1)}, bf16[320,352]{1,0:T(8,128)(2,1)}, bf16[320,352]{1,0:T(8,128)(2,1)}) custom-call(bf16[4,336,512]{2,1,0:T(8,128)(2,1)S(1)} %all-to-all-done.1.refs_0_, bf16[352,1024]{1,0:T(8,128)(2,1)S(1)} %copy-done.3, bf16[352,1024]{1,0:T(8,128)(2,1)S(1)} %copy-done.5, ...), custom_call_target="tpu_custom_call" | custom-call | flops 1150000000 | bytes 1000000 | tf_op jit(solution)/shard_map/pallas_call | solution.py:50
  96.8 3.0 %all-to-all-done.2 = bf16[16,24,256]{2,1,0:T(8,128)(2,1)S(1)} async-done(((bf16[16,24,256]{2,1,0:T(8,128)(2,1)}), bf16[16,24,256]{2,1,0:T(8,128)(2,1)S(1)}, u32[]{:S(2)}, u32[]{:S(2)}) %all-to-all-start.2) | async-done | bytes 196640 | tf_op jit(solution)/shard_map/all_to_all | solution.py:357
  101.5 3.5 %all-to-all-start.3 = ((bf16[4,336,256]{2,1,0:T(8,128)(2,1)}), bf16[4,336,256]{2,1,0:T(8,128)(2,1)S(1)}, u32[]{:S(2)}, u32[]{:S(2)}) async-start(bf16[4,336,256]{2,1,0:T(8,128)(2,1)} %shard_map.153), calls=%async_computation.3 | async-start | bytes 1376256 | tf_op jit(solution)/shard_map/all_to_all | solution.py:357
  105.0 12.3 %all_gather.7.refs_2_ = bf16[512,256]{1,0:T(8,128)(2,1)S(1)} all-gather(bf16[128,256]{1,0:T(8,128)(2,1)S(1)} %get-tuple-element.60), channel_id=1, replica_groups=mesh['ep_0'=16,'ep_1'=4,'ep_2'=2,'tp'=4] {'ep_1'}, dimensions={0}, use_global_device_ids=true | all-gather | bytes 327680 | tf_op jit(solution)/shard_map/all_gather | solution.py:445
  117.3 1.4 shard_map.154.refs_8_
  118.6 12.2 %all-to-all-start.4 = ((bf16[64,8,256]{2,1,0:T(8,128)(2,1)}), bf16[64,8,256]{2,1,0:T(8,128)(2,1)S(1)}, u32[]{:S(2)}, u32[]{:S(2)}) async-start(bf16[64,8,256]{2,1,0:T(8,128)(2,1)} %bitcast.13), calls=%async_computation.4 | async-start | bytes 524288 | tf_op jit(solution)/shard_map/all_to_all | solution.py:357
  130.9 1.9 %collective-permute-start.7 = (bf16[512,256]{1,0:T(8,128)(2,1)S(1)}, bf16[512,256]{1,0:T(8,128)(2,1)S(1)}, u32[]{:S(2)}, u32[]{:S(2)}) collective-permute-start(bf16[512,256]{1,0:T(8,128)(2,1)S(1)} %all_gather.7.refs_2_), channel_id=1, source_target_pairs={{0,4},{4,0},{1,5},{5,1},{2,6},{6,2},{3,7},{7,3},{8,12},{12,8},{9,1... | collective-permute-start | bytes 786440 | tf_op jit(solution)/shard_map/ppermute | solution.py:362
  132.8 4.7 %shard_map.156 = (bf16[352,1024]{1,0:T(8,128)(2,1)}, bf16[352,1024]{1,0:T(8,128)(2,1)}, bf16[352,1024]{1,0:T(8,128)(2,1)}, f32[8,128]{1,0:T(8,128)S(1)}) custom-call(bf16[4,336,512]{2,1,0:T(8,128)(2,1)S(1)} %all-to-all-done.1.refs_0_, bf16[4,336,512]{2,1,0:T(8,128)(2,1)} %collective-permute-done.5.refs_0_.refs_1_, ...), custom_call_target="tpu_custom_call" | custom-call | flops 1400000000 | bytes 1000000 | tf_op jit(solution)/shard_map/pallas_call | solution.py:50
  137.8 13.7 %all-to-all-done.4 = bf16[64,8,256]{2,1,0:T(8,128)(2,1)S(1)} async-done(((bf16[64,8,256]{2,1,0:T(8,128)(2,1)}), bf16[64,8,256]{2,1,0:T(8,128)(2,1)S(1)}, u32[]{:S(2)}, u32[]{:S(2)}) %all-to-all-start.4) | async-done | bytes 262176 | tf_op jit(solution)/shard_map/all_to_all | solution.py:357
  (27 shorter events, 8.0 us)
Async XLA Ops:
  3.2 34.8 %copy-start = (bf16[256,8]{0,1:T(8,128)(2,1)S(1)}, bf16[256,8]{0,1:T(8,128)(2,1)}, u32[]{:S(2)}) copy-start(bf16[256,8]{0,1:T(8,128)(2,1)} %param.16) | copy-start | bytes 12292
  3.2 45.2 %all-to-all-start = ((bf16[64,8,384]{2,1,0:T(8,128)(2,1)}), bf16[64,8,384]{2,1,0:T(8,128)(2,1)S(1)}, u32[]{:S(2)}, u32[]{:S(2)}) async-start(bf16[64,8,384]{2,1,0:T(8,128)(2,1)} %bitcast.2), calls=%async_computation | async-start | bytes 786432 | tf_op jit(solution)/shard_map/all_to_all | solution.py:357
  36.1 5.2 %collective-permute-start = (f32[1024,256]{1,0:T(8,128)S(1)}, f32[1024,256]{1,0:T(8,128)S(1)}, u32[]{:S(2)}, u32[]{:S(2)}) collective-permute-start(f32[1024,256]{1,0:T(8,128)S(1)} %shard_map.145.refs_0_), channel_id=1, source_target_pairs={{0,4},{4,0},{1,5},{5,1},{2,6},{6,2},{3,7},{7,3},{8,12},{12,8},{9,1... | collective-permute-start | bytes 3145736 | tf_op jit(solution)/shard_map/ppermute | solution.py:362
  38.0 3.2 %collective-permute-start.1 = (bf16[8,256]{1,0:T(8,128)(2,1)S(1)}, bf16[8,256]{1,0:T(8,128)(2,1)S(1)}, u32[]{:S(2)}, u32[]{:S(2)}) collective-permute-start(bf16[8,256]{1,0:T(8,128)(2,1)S(1)} %bitcast.31), channel_id=1, source_target_pairs={{0,4},{4,0},{1,5},{5,1},{2,6},{6,2},{3,7},{7,3},{8,12},{12,8},{9,1... | collective-permute-start | bytes 12296 | tf_op jit(solution)/shard_map/ppermute | solution.py:362
  50.0 21.0 %all-to-all-start.1 = ((bf16[4,336,512]{2,1,0:T(8,128)(2,1)}), bf16[4,336,512]{2,1,0:T(8,128)(2,1)S(1)}, u32[]{:S(2)}, u32[]{:S(2)}) async-start(bf16[4,336,512]{2,1,0:T(8,128)(2,1)} %shard_map.147), calls=%async_computation.1 | async-start | bytes 2752512 | tf_op jit(solution)/shard_map/all_to_all | solution.py:357
  54.5 8.6 %collective-permute-start.2 = (bf16[256,256]{1,0:T(8,128)(2,1)S(1)}, bf16[256,256]{1,0:T(8,128)(2,1)S(1)}, u32[]{:S(2)}, u32[]{:S(2)}) collective-permute-start(bf16[256,256]{1,0:T(8,128)(2,1)S(1)} %get-tuple-element.47), channel_id=1, source_target_pairs={{0,8},{8,16},{16,24},{24,0},{1,9},{9,17},{17,25},{25,1},{2,10},{10... | collective-permute-start | bytes 393224 | tf_op jit(solution)/shard_map/ppermute | solution.py:362
  56.7 9.6 %collective-permute-start.3 = (bf16[256,256]{1,0:T(8,128)(2,1)S(1)}, bf16[256,256]{1,0:T(8,128)(2,1)S(1)}, u32[]{:S(2)}, u32[]{:S(2)}) collective-permute-start(bf16[256,256]{1,0:T(8,128)(2,1)S(1)} %get-tuple-element.48), channel_id=1, source_target_pairs={{0,16},{8,24},{16,0},{24,8},{1,17},{9,25},{17,1},{25,9},{2,18},{10... | collective-permute-start | bytes 393224 | tf_op jit(solution)/shard_map/ppermute | solution.py:362
  61.2 8.1 %collective-permute-start.4 = (bf16[256,256]{1,0:T(8,128)(2,1)S(1)}, bf16[256,256]{1,0:T(8,128)(2,1)S(1)}, u32[]{:S(2)}, u32[]{:S(2)}) collective-permute-start(bf16[256,256]{1,0:T(8,128)(2,1)S(1)} %get-tuple-element.49), channel_id=1, source_target_pairs={{0,24},{8,0},{16,8},{24,16},{1,25},{9,1},{17,9},{25,17},{2,26},{10... | collective-permute-start | bytes 393224 | tf_op jit(solution)/shard_map/ppermute | solution.py:362
  71.1 12.8 %collective-permute-start.5 = (bf16[4,336,512]{2,1,0:T(8,128)(2,1)S(1)}, bf16[4,336,512]{2,1,0:T(8,128)(2,1)}, u32[]{:S(2)}, u32[]{:S(2)}) collective-permute-start(bf16[4,336,512]{2,1,0:T(8,128)(2,1)S(1)} %all-to-all-done.1.refs_0_), channel_id=1, source_target_pairs={{0,4},{4,0},{1,5},{5,1},{2,6},{6,2},{3,7},{7,3},{8,12},{12,8},{9,1... | collective-permute-start | bytes 4128776 | tf_op jit(solution)/shard_map/ppermute | solution.py:362
  74.6 0.9 copy-start.2
  75.4 0.9 copy-start.4
  76.3 0.9 copy-start.6
  77.1 22.6 %all-to-all-start.2 = ((bf16[16,24,256]{2,1,0:T(8,128)(2,1)}), bf16[16,24,256]{2,1,0:T(8,128)(2,1)S(1)}, u32[]{:S(2)}, u32[]{:S(2)}) async-start(bf16[16,24,256]{2,1,0:T(8,128)(2,1)} %bitcast.10), calls=%async_computation.2 | async-start | bytes 393216 | tf_op jit(solution)/shard_map/all_to_all | solution.py:357
  83.9 1.1 copy-start.3
  85.0 1.1 copy-start.5
  86.1 1.1 copy-start.7
  92.0 7.8 %copy-start.1 = (f32[1024]{0:T(1024)S(1)}, f32[1024]{0:T(1024)}, u32[]{:S(2)}) copy-start(f32[1024]{0:T(1024)} %param.17) | copy-start | bytes 12292
  92.0 7.8 %collective-permute-start.6 = (bf16[4,336,256]{2,1,0:T(8,128)(2,1)}, bf16[4,336,256]{2,1,0:T(8,128)(2,1)S(1)}, u32[]{:S(2)}, u32[]{:S(2)}) collective-permute-start(bf16[4,336,256]{2,1,0:T(8,128)(2,1)} %get-tuple-element.55), channel_id=1, source_target_pairs={{0,4},{4,0},{1,5},{5,1},{2,6},{6,2},{3,7},{7,3},{8,12},{12,8},{9,1... | collective-permute-start | bytes 2064392 | tf_op jit(solution)/shard_map/ppermute | solution.py:362
  101.5 15.8 %all-to-all-start.3 = ((bf16[4,336,256]{2,1,0:T(8,128)(2,1)}), bf16[4,336,256]{2,1,0:T(8,128)(2,1)S(1)}, u32[]{:S(2)}, u32[]{:S(2)}) async-start(bf16[4,336,256]{2,1,0:T(8,128)(2,1)} %shard_map.153), calls=%async_computation.3 | async-start | bytes 1376256 | tf_op jit(solution)/shard_map/all_to_all | solution.py:357
  118.6 32.9 %all-to-all-start.4 = ((bf16[64,8,256]{2,1,0:T(8,128)(2,1)}), bf16[64,8,256]{2,1,0:T(8,128)(2,1)S(1)}, u32[]{:S(2)}, u32[]{:S(2)}) async-start(bf16[64,8,256]{2,1,0:T(8,128)(2,1)} %bitcast.13), calls=%async_computation.4 | async-start | bytes 524288 | tf_op jit(solution)/shard_map/all_to_all | solution.py:357
  130.9 6.7 %collective-permute-start.7 = (bf16[512,256]{1,0:T(8,128)(2,1)S(1)}, bf16[512,256]{1,0:T(8,128)(2,1)S(1)}, u32[]{:S(2)}, u32[]{:S(2)}) collective-permute-start(bf16[512,256]{1,0:T(8,128)(2,1)S(1)} %all_gather.7.refs_2_), channel_id=1, source_target_pairs={{0,4},{4,0},{1,5},{5,1},{2,6},{6,2},{3,7},{7,3},{8,12},{12,8},{9,1... | collective-permute-start | bytes 786440 | tf_op jit(solution)/shard_map/ppermute | solution.py:362
